TPU v7x, 256 devices: a whole 4x4x8 slice. The times are simulated.
256 devices in a mesh: sp: 32 (over z, x), tp: 8 (over y, core).
Axes of the slice: x: 4, y: 4, z: 8, core: 2. Of those that a mesh axis runs over, the one named last changes fastest.
Arguments:
- resid: bfloat16 [12288, 2048], P('sp'), may hold values from -6 to 6
- cotangent: bfloat16 [12288, 2048], P('sp'), may hold values from -0.59765625 to 0.59765625
- routes: int32 [12288, 2], P('sp'), may hold values from 0 to 31, all different within a row; in each aligned block of 384 rows (0 to 383, 384 to 767, ...) at most 48 rows name the same one
- route_weight: float32 [12288, 2], P('sp'), may hold values from 0.3 to 2.2
- w_gate: bfloat16 [32, 2048, 1024], P('sp', None, 'tp'), may hold values from -0.125 to 0.125
- w_up: bfloat16 [32, 2048, 1024], P('sp', None, 'tp'), may hold values from -0.125 to 0.125
- w_down: bfloat16 [32, 1024, 2048], P('sp', 'tp'), may hold values from -0.1875 to 0.1875
- out_proj: bfloat16 [2048, 2816], P(None, 'tp'), may hold values from -0.109375 to 0.109375
- gate_pre: bfloat16 [12288, 2816], P('sp', 'tp'), may hold values from -8 to 8
- log_decay: float32 [12288, 2816], P('sp', 'tp'), may hold values from -1 to 0
- state_before: float32 [12288, 2816], P('sp', 'tp'), may hold values from -6 to 6
- step_input: bfloat16 [12288, 2816], P('sp', 'tp'), may hold values from -6 to 6
Outputs:
- grad_gate: float32 [32, 2048, 1024], P('sp', None, 'tp')
- grad_up: float32 [32, 2048, 1024], P('sp', None, 'tp')
- grad_down: float32 [32, 1024, 2048], P('sp', 'tp')
- grad_proj: float32 [2048, 2816], P('sp', 'tp')
- grad_gate_pre: bfloat16 [12288, 2816], P('sp', 'tp')
- grad_step_input: float32 [12288, 2816], P('sp', 'tp')
- grad_log_decay: float32 [12288, 2816], P('sp', 'tp')
Inputs may be any that keep to these rules, and one draw needn't show every extreme that they name: `routes`: each row names 2 different experts. In the rows of one device no expert is named more than 48 times; some expert is named exactly 48 times in the rows of some devices.
All inputs are finite; a program needn't handle non-finite values.
Results may differ from a plain program's by a relative error of at most 0.02.
Values may be sent and summed in bfloat16 or wider, within the bound.
No kernel may reach another device: no remote copies, remote signals or barrier semaphores. Data moves between devices by JAX's collectives and lax.ppermute only.
A program may use at most 128 MiB of HBM per device.

v0:
```python
import functools

import jax
import jax.numpy as jnp
from jax import lax
from jax.experimental import pallas as pl
from jax.experimental.pallas import tpu as pltpu
from jax.sharding import Mesh, PartitionSpec as P


BF16 = jnp.bfloat16
F32 = jnp.float32
SP = ("z", "x")
TP = ("y", "c")
ALL = ("z", "x", "y", "c")

TOK = 384
D = 2048
CAP = 48
N_EXP = 32
N_TP = 8
PART = CAP // N_TP
ROWS = N_EXP * PART
CH = 352
STRIP = 32
GELU_C = 0.7978845608028654
GELU_A = 0.044715


def iota(shape, dim):
    return lax.broadcasted_iota(jnp.int32, shape, dim)


def in_hbm(*arrays):
    held = tuple(pltpu.with_memory_space_constraint(a, pltpu.HBM) for a in arrays)
    return held if len(held) > 1 else held[0]


def vmem(mib):
    return pltpu.CompilerParams(vmem_limit_bytes=mib * 1024 * 1024)


def dot(a, b):
    return jnp.dot(a, b, preferred_element_type=F32)


def dot_nt(a, b):
    return lax.dot_general(a, b, (((1,), (1,)), ((), ())), preferred_element_type=F32)


def dot_tn(a, b):
    return lax.dot_general(a, b, (((0,), (0,)), ((), ())), preferred_element_type=F32)


FIRST = (6, 4, 2)


def pack_kernel(gate_ref, up_ref, down_ref, a_ref, b_ref, abuf, bbuf, down_buf, sems):
    third = D // 2
    loads = [
        pltpu.make_async_copy(down_ref, down_buf, sems.at[0]),
        pltpu.make_async_copy(gate_ref, abuf.at[pl.ds(0, D)], sems.at[1]),
        pltpu.make_async_copy(up_ref.at[pl.ds(0, third)], abuf.at[pl.ds(D, third)], sems.at[2]),
        pltpu.make_async_copy(up_ref.at[pl.ds(third, third)], bbuf.at[pl.ds(0, third)], sems.at[3]),
    ]
    for load in loads:
        load.start()
    loads[1].wait()
    loads[2].wait()
    out_a = pltpu.make_async_copy(abuf, a_ref, sems.at[4])
    out_a.start()
    loads[0].wait()
    bbuf[third:, :] = down_buf[...].T
    loads[3].wait()
    out_b = pltpu.make_async_copy(bbuf, b_ref, sems.at[5])
    out_b.start()
    out_a.wait()
    out_b.wait()


def pack(gate, up, down):
    anywhere = pl.BlockSpec(memory_space=pl.ANY)
    half = pltpu.HBM((3 * D // 2, 128), BF16)
    return pl.pallas_call(
        pack_kernel,
        in_specs=[anywhere] * 3,
        out_specs=(anywhere, anywhere),
        out_shape=(half, half),
        scratch_shapes=[
            pltpu.VMEM((3 * D // 2, 128), BF16),
            pltpu.VMEM((3 * D // 2, 128), BF16),
            pltpu.VMEM((128, D), BF16),
            pltpu.SemaphoreType.DMA((6,)),
        ],
        compiler_params=vmem(4),
        name="pack",
    )(*in_hbm(gate, up, down))


def dispatch_kernel(tp_ref, routes_ref, weight_ref, res_a, res_b, cot_a, cot_b, out_ref, pick_ref, scale_ref):
    @pl.when(pl.program_id(0) == 0)
    def _():
        r0, r1 = routes_ref[0:1, :], routes_ref[1:2, :]
        e = iota((N_EXP, TOK), 0)
        oh0, oh1 = e == r0, e == r1
        member = jnp.where(oh0 | oh1, 1.0, 0.0).astype(BF16)
        before = jnp.where(iota((TOK, TOK), 0) < iota((TOK, TOK), 1), 1.0, 0.0).astype(BF16)
        rank = dot(member, before)
        s0 = r0 * CAP + jnp.sum(jnp.where(oh0, rank, 0.0), axis=0, keepdims=True).astype(jnp.int32)
        s1 = r1 * CAP + jnp.sum(jnp.where(oh1, rank, 0.0), axis=0, keepdims=True).astype(jnp.int32)
        row = iota((8 * N_EXP, TOK), 0)
        q = row & 7
        for j in range(3):
            first = q < FIRST[j]
            i = 8 * j + q - jnp.where(first, 6 * j, 6 * (j + 1))
            slot = (row >> 3) * CAP + PART * tp_ref[0] + i
            m0, m1 = slot == s0, slot == s1
            hit = m0 | m1
            pick_ref[j, :, :TOK] = jnp.where(hit & first, 1.0, 0.0).astype(BF16)
            pick_ref[j, :, TOK:] = jnp.where(hit & ~first, 1.0, 0.0).astype(BF16)
            w = jnp.where(m0, weight_ref[0:1, :], 0.0) + jnp.where(m1, weight_ref[1:2, :], 0.0)
            w = jnp.sum(w, axis=1, keepdims=True)
            cot_row = (q[:, 0:1] < FIRST[j]) if j % 2 else (q[:, 0:1] >= FIRST[j])
            scale_ref[j] = jnp.broadcast_to(jnp.where(cot_row, w, 1.0), (8 * N_EXP, 128))

    classes = (res_a, cot_a, res_b, cot_b)
    for j in range(3):
        rhs = jnp.concatenate([classes[j][...], classes[j + 1][...]], axis=0)
        got = dot(pick_ref[j], rhs) * scale_ref[j][:, 0:1]
        out_ref[:, 8 * j : 8 * j + 8, :] = got.reshape(N_EXP, 8, got.shape[1]).astype(BF16)


def dispatch(tp, routes_t, weight_t, resid, cotangent):
    bn = 256
    half = D // 2 // bn
    return pl.pallas_call(
        dispatch_kernel,
        grid_spec=pltpu.PrefetchScalarGridSpec(
            num_scalar_prefetch=1,
            grid=(half,),
            in_specs=[
                pl.BlockSpec((2, TOK), lambda n, s: (0, 0)),
                pl.BlockSpec((2, TOK), lambda n, s: (0, 0)),
                pl.BlockSpec((TOK, bn), lambda n, s: (0, n)),
                pl.BlockSpec((TOK, bn), lambda n, s: (0, n + half)),
                pl.BlockSpec((TOK, bn), lambda n, s: (0, n)),
                pl.BlockSpec((TOK, bn), lambda n, s: (0, n + half)),
            ],
            out_specs=pl.BlockSpec((N_EXP, 24, bn), lambda n, s: (0, 0, n)),
            scratch_shapes=[
                pltpu.VMEM((3, 8 * N_EXP, 2 * TOK), BF16),
                pltpu.VMEM((3, 8 * N_EXP, 128), F32),
            ],
        ),
        out_shape=pltpu.HBM((N_EXP, 24, D // 2), BF16),
        compiler_params=vmem(14),
        name="dispatch",
    )(tp, routes_t, weight_t, resid, resid, cotangent, cotangent)


def place_kernel(routes_ref, out_ref):
    r0, r1 = routes_ref[:, 0:1], routes_ref[:, 1:2]
    e = iota((TOK, N_EXP), 1)
    oh0, oh1 = e == r0, e == r1
    member = jnp.where(oh0 | oh1, 1.0, 0.0).astype(BF16)
    before = jnp.where(iota((TOK, TOK), 1) < iota((TOK, TOK), 0), 1.0, 0.0).astype(BF16)
    rank = dot(before, member)

    def line(oh, r):
        k = jnp.sum(jnp.where(oh, rank, 0.0), axis=1, keepdims=True).astype(jnp.int32)
        t = (k * 43) >> 8
        return r * 64 + t * 8 + (k - t * PART)

    col = iota((TOK, 8 * N_TP * N_EXP), 1)
    hit = (col == line(oh0, r0)) | (col == line(oh1, r1))
    out_ref[...] = jnp.where(hit, 1.0, 0.0).astype(BF16)


def place(routes):
    return pl.pallas_call(
        place_kernel,
        out_shape=pltpu.HBM((TOK, 8 * N_TP * N_EXP), BF16),
        compiler_params=vmem(8),
        name="place",
    )(routes)


def select_kernel(got_ref, rows_ref):
    tiles = [
        got_ref[:, 8 * j : 8 * j + 8, :].astype(F32).reshape(8 * N_EXP, D // 2).astype(BF16) for j in range(3)
    ]
    k = iota((ROWS, 8 * N_EXP), 0)
    col = iota((ROWS, 8 * N_EXP), 1)
    source, q = col >> 3, col & 7
    for cls in range(4):
        total = None
        for j in (cls - 1, cls):
            if 0 <= j < 3:
                i = 8 * j + q - 6 * cls
                sel = jnp.where((k == source * PART + i) & (i >= 0) & (i < PART), 1.0, 0.0).astype(BF16)
                part = dot(sel, tiles[j])
                total = part if total is None else total + part
        rows_ref[cls % 2, :, (cls // 2) * (D // 2) : (cls // 2 + 1) * (D // 2)] = total.astype(BF16)


def select(got):
    return pl.pallas_call(
        select_kernel,
        out_shape=pltpu.HBM((2, ROWS, D), BF16),
        compiler_params=vmem(12),
        name="select",
    )(got)


def expert_kernel(rows_ref, *refs):
    weights, out_ref, acts_ref = refs[:16], refs[16], refs[17]
    gate_up, down, grads, sems = refs[18:]
    mid = D // 2
    copies = [[], [], [], []]
    for j in range(4):
        for side in range(2):
            part_a, part_b = weights[8 * side + 2 * j], weights[8 * side + 2 * j + 1]
            at = 128 * side
            g, u, d = pl.ds(512 * j + at, 128), pl.ds(512 * j + 256 + at, 128), pl.ds(256 * j + at, 128)
            moves = (
                (part_a.at[pl.ds(0, D)], gate_up.at[:, g]),
                (part_a.at[pl.ds(D, mid)], gate_up.at[pl.ds(0, mid), u]),
                (part_b.at[pl.ds(0, mid)], gate_up.at[pl.ds(mid, mid), u]),
                (part_b.at[pl.ds(mid, D)], down.at[:, d]),
            )
            for n, (src, dst) in enumerate(moves):
                copies[j].append(pltpu.make_async_copy(src, dst, sems.at[j, 4 * side + n]))
    for group in copies:
        for copy in group:
            copy.start()

    def chunk(j, _):
        for n in range(4):
            @pl.when(j == n)
            def _():
                for copy in copies[n]:
                    copy.wait()

        at = pl.multiple_of(512 * j, 512)
        both = dot(rows_ref[0], gate_up[:, pl.ds(at, 512)])
        gate, up = both[:, :256], both[:, 256:]
        d_hidden = dot(rows_ref[1], down[:, pl.ds(pl.multiple_of(256 * j, 256), 256)])
        sig = jax.nn.sigmoid(gate)
        silu = gate * sig
        d_gate = (d_hidden * up * (sig * (1.0 + gate * (1.0 - sig)))).astype(BF16)
        d_up = (d_hidden * silu).astype(BF16)
        acts_ref[j, 0] = d_gate
        acts_ref[j, 1] = d_up
        acts_ref[j, 2] = (silu * up).astype(BF16)
        grads[:, pl.ds(at, 256)] = d_gate
        grads[:, pl.ds(pl.multiple_of(at + 256, 256), 256)] = d_up
        return 0

    lax.fori_loop(0, 4, chunk, 0)
    line = iota((8 * N_EXP, ROWS), 0)
    spread = (iota((8 * N_EXP, ROWS), 1) == (line >> 3) * PART + (line & 7)) & ((line & 7) < PART)
    spread = jnp.where(spread, 1.0, 0.0).astype(BF16)

    def columns(t, _):
        rows = pl.ds(pl.multiple_of(256 * t, 256), 256)
        back = dot(spread, dot_nt(grads[...], gate_up[rows, :]).astype(BF16)).reshape(N_EXP, 8, 256)
        for h in range(2):
            out_ref[:, t, 8 * h : 8 * h + 8, :] = back[:, :, 128 * h : 128 * h + 128].astype(BF16)
        return 0

    lax.fori_loop(0, N_TP, columns, 0)


def experts(rows, weights):
    return pl.pallas_call(
        expert_kernel,
        in_specs=[pl.BlockSpec(memory_space=pltpu.VMEM)] + [pl.BlockSpec(memory_space=pl.ANY)] * 16,
        out_shape=(pltpu.HBM((N_EXP, N_TP, 16, 128), BF16), pltpu.HBM((4, 3, ROWS, 256), BF16)),
        scratch_shapes=[
            pltpu.VMEM((D, D), BF16),
            pltpu.VMEM((D, D // 2), BF16),
            pltpu.VMEM((ROWS, D), BF16),
            pltpu.SemaphoreType.DMA((4, 8)),
        ],
        compiler_params=vmem(32),
        name="experts",
    )(*in_hbm(rows, *weights))


def weight_grad_kernel(*refs):
    rows, far, acts = refs[0:3], refs[3:5], refs[5:9]
    keep_ref, send_ref, xbuf, hbuf, sems = refs[9:]
    copies = []
    for n in range(4):
        at = pl.ds(ROWS * n, ROWS)
        if n < 3:
            copies.append(pltpu.make_async_copy(rows[n], xbuf.at[:, at, :], sems.at[0, n]))
        act = acts[n].at[0] if n == 0 else acts[n]
        copies.append(pltpu.make_async_copy(act, hbuf.at[:, at, :], sems.at[1, n]))
    for n in range(2):
        copies.append(pltpu.make_async_copy(far[n], xbuf.at[n, pl.ds(3 * ROWS, ROWS), :], sems.at[0, 3 + n]))
    for copy in copies:
        copy.start()
    for copy in copies:
        copy.wait()

    def columns(t, _):
        cols = pl.ds(pl.multiple_of(256 * t, 256), 256)
        for n in range(2):
            both = dot_tn(xbuf[0, :, cols], hbuf[n])
            rows = pl.ds(pl.multiple_of(D * n + 256 * t, 256), 256)
            keep_ref[rows, :] = both[:, :128]
            send_ref[rows, :] = both[:, 128:]
        both = dot_tn(hbuf[2], xbuf[1, :, cols])
        for h in range(2):
            rows = pl.ds(pl.multiple_of(2 * D + 256 * t + 128 * h, 128), 128)
            keep_ref[rows, :] = both[:128, 128 * h : 128 * h + 128]
            send_ref[rows, :] = both[128:, 128 * h : 128 * h + 128]
        return 0

    lax.fori_loop(0, N_TP, columns, 0)


def weight_grads(rows, far, acts):
    part = pltpu.HBM((3 * D, 128), F32)
    return pl.pallas_call(
        weight_grad_kernel,
        in_specs=[pl.BlockSpec(memory_space=pl.ANY)] * 9,
        out_shape=(part, part),
        scratch_shapes=[
            pltpu.VMEM((2, 4 * ROWS, D), BF16),
            pltpu.VMEM((3, 4 * ROWS, 256), BF16),
            pltpu.SemaphoreType.DMA((2, 5)),
        ],
        compiler_params=vmem(26),
        name="weight_grads",
    )(*in_hbm(*rows, *far, *acts))


def finish_kernel(keep_g, keep_u, keep_d, got_g, got_u, got_d, gate_ref, up_ref, down_ref):
    gate_ref[...] = keep_g[...] + got_g[...]
    up_ref[...] = keep_u[...] + got_u[...]
    for n in range(4):
        rows = slice(128 * n, 128 * n + 128)
        down_ref[:, rows] = keep_d[rows, :] + got_d[rows, :]


def finish(keep, got):
    block = 512
    count = D // block
    tall = [pl.BlockSpec((block, 128), functools.partial(lambda k, n: (n + k * count, 0), k)) for k in range(3)]
    return pl.pallas_call(
        finish_kernel,
        grid=(count,),
        in_specs=tall + tall,
        out_specs=(tall[0], tall[0], pl.BlockSpec((128, block), lambda n: (0, n))),
        out_shape=(
            jax.ShapeDtypeStruct((D, 128), F32),
            jax.ShapeDtypeStruct((D, 128), F32),
            jax.ShapeDtypeStruct((128, D), F32),
        ),
        compiler_params=vmem(8),
        name="finish",
    )(*[in_hbm(keep)] * 3, *[in_hbm(got)] * 3)


def combine_kernel(tp_ref, place_ref, back_ref, cot_ref, out_ref):
    halves = [
        back_ref[:, 8 * h : 8 * h + 8, :].astype(F32).reshape(8 * N_TP * N_EXP, 128).astype(BF16) for h in range(2)
    ]
    routed = dot(place_ref[...], jnp.concatenate(halves, axis=1))
    out_ref[...] = (cot_ref[...].astype(F32) + routed).T.astype(BF16)


def combine(tp, placed, back, cotangent):
    cols = D // N_TP
    return pl.pallas_call(
        combine_kernel,
        grid_spec=pltpu.PrefetchScalarGridSpec(
            num_scalar_prefetch=1,
            grid=(1,),
            in_specs=[
                pl.BlockSpec(placed.shape, lambda n, s: (0, 0)),
                pl.BlockSpec(back.shape, lambda n, s: (0, 0, 0)),
                pl.BlockSpec((TOK, cols), lambda n, s: (0, s[0])),
            ],
            out_specs=pl.BlockSpec((cols, TOK), lambda n, s: (0, 0)),
        ),
        out_shape=jax.ShapeDtypeStruct((cols, TOK), BF16),
        compiler_params=vmem(12),
        name="combine",
    )(tp, in_hbm(placed), back, cotangent)


def prepare_kernel(gate_ref, log_ref, before_ref, step_ref, mixed_ref, gelu_ref, slope_ref, prefix_ref, suffix_ref, turn_ref):
    lane = iota((STRIP, TOK), 1)
    turn_ref[...] = jnp.zeros_like(turn_ref)

    def strip(n, _):
        at = pl.ds(pl.multiple_of(n * STRIP, STRIP), STRIP)
        x = gate_ref[at, :].astype(F32)
        th = jnp.tanh(GELU_C * (x + GELU_A * (x * x * x)))
        gelu = 0.5 * x * (1.0 + th)
        back = 0.5 * (1.0 + th) + 0.5 * x * (1.0 - th * th) * (GELU_C * (1.0 + 3.0 * GELU_A * (x * x)))
        logs = log_ref[at, :]
        states = jnp.exp(logs) * before_ref[at, :] + step_ref[at, :].astype(F32)
        turn_ref[at, :] = gelu * states
        gelu_ref[at, :] = gelu
        slope_ref[at, :] = states * back
        total = logs
        d = 1
        while d < TOK:
            total = total + jnp.where(lane >= d, pltpu.roll(total, d, 1), 0.0)
            d *= 2
        prefix_ref[at, :] = jnp.exp(total)
        suffix_ref[at, :] = jnp.exp(total[:, TOK - 1 : TOK] - total)
        return 0

    lax.fori_loop(0, CH // STRIP, strip, 0)
    mixed_ref[...] = turn_ref[...].T[:, :CH].astype(BF16)


def prepare(gate_pre, log_decay, state_before, step_input):
    shape = gate_pre.shape
    wide = pltpu.HBM(shape, F32)
    return pl.pallas_call(
        prepare_kernel,
        out_shape=(pltpu.HBM(shape[::-1], BF16), wide, wide, wide, wide),
        scratch_shapes=[pltpu.VMEM((TOK, TOK), F32)],
        compiler_params=vmem(8),
        name="prepare",
    )(gate_pre, log_decay, state_before, step_input)


def project_kernel(order_ref, *refs):
    grads, (proj_ref, mixed_ref, gelu_ref, slope_ref, prefix_ref) = refs[:8], refs[8:13]
    pieces, (ggp_ref, direct_ref, link_ref, block_ref, turn_ref) = refs[13:17], refs[17:]
    d_mixed = jnp.zeros((CH, TOK), F32)
    for k in range(N_TP):
        group = order_ref[k]
        grad = grads[k][...]
        cols = pl.ds(pl.multiple_of(group * 256, 256), 256)
        d_mixed = d_mixed + dot(proj_ref[:, cols], grad)
        block_ref[...] = dot(grad, mixed_ref[...])
        for m in range(4):
            at = pl.ds(pl.multiple_of(((order_ref[8] + m) & 3) * 64, 64), 64)
            pieces[m][pl.ds(group, 1)] = block_ref[at, :].astype(BF16)[None]
    ggp_ref[...] = (d_mixed * slope_ref[...]).astype(BF16)
    direct = d_mixed * gelu_ref[...]
    direct_ref[...] = direct
    turn_ref[...] = jnp.zeros_like(turn_ref)
    turn_ref[0:CH, 0:1] = prefix_ref[:, TOK - 1 : TOK]
    turn_ref[0:CH, 1:2] = jnp.sum(prefix_ref[...] * direct, axis=1, keepdims=True)
    link_ref[...] = turn_ref[...].T[0:2, 0:CH]


def project(order, grads, out_proj, mixed, gelu, slope, prefix):
    piece = pltpu.HBM((8, 64, CH), BF16)
    return pl.pallas_call(
        project_kernel,
        in_specs=[pl.BlockSpec(memory_space=pltpu.SMEM)] + [pl.BlockSpec(memory_space=pltpu.VMEM)] * 13,
        out_shape=(
            piece, piece, piece, piece,
            pltpu.HBM((CH, TOK), BF16),
            pltpu.HBM((CH, TOK), F32),
            pltpu.HBM((2, CH), F32),
        ),
        scratch_shapes=[pltpu.VMEM((256, CH), F32), pltpu.VMEM((TOK, 128), F32)],
        compiler_params=vmem(14),
        name="project",
    )(order, *grads, out_proj, mixed, gelu, slope, prefix)


def local_kernel(direct_ref, log_ref, out_ref):
    lane = iota((STRIP, TOK), 1)

    def strip(n, _):
        at = pl.ds(pl.multiple_of(n * STRIP, STRIP), STRIP)
        a = jnp.where(lane < TOK - 1, pltpu.roll(jnp.exp(log_ref[at, :]), TOK - 1, 1), 1.0)
        b = direct_ref[at, :]
        d = 1
        while d < TOK:
            b = b + a * jnp.where(lane < TOK - d, pltpu.roll(b, TOK - d, 1), 0.0)
            if 2 * d < TOK:
                a = a * jnp.where(lane < TOK - d, pltpu.roll(a, TOK - d, 1), 1.0)
            d *= 2
        out_ref[at, :] = b
        return 0

    lax.fori_loop(0, CH // STRIP, strip, 0)


def local_scan(direct, log_decay):
    return pl.pallas_call(
        local_kernel,
        out_shape=jax.ShapeDtypeStruct((CH, TOK), F32),
        compiler_params=vmem(6),
        name="local_scan",
    )(direct, log_decay)


def recur_kernel(at_ref, links_ref, local_ref, suffix_ref, log_ref, before_ref, step_ref, decay_ref, turn_ref):
    mine = at_ref[0]
    arriving = jnp.zeros((1, CH), F32)
    for s in range(N_EXP - 1, 0, -1):
        arriving = jnp.where(s > mine, links_ref[s, 1:2, :] + links_ref[s, 0:1, :] * arriving, arriving)
    turn_ref[...] = jnp.zeros_like(turn_ref)
    turn_ref[0:1, 0:CH] = arriving
    column = turn_ref[...].T[:CH, 0:1]
    g = local_ref[...] + suffix_ref[...] * column
    step_ref[...] = g
    decay_ref[...] = g * jnp.exp(log_ref[...]) * before_ref[...]


def recur(at, links, local, suffix, log_decay, state_before):
    return pl.pallas_call(
        recur_kernel,
        in_specs=[pl.BlockSpec(memory_space=pltpu.SMEM)] + [pl.BlockSpec(memory_space=pltpu.VMEM)] * 5,
        out_shape=(
            jax.ShapeDtypeStruct((CH, TOK), F32),
            jax.ShapeDtypeStruct((CH, TOK), F32),
        ),
        scratch_shapes=[pltpu.VMEM((128, TOK), F32)],
        compiler_params=vmem(8),
        name="recur",
    )(at, links, local, suffix, log_decay, state_before)


def shifted(value, axis, by):
    n = lax.axis_size(axis)
    return lax.ppermute(value, axis, [(i, (i + by) % n) for i in range(n)])


def on_device(resid, cotangent, routes, route_weight, w_gate, w_up, w_down, out_proj, gate_pre, log_decay,
              state_before, step_input):
    y, c = lax.axis_index("y"), lax.axis_index("c")
    tp = (2 * y + c).astype(jnp.int32)
    tp_vec = tp[None]

    own_a, own_b = pack(w_gate[0], w_up[0], w_down[0])
    prev_a = shifted(own_a, "y", 1)
    next_b = shifted(own_b, "y", -1)
    prev_b = shifted(own_b, "y", 1)
    next_a = shifted(own_a, "y", -1)
    far_a = shifted(prev_a, "y", 1)
    far_b = shifted(next_b, "y", -1)
    mine = (own_a, own_b, prev_a, prev_b, next_a, next_b, far_a, far_b)
    weights = mine + tuple(shifted(w, "c", 1) for w in mine)

    sent = dispatch(tp_vec, routes.T, route_weight.T, resid, cotangent)
    got = lax.all_to_all(sent, SP, split_axis=0, concat_axis=0, tiled=True)

    placed = place(routes)
    log_t, before_t = log_decay.T, state_before.T
    mixed, gelu, slope, prefix, suffix = prepare(gate_pre.T, log_t, before_t, step_input.T)
    ys = jnp.stack([y, y - 1, y + 1, y + 2]) % 4
    order = jnp.concatenate([2 * ys + c, 2 * ys + 1 - c, lax.axis_index("x")[None]]).astype(jnp.int32)
    got, order = lax.optimization_barrier((got, order))

    rows = select(got)
    rows_after = shifted(rows, "y", -1)
    rows_before = shifted(rows, "y", 1)
    back, acts = experts(rows, weights)
    back = lax.all_to_all(back.reshape(N_EXP * N_TP, 16, 128), ALL, split_axis=0, concat_axis=0, tiled=True)
    all_acts = [acts]
    for j, by in ((1, -1), (2, 1), (3, 2)):
        all_acts.append(shifted(acts[j], "y", by))
    part = combine(tp_vec, placed, back, cotangent)

    near = (part, shifted(part, "y", 1), shifted(part, "y", -1), shifted(part, "y", 2))
    grads = (*near, *(shifted(g, "c", 1) for g in near))
    *pieces, grad_gate_pre, direct, link = project(order, grads, out_proj.T, mixed, gelu, slope, prefix)

    far_in, far_cot, pieces[0] = lax.optimization_barrier((rows_before[0], rows_after[1], pieces[0]))

    over_x = [pieces[0]]
    for m in (1, 2, 3):
        over_x.append(shifted(pieces[m], "x", m))
    link = jnp.broadcast_to(link, (N_EXP, *link.shape))
    links = lax.all_to_all(link, SP, split_axis=0, concat_axis=0, tiled=True)
    over_x = sum(p.astype(F32) for p in over_x).astype(BF16)
    over_z = lax.all_to_all(over_x, "z", split_axis=0, concat_axis=0, tiled=True)
    grad_proj = over_z.astype(F32).sum(axis=0)

    sp = (4 * lax.axis_index("z") + lax.axis_index("x")).astype(jnp.int32)
    local = local_scan(direct, log_t)
    grad_step_input, grad_log_decay = recur(sp[None], links, local, suffix, log_t, before_t)

    far_in = shifted(far_in, "y", 1)
    far_cot = shifted(far_cot, "y", -1)
    far = (far_in, far_cot)
    keep, send = weight_grads((rows, rows_after, rows_before), far, all_acts)
    send = shifted(send, "c", 1)
    grad_gate, grad_up, grad_down = finish(keep, send)
    return (
        grad_gate[None],
        grad_up[None],
        grad_down[None],
        grad_proj,
        grad_gate_pre.T,
        grad_step_input.T,
        grad_log_decay.T,
    )


def solution(mesh):
    grid = Mesh(mesh.devices.reshape(8, 4, 4, 2), ALL)


    return jax.shard_map(
        on_device,
        mesh=grid,
        in_specs=(
            P(SP, None),
            P(SP, None),
            P(SP, None),
            P(SP, None),
            P(SP, None, TP),
            P(SP, None, TP),
            P(SP, TP, None),
            P(None, TP),
            P(SP, TP),
            P(SP, TP),
            P(SP, TP),
            P(SP, TP),
        ),
        out_specs=(
            P(SP, None, TP),
            P(SP, None, TP),
            P(SP, TP, None),
            P(SP, TP),
            P(SP, TP),
            P(SP, TP),
            P(SP, TP),
        ),
        check_vma=False,
    )
```

profile of v0, /device:TPU:8, one launch (start us, length us, event | category | flops | bytes accessed | tf_op | source)
XLA Modules:
  0.0 269.1 jit_solution(1410312270652588478)
XLA Ops:
  4.8 4.1 %dispatch.1 = bf16[32,24,1024]{2,1,0:T(8,128)(2,1)} custom-call(s32[1]{0:T(128)} %bitcast.tp_ref, s32[2,384]{1,0:T(2,128)S(1)} %bitcast.42, f32[2,384]{1,0:T(2,128)S(1)} %bitcast.43, bf16[384,2048]{1,0:T(8,128)(2,1)S(1)} %copy-done.2, bf16[384,2048]{1,0:T(8,128)(2,1)S(1)} %copy-done.2, bf16[384,2048]{1,0:T(8,128)(2,1)S(1)} %copy-done, ...), custom_call_target="tpu_custom_call" | custom-call | tf_op jit(solution)/shard_map/dispatch/pallas_call | solution.py:136
  9.0 11.3 %all-to-all-start = ((bf16[32,24,1024]{2,1,0:T(8,128)(2,1)}), bf16[32,24,1024]{2,1,0:T(8,128)(2,1)S(1)}, u32[]{:S(2)}, u32[]{:S(2)}) async-start(bf16[32,24,1024]{2,1,0:T(8,128)(2,1)} %dispatch.1), calls=%async_computation | async-start | bytes 3145728 | tf_op jit(solution)/shard_map/all_to_all | solution.py:551
  26.9 16.6 %collective-permute-done.2.refs_2_ = bf16[3072,128]{1,0:T(8,128)(2,1)S(1)} collective-permute-done((bf16[3072,128]{1,0:T(8,128)(2,1)}, bf16[3072,128]{1,0:T(8,128)(2,1)S(1)}, u32[]{:S(2)}, u32[]{:S(2)}) %collective-permute-start.2) | collective-permute-done | bytes 786464 | tf_op jit(solution)/shard_map/ppermute | solution.py:531
  46.4 14.0 %collective-permute-done.3.refs_3_ = bf16[3072,128]{1,0:T(8,128)(2,1)} collective-permute-done((bf16[3072,128]{1,0:T(8,128)(2,1)}, bf16[3072,128]{1,0:T(8,128)(2,1)}, u32[]{:S(2)}, u32[]{:S(2)}) %collective-permute-start.3) | collective-permute-done | bytes 786464 | tf_op jit(solution)/shard_map/ppermute | solution.py:531
  62.7 13.1 %collective-permute-done.6.refs_6_ = bf16[3072,128]{1,0:T(8,128)(2,1)} collective-permute-done((bf16[3072,128]{1,0:T(8,128)(2,1)S(1)}, bf16[3072,128]{1,0:T(8,128)(2,1)}, u32[]{:S(2)}, u32[]{:S(2)}) %collective-permute-start.6) | collective-permute-done | bytes 786464 | tf_op jit(solution)/shard_map/ppermute | solution.py:531
  81.2 14.1 %experts.1 = (bf16[32,8,16,128]{3,2,1,0:T(8,128)(2,1)}, bf16[4,3,192,256]{3,2,1,0:T(8,128)(2,1)}) custom-call(bf16[2,192,2048]{2,1,0:T(8,128)(2,1)} %select.3.rows_ref.refs_0_, bf16[3072,128]{1,0:T(8,128)(2,1)} %get-tuple-element.37.refs_0_, bf16[3072,128]{1,0:T(8,128)(2,1)} %get-tuple-element.38.refs_1_, bf16[3072,128]{1,0:T(8,128)(2,1)} %copy-done.19, ...), custom_call_target="tpu_custom_call" | custom-call | tf_op jit(solution)/shard_map/experts/pallas_call | solution.py:275
  95.4 13.5 %all-to-all-start.1 = ((bf16[256,16,128]{2,1,0:T(8,128)(2,1)}), bf16[256,16,128]{2,1,0:T(8,128)(2,1)S(1)}, u32[]{:S(2)}, u32[]{:S(2)}) async-start(bf16[256,16,128]{2,1,0:T(8,128)(2,1)} %bitcast.44), calls=%async_computation.1 | async-start | bytes 2097152 | tf_op jit(solution)/shard_map/all_to_all | solution.py:564
  116.4 8.1 %prepare.1 = (bf16[384,352]{1,0:T(8,128)(2,1)}, f32[352,384]{1,0:T(8,128)}, f32[352,384]{1,0:T(8,128)}, f32[352,384]{1,0:T(8,128)}, f32[352,384]{1,0:T(8,128)}) custom-call(bf16[352,384]{1,0:T(8,128)(2,1)S(1)} %bitcast.40, f32[352,384]{1,0:T(8,128)S(1)} %bitcast.34, f32[352,384]{1,0:T(8,128)S(1)} %bitcast.37, bf16[352,384]{1,0:T(8,128)(2,1)S(1)} %bitcast.41), custom_call_target="tpu_custom_call" | custom-call | tf_op jit(solution)/shard_map/prepare/pallas_call | solution.py:426
  124.6 14.9 %all-to-all-done.1.back_ref = bf16[256,16,128]{2,1,0:T(8,128)(2,1)S(1)} async-done(((bf16[256,16,128]{2,1,0:T(8,128)(2,1)}), bf16[256,16,128]{2,1,0:T(8,128)(2,1)S(1)}, u32[]{:S(2)}, u32[]{:S(2)}) %all-to-all-start.1) | async-done | bytes 1048608 | tf_op jit(solution)/shard_map/all_to_all | solution.py:564
  143.7 2.8 %collective-permute-start.18 = (bf16[256,384]{1,0:T(8,128)(2,1)S(1)}, bf16[256,384]{1,0:T(8,128)(2,1)S(1)}, u32[]{:S(2)}, u32[]{:S(2)}) collective-permute-start(bf16[256,384]{1,0:T(8,128)(2,1)S(1)} %combine.1.refs_0_), channel_id=1, source_target_pairs={{0,4},{2,6},{4,0},{6,2},{1,5},{3,7},{5,1},{7,3},{8,12},{10,14},{12... | collective-permute-start | bytes 589832 | tf_op jit(solution)/shard_map/ppermute | solution.py:531
  146.6 10.4 %collective-permute-done.refs_1_ = bf16[2,192,2048]{2,1,0:T(8,128)(2,1)} collective-permute-done((bf16[2,192,2048]{2,1,0:T(8,128)(2,1)}, bf16[2,192,2048]{2,1,0:T(8,128)(2,1)}, u32[]{:S(2)}, u32[]{:S(2)}) %collective-permute-start) | collective-permute-done | bytes 1572896 | tf_op jit(solution)/shard_map/ppermute | solution.py:531
  158.2 3.7 %collective-permute-done.16.refs_1_ = bf16[256,384]{1,0:T(8,128)(2,1)S(1)} collective-permute-done((bf16[256,384]{1,0:T(8,128)(2,1)S(1)}, bf16[256,384]{1,0:T(8,128)(2,1)S(1)}, u32[]{:S(2)}, u32[]{:S(2)}) %collective-permute-start.16) | collective-permute-done | bytes 196640 | tf_op jit(solution)/shard_map/ppermute | solution.py:531
  162.5 3.1 %collective-permute-done.18.refs_3_ = bf16[256,384]{1,0:T(8,128)(2,1)S(1)} collective-permute-done((bf16[256,384]{1,0:T(8,128)(2,1)S(1)}, bf16[256,384]{1,0:T(8,128)(2,1)S(1)}, u32[]{:S(2)}, u32[]{:S(2)}) %collective-permute-start.18) | collective-permute-done | bytes 196640 | tf_op jit(solution)/shard_map/ppermute | solution.py:531
  167.0 4.2 %project.1 = (bf16[8,64,352]{2,1,0:T(8,128)(2,1)}, bf16[8,64,352]{2,1,0:T(8,128)(2,1)}, bf16[8,64,352]{2,1,0:T(8,128)(2,1)}, bf16[8,64,352]{2,1,0:T(8,128)(2,1)}...) custom-call(s32[9]{0:T(128)S(1)} %pad_add_fusion.order_ref, ...), custom_call_target="tpu_custom_call" | custom-call | tf_op jit(solution)/shard_map/project/pallas_call | solution.py:459
  174.0 3.3 %collective-permute-start.25 = (bf16[3,192,256]{2,1,0:T(8,128)(2,1)S(1)}, bf16[3,192,256]{2,1,0:T(8,128)(2,1)S(1)}, u32[]{:S(2)}, u32[]{:S(2)}) collective-permute-start(bf16[3,192,256]{2,1,0:T(8,128)(2,1)S(1)} %get-tuple-element.67), channel_id=1, source_target_pairs={{0,6},{2,0},{4,2},{6,4},{1,7},{3,1},{5,3},{7,5},{8,14},{10,8},{12,... | collective-permute-start | bytes 884744 | tf_op jit(solution)/shard_map/ppermute | solution.py:531
  179.5 18.6 %collective-permute-done.25.refs_6_ = bf16[3,192,256]{2,1,0:T(8,128)(2,1)S(1)} collective-permute-done((bf16[3,192,256]{2,1,0:T(8,128)(2,1)S(1)}, bf16[3,192,256]{2,1,0:T(8,128)(2,1)S(1)}, u32[]{:S(2)}, u32[]{:S(2)}) %collective-permute-start.25) | collective-permute-done | bytes 294944 | tf_op jit(solution)/shard_map/ppermute | solution.py:531
  198.6 7.6 %collective-permute-done.27.refs_8_ = bf16[3,192,256]{2,1,0:T(8,128)(2,1)S(1)} collective-permute-done((bf16[3,192,256]{2,1,0:T(8,128)(2,1)S(1)}, bf16[3,192,256]{2,1,0:T(8,128)(2,1)S(1)}, u32[]{:S(2)}, u32[]{:S(2)}) %collective-permute-start.27) | collective-permute-done | bytes 294944 | tf_op jit(solution)/shard_map/ppermute | solution.py:531
  208.1 10.4 %weight_grads.1 = (f32[6144,128]{1,0:T(8,128)}, f32[6144,128]{1,0:T(8,128)}) custom-call(bf16[2,192,2048]{2,1,0:T(8,128)(2,1)} %select.3.rows_ref.refs_0_, bf16[2,192,2048]{2,1,0:T(8,128)(2,1)} %collective-permute-done.refs_1_, bf16[2,192,2048]{2,1,0:T(8,128)(2,1)} %collective-permute-done.1.refs_2_, bf16[192,2048]{1,0:T(8,128)(2,1)} %copy-done.23, ...), custom_call_target="tpu_custom_call" | custom-call | tf_op jit(solution)/shard_map/weight_grads/pallas_call | solution.py:326
  224.8 6.8 %all-to-all-start.3 = ((f32[32,2,352]{2,1,0:T(2,128)}), f32[32,2,352]{2,1,0:T(2,128)S(1)}, u32[]{:S(2)}, u32[]{:S(2)}) async-start(f32[32,2,352]{2,1,0:T(2,128)} %broadcast_in_dim.27), calls=%async_computation.3 | async-start | bytes 196608 | tf_op jit(solution)/shard_map/all_to_all | solution.py:580
  231.6 10.1 %collective-permute-done.30 = bf16[8,64,352]{2,1,0:T(8,128)(2,1)S(1)} collective-permute-done((bf16[8,64,352]{2,1,0:T(8,128)(2,1)S(1)}, bf16[8,64,352]{2,1,0:T(8,128)(2,1)S(1)}, u32[]{:S(2)}, u32[]{:S(2)}) %collective-permute-start.30) | collective-permute-done | bytes 360480 | tf_op jit(solution)/shard_map/ppermute | solution.py:531
  242.7 6.5 %all-to-all-start.2 = ((bf16[8,64,352]{2,1,0:T(8,128)(2,1)}), bf16[8,64,352]{2,1,0:T(8,128)(2,1)S(1)}, u32[]{:S(2)}, u32[]{:S(2)}) async-start(bf16[8,64,352]{2,1,0:T(8,128)(2,1)} %add_convert_fusion), calls=%async_computation.2 | async-start | bytes 786432 | tf_op jit(solution)/shard_map/all_to_all | solution.py:582
  249.2 7.0 %local_scan.1.local_ref = f32[352,384]{1,0:T(8,128)S(1)} custom-call(f32[352,384]{1,0:T(8,128)S(1)} %copy-done.10, f32[352,384]{1,0:T(8,128)S(1)} %bitcast.35), custom_call_target="tpu_custom_call" | custom-call | tf_op jit(solution)/shard_map/local_scan/pallas_call | solution.py:494
  257.6 6.0 %all-to-all-done.2 = bf16[8,64,352]{2,1,0:T(8,128)(2,1)S(1)} async-done(((bf16[8,64,352]{2,1,0:T(8,128)(2,1)}), bf16[8,64,352]{2,1,0:T(8,128)(2,1)S(1)}, u32[]{:S(2)}, u32[]{:S(2)}) %all-to-all-start.2) | async-done | bytes 360480 | tf_op jit(solution)/shard_map/all_to_all | solution.py:582
  264.2 4.9 %finish.1 = (f32[2048,128]{1,0:T(8,128)}, f32[2048,128]{1,0:T(8,128)}, f32[128,2048]{1,0:T(8,128)}) custom-call(f32[6144,128]{1,0:T(8,128)} %get-tuple-element.48.keep_g.keep_u.keep_d, f32[6144,128]{1,0:T(8,128)} %get-tuple-element.48.keep_g.keep_u.keep_d, f32[6144,128]{1,0:T(8,128)} %get-tuple-element.48.keep_g.keep_u.keep_d, ...), custom_call_target="tpu_custom_call" | custom-call | tf_op jit(solution)/shard_map/finish/pallas_call | solution.py:352
  (134 shorter events, 52.9 us)
Async XLA Ops:
  9.0 70.1 %all-to-all-start = ((bf16[32,24,1024]{2,1,0:T(8,128)(2,1)}), bf16[32,24,1024]{2,1,0:T(8,128)(2,1)S(1)}, u32[]{:S(2)}, u32[]{:S(2)}) async-start(bf16[32,24,1024]{2,1,0:T(8,128)(2,1)} %dispatch.1), calls=%async_computation | async-start | bytes 3145728 | tf_op jit(solution)/shard_map/all_to_all | solution.py:551
  22.8 20.7 %collective-permute-start.2 = (bf16[3072,128]{1,0:T(8,128)(2,1)}, bf16[3072,128]{1,0:T(8,128)(2,1)S(1)}, u32[]{:S(2)}, u32[]{:S(2)}) collective-permute-start(bf16[3072,128]{1,0:T(8,128)(2,1)} %get-tuple-element.37.refs_0_), channel_id=1, source_target_pairs={{0,2},{2,4},{4,6},{6,0},{1,3},{3,5},{5,7},{7,1},{8,10},{10,12},{12... | collective-permute-start | bytes 2359304 | tf_op jit(solution)/shard_map/ppermute | solution.py:531
  24.4 20.7 %collective-permute-start.5 = (bf16[3072,128]{1,0:T(8,128)(2,1)}, bf16[3072,128]{1,0:T(8,128)(2,1)}, u32[]{:S(2)}, u32[]{:S(2)}) collective-permute-start(bf16[3072,128]{1,0:T(8,128)(2,1)} %get-tuple-element.38.refs_1_), channel_id=1, source_target_pairs={{0,6},{2,0},{4,2},{6,4},{1,7},{3,1},{5,3},{7,5},{8,14},{10,8},{12,... | collective-permute-start | bytes 2359304 | tf_op jit(solution)/shard_map/ppermute | solution.py:531
  24.9 35.6 %collective-permute-start.3 = (bf16[3072,128]{1,0:T(8,128)(2,1)}, bf16[3072,128]{1,0:T(8,128)(2,1)}, u32[]{:S(2)}, u32[]{:S(2)}) collective-permute-start(bf16[3072,128]{1,0:T(8,128)(2,1)} %get-tuple-element.38.refs_1_), channel_id=1, source_target_pairs={{0,2},{2,4},{4,6},{6,0},{1,3},{3,5},{5,7},{7,1},{8,10},{10,12},{12... | collective-permute-start | bytes 2359304 | tf_op jit(solution)/shard_map/ppermute | solution.py:531
  26.4 35.6 %collective-permute-start.4 = (bf16[3072,128]{1,0:T(8,128)(2,1)}, bf16[3072,128]{1,0:T(8,128)(2,1)}, u32[]{:S(2)}, u32[]{:S(2)}) collective-permute-start(bf16[3072,128]{1,0:T(8,128)(2,1)} %get-tuple-element.37.refs_0_), channel_id=1, source_target_pairs={{0,6},{2,0},{4,2},{6,4},{1,7},{3,1},{5,3},{7,5},{8,14},{10,8},{12,... | collective-permute-start | bytes 2359304 | tf_op jit(solution)/shard_map/ppermute | solution.py:531
  26.9 35.2 %collective-permute-start.8 = (bf16[3072,128]{1,0:T(8,128)(2,1)}, bf16[3072,128]{1,0:T(8,128)(2,1)S(1)}, u32[]{:S(2)}, u32[]{:S(2)}) collective-permute-start(bf16[3072,128]{1,0:T(8,128)(2,1)} %get-tuple-element.37.refs_0_), channel_id=1, source_target_pairs={{0,1},{1,0},{2,3},{3,2},{4,5},{5,4},{6,7},{7,6},{8,9},{9,8},{10,11... | collective-permute-start | bytes 2359304 | tf_op jit(solution)/shard_map/ppermute | solution.py:531
  43.5 19.1 %collective-permute-start.9 = (bf16[3072,128]{1,0:T(8,128)(2,1)}, bf16[3072,128]{1,0:T(8,128)(2,1)S(1)}, u32[]{:S(2)}, u32[]{:S(2)}) collective-permute-start(bf16[3072,128]{1,0:T(8,128)(2,1)} %get-tuple-element.38.refs_1_), channel_id=1, source_target_pairs={{0,1},{1,0},{2,3},{3,2},{4,5},{5,4},{6,7},{7,6},{8,9},{9,8},{10,11... | collective-permute-start | bytes 2359304 | tf_op jit(solution)/shard_map/ppermute | solution.py:531
  45.1 30.7 %collective-permute-start.6 = (bf16[3072,128]{1,0:T(8,128)(2,1)S(1)}, bf16[3072,128]{1,0:T(8,128)(2,1)}, u32[]{:S(2)}, u32[]{:S(2)}) collective-permute-start(bf16[3072,128]{1,0:T(8,128)(2,1)S(1)} %collective-permute-done.2.refs_2_), channel_id=1, source_target_pairs={{0,2},{2,4},{4,6},{6,0},{1,3},{3,5},{5,7},{7,1},{8,10},{10,12},{12... | collective-permute-start | bytes 2359304 | tf_op jit(solution)/shard_map/ppermute | solution.py:531
  62.1 18.9 %collective-permute-start.13 = (bf16[3072,128]{1,0:T(8,128)(2,1)}, bf16[3072,128]{1,0:T(8,128)(2,1)}, u32[]{:S(2)}, u32[]{:S(2)}) collective-permute-start(bf16[3072,128]{1,0:T(8,128)(2,1)} %collective-permute-done.5.refs_5_), channel_id=1, source_target_pairs={{0,1},{1,0},{2,3},{3,2},{4,5},{5,4},{6,7},{7,6},{8,9},{9,8},{10,11... | collective-permute-start | bytes 2359304 | tf_op jit(solution)/shard_map/ppermute | solution.py:531
  95.4 44.1 %all-to-all-start.1 = ((bf16[256,16,128]{2,1,0:T(8,128)(2,1)}), bf16[256,16,128]{2,1,0:T(8,128)(2,1)S(1)}, u32[]{:S(2)}, u32[]{:S(2)}) async-start(bf16[256,16,128]{2,1,0:T(8,128)(2,1)} %bitcast.44), calls=%async_computation.1 | async-start | bytes 2097152 | tf_op jit(solution)/shard_map/all_to_all | solution.py:564
  108.9 48.0 %collective-permute-start = (bf16[2,192,2048]{2,1,0:T(8,128)(2,1)}, bf16[2,192,2048]{2,1,0:T(8,128)(2,1)}, u32[]{:S(2)}, u32[]{:S(2)}) collective-permute-start(bf16[2,192,2048]{2,1,0:T(8,128)(2,1)} %select.3.rows_ref.refs_0_), channel_id=1, source_target_pairs={{0,6},{2,0},{4,2},{6,4},{1,7},{3,1},{5,3},{7,5},{8,14},{10,8},{12,... | collective-permute-start | bytes 4718600 | tf_op jit(solution)/shard_map/ppermute | solution.py:531
  111.1 54.4 %collective-permute-start.1 = (bf16[2,192,2048]{2,1,0:T(8,128)(2,1)}, bf16[2,192,2048]{2,1,0:T(8,128)(2,1)}, u32[]{:S(2)}, u32[]{:S(2)}) collective-permute-start(bf16[2,192,2048]{2,1,0:T(8,128)(2,1)} %select.3.rows_ref.refs_0_), channel_id=1, source_target_pairs={{0,2},{2,4},{4,6},{6,0},{1,3},{3,5},{5,7},{7,1},{8,10},{10,12},{12... | collective-permute-start | bytes 4718600 | tf_op jit(solution)/shard_map/ppermute | solution.py:531
  141.6 20.3 %collective-permute-start.16 = (bf16[256,384]{1,0:T(8,128)(2,1)S(1)}, bf16[256,384]{1,0:T(8,128)(2,1)S(1)}, u32[]{:S(2)}, u32[]{:S(2)}) collective-permute-start(bf16[256,384]{1,0:T(8,128)(2,1)S(1)} %combine.1.refs_0_), channel_id=1, source_target_pairs={{0,2},{2,4},{4,6},{6,0},{1,3},{3,5},{5,7},{7,1},{8,10},{10,12},{12... | collective-permute-start | bytes 589832 | tf_op jit(solution)/shard_map/ppermute | solution.py:531
  142.9 19.0 %collective-permute-start.17 = (bf16[256,384]{1,0:T(8,128)(2,1)S(1)}, bf16[256,384]{1,0:T(8,128)(2,1)S(1)}, u32[]{:S(2)}, u32[]{:S(2)}) collective-permute-start(bf16[256,384]{1,0:T(8,128)(2,1)S(1)} %combine.1.refs_0_), channel_id=1, source_target_pairs={{0,6},{2,0},{4,2},{6,4},{1,7},{3,1},{5,3},{7,5},{8,14},{10,8},{12,... | collective-permute-start | bytes 589832 | tf_op jit(solution)/shard_map/ppermute | solution.py:531
  143.7 21.8 %collective-permute-start.18 = (bf16[256,384]{1,0:T(8,128)(2,1)S(1)}, bf16[256,384]{1,0:T(8,128)(2,1)S(1)}, u32[]{:S(2)}, u32[]{:S(2)}) collective-permute-start(bf16[256,384]{1,0:T(8,128)(2,1)S(1)} %combine.1.refs_0_), channel_id=1, source_target_pairs={{0,4},{2,6},{4,0},{6,2},{1,5},{3,7},{5,1},{7,3},{8,12},{10,14},{12... | collective-permute-start | bytes 589832 | tf_op jit(solution)/shard_map/ppermute | solution.py:531
  171.2 35.0 %collective-permute-start.23 = (bf16[192,2048]{1,0:T(8,128)(2,1)S(1)}, bf16[192,2048]{1,0:T(8,128)(2,1)S(1)}, u32[]{:S(2)}, u32[]{:S(2)}) collective-permute-start(bf16[192,2048]{1,0:T(8,128)(2,1)S(1)} %slice_bitcast_fusion.1), channel_id=1, source_target_pairs={{0,2},{2,4},{4,6},{6,0},{1,3},{3,5},{5,7},{7,1},{8,10},{10,12},{12... | collective-permute-start | bytes 2359304 | tf_op jit(solution)/shard_map/ppermute | solution.py:531
  172.0 34.2 %collective-permute-start.24 = (bf16[192,2048]{1,0:T(8,128)(2,1)S(1)}, bf16[192,2048]{1,0:T(8,128)(2,1)S(1)}, u32[]{:S(2)}, u32[]{:S(2)}) collective-permute-start(bf16[192,2048]{1,0:T(8,128)(2,1)S(1)} %slice_bitcast_fusion), channel_id=1, source_target_pairs={{0,6},{2,0},{4,2},{6,4},{1,7},{3,1},{5,3},{7,5},{8,14},{10,8},{12,... | collective-permute-start | bytes 2359304 | tf_op jit(solution)/shard_map/ppermute | solution.py:531
  174.0 24.2 %collective-permute-start.25 = (bf16[3,192,256]{2,1,0:T(8,128)(2,1)S(1)}, bf16[3,192,256]{2,1,0:T(8,128)(2,1)S(1)}, u32[]{:S(2)}, u32[]{:S(2)}) collective-permute-start(bf16[3,192,256]{2,1,0:T(8,128)(2,1)S(1)} %get-tuple-element.67), channel_id=1, source_target_pairs={{0,6},{2,0},{4,2},{6,4},{1,7},{3,1},{5,3},{7,5},{8,14},{10,8},{12,... | collective-permute-start | bytes 884744 | tf_op jit(solution)/shard_map/ppermute | solution.py:531
  177.3 21.3 %collective-permute-start.26 = (bf16[3,192,256]{2,1,0:T(8,128)(2,1)S(1)}, bf16[3,192,256]{2,1,0:T(8,128)(2,1)S(1)}, u32[]{:S(2)}, u32[]{:S(2)}) collective-permute-start(bf16[3,192,256]{2,1,0:T(8,128)(2,1)S(1)} %get-tuple-element.66), channel_id=1, source_target_pairs={{0,2},{2,4},{4,6},{6,0},{1,3},{3,5},{5,7},{7,1},{8,10},{10,12},{12... | collective-permute-start | bytes 884744 | tf_op jit(solution)/shard_map/ppermute | solution.py:531
  177.3 28.9 %collective-permute-start.27 = (bf16[3,192,256]{2,1,0:T(8,128)(2,1)S(1)}, bf16[3,192,256]{2,1,0:T(8,128)(2,1)S(1)}, u32[]{:S(2)}, u32[]{:S(2)}) collective-permute-start(bf16[3,192,256]{2,1,0:T(8,128)(2,1)S(1)} %get-tuple-element.65), channel_id=1, source_target_pairs={{0,4},{2,6},{4,0},{6,2},{1,5},{3,7},{5,1},{7,3},{8,12},{10,14},{12... | collective-permute-start | bytes 884744 | tf_op jit(solution)/shard_map/ppermute | solution.py:531
  218.5 45.7 %collective-permute-start.28 = (f32[6144,128]{1,0:T(8,128)}, f32[6144,128]{1,0:T(8,128)}, u32[]{:S(2)}, u32[]{:S(2)}) collective-permute-start(f32[6144,128]{1,0:T(8,128)} %get-tuple-element.49), channel_id=1, source_target_pairs={{0,1},{1,0},{2,3},{3,2},{4,5},{5,4},{6,7},{7,6},{8,9},{9,8},{10,11... | collective-permute-start | bytes 9437192 | tf_op jit(solution)/shard_map/ppermute | solution.py:531
  220.1 21.6 %collective-permute-start.30 = (bf16[8,64,352]{2,1,0:T(8,128)(2,1)S(1)}, bf16[8,64,352]{2,1,0:T(8,128)(2,1)S(1)}, u32[]{:S(2)}, u32[]{:S(2)}) collective-permute-start(bf16[8,64,352]{2,1,0:T(8,128)(2,1)S(1)} %copy-done.31), channel_id=1, source_target_pairs={{0,16},{8,24},{16,0},{24,8},{1,17},{9,25},{17,1},{25,9},{2,18},{10... | collective-permute-start | bytes 1081352 | tf_op jit(solution)/shard_map/ppermute | solution.py:531
  222.7 19.0 %collective-permute-start.31 = (bf16[8,64,352]{2,1,0:T(8,128)(2,1)S(1)}, bf16[8,64,352]{2,1,0:T(8,128)(2,1)S(1)}, u32[]{:S(2)}, u32[]{:S(2)}) collective-permute-start(bf16[8,64,352]{2,1,0:T(8,128)(2,1)S(1)} %copy-done.30), channel_id=1, source_target_pairs={{0,24},{8,0},{16,8},{24,16},{1,25},{9,1},{17,9},{25,17},{2,26},{10... | collective-permute-start | bytes 1081352 | tf_op jit(solution)/shard_map/ppermute | solution.py:531
  242.7 20.9 %all-to-all-start.2 = ((bf16[8,64,352]{2,1,0:T(8,128)(2,1)}), bf16[8,64,352]{2,1,0:T(8,128)(2,1)S(1)}, u32[]{:S(2)}, u32[]{:S(2)}) async-start(bf16[8,64,352]{2,1,0:T(8,128)(2,1)} %add_convert_fusion), calls=%async_computation.2 | async-start | bytes 786432 | tf_op jit(solution)/shard_map/all_to_all | solution.py:582
  (44 other events, 662.4 us)
where the time goes:
time: 271 us; the launch traced here: 269 us
  waiting for transfers between devices  122 us (45%)
  starting transfers between devices  68 us (25%)
  Pallas kernels  62.8 us (23%)
  local copies, waits for them, and re-layouts  13.2 us (5%)
    ppermute x32, waiting for transfers between devices, shifted(): return lax.ppermute(value, axis, [(i, (i + by) % n) for i in range(n)])  101 us
    ppermute x32, starting transfers between devices, shifted(): return lax.ppermute(value, axis, [(i, (i + by) % n) for i in range(n)])  29.8 us
    all_to_all x1, waiting for transfers between devices, on_device(): lax.all_to_all(back.reshape(N_EXP * N_TP, 16, 128), ALL, split_axis=0, co...  14.9 us
    pallas_call x1, Pallas kernels, experts(): pl.pallas_call(expert_kernel, in_specs=[pl.BlockSpec(memory_space=pltpu.V...  14.1 us
    all_to_all x1, starting transfers between devices, on_device(): lax.all_to_all(back.reshape(N_EXP * N_TP, 16, 128), ALL, split_axis=0, co...  13.5 us
    all_to_all x1, starting transfers between devices, on_device(): got = lax.all_to_all(sent, SP, split_axis=0, concat_axis=0, tiled=True)  11.3 us
    pallas_call x1, Pallas kernels, weight_grads(): pl.pallas_call(weight_grad_kernel, in_specs=[pl.BlockSpec(memory_space=pl...  10.4 us
    unnamed x65, local copies, waits for them, and re-layouts  10.1 us
  transfers between devices with their start and end apart: 36, of which 16 were waited for; matrix products, arithmetic and copies ran while one was open for 2% of the time, Pallas kernels for 9%

commit v1 on v0

--- a/solution.py
+++ b/solution.py
@@ -1,5 +1,3 @@
-import functools
-
 import jax
 import jax.numpy as jnp
 from jax import lax
@@ -155,7 +153,7 @@
         out_shape=pltpu.HBM((N_EXP, 24, D // 2), BF16),
         compiler_params=vmem(14),
         name="dispatch",
-    )(tp, routes_t, weight_t, resid, resid, cotangent, cotangent)
+    )(tp, routes_t, weight_t, *in_hbm(resid, resid, cotangent, cotangent))
 
 
 def place_kernel(routes_ref, out_ref):
@@ -213,8 +211,8 @@
 
 
 def expert_kernel(rows_ref, *refs):
-    weights, out_ref, acts_ref = refs[:16], refs[16], refs[17]
-    gate_up, down, grads, sems = refs[18:]
+    weights, out_ref, acts = refs[:16], refs[16], refs[17:21]
+    gate_up, down, grads, sems = refs[21:]
     mid = D // 2
     copies = [[], [], [], []]
     for j in range(4):
@@ -249,9 +247,13 @@
         silu = gate * sig
         d_gate = (d_hidden * up * (sig * (1.0 + gate * (1.0 - sig)))).astype(BF16)
         d_up = (d_hidden * silu).astype(BF16)
-        acts_ref[j, 0] = d_gate
-        acts_ref[j, 1] = d_up
-        acts_ref[j, 2] = (silu * up).astype(BF16)
+        made = (d_gate, d_up, (silu * up).astype(BF16))
+        for n in range(4):
+            @pl.when(j == n)
+            def _():
+                for k in range(3):
+                    acts[n][k] = made[k]
+
         grads[:, pl.ds(at, 256)] = d_gate
         grads[:, pl.ds(pl.multiple_of(at + 256, 256), 256)] = d_up
         return 0
@@ -272,10 +274,11 @@
 
 
 def experts(rows, weights):
+    act = pltpu.HBM((3, ROWS, 256), BF16)
     return pl.pallas_call(
         expert_kernel,
         in_specs=[pl.BlockSpec(memory_space=pltpu.VMEM)] + [pl.BlockSpec(memory_space=pl.ANY)] * 16,
-        out_shape=(pltpu.HBM((N_EXP, N_TP, 16, 128), BF16), pltpu.HBM((4, 3, ROWS, 256), BF16)),
+        out_shape=(pltpu.HBM((N_EXP, N_TP, 16, 128), BF16), act, act, act, act),
         scratch_shapes=[
             pltpu.VMEM((D, D), BF16),
             pltpu.VMEM((D, D // 2), BF16),
@@ -288,17 +291,13 @@
 
 
 def weight_grad_kernel(*refs):
-    rows, far, acts = refs[0:3], refs[3:5], refs[5:9]
-    keep_ref, send_ref, xbuf, hbuf, sems = refs[9:]
+    rows, acts = refs[0:3], refs[3:6]
+    keep_ref, send_ref, xbuf, hbuf, sems = refs[6:]
     copies = []
-    for n in range(4):
+    for n in range(3):
         at = pl.ds(ROWS * n, ROWS)
-        if n < 3:
-            copies.append(pltpu.make_async_copy(rows[n], xbuf.at[:, at, :], sems.at[0, n]))
-        act = acts[n].at[0] if n == 0 else acts[n]
-        copies.append(pltpu.make_async_copy(act, hbuf.at[:, at, :], sems.at[1, n]))
-    for n in range(2):
-        copies.append(pltpu.make_async_copy(far[n], xbuf.at[n, pl.ds(3 * ROWS, ROWS), :], sems.at[0, 3 + n]))
+        copies.append(pltpu.make_async_copy(rows[n], xbuf.at[:, at, :], sems.at[0, n]))
+        copies.append(pltpu.make_async_copy(acts[n], hbuf.at[:, at, :], sems.at[1, n]))
     for copy in copies:
         copy.start()
     for copy in copies:
@@ -308,52 +307,79 @@
         cols = pl.ds(pl.multiple_of(256 * t, 256), 256)
         for n in range(2):
             both = dot_tn(xbuf[0, :, cols], hbuf[n])
-            rows = pl.ds(pl.multiple_of(D * n + 256 * t, 256), 256)
-            keep_ref[rows, :] = both[:, :128]
-            send_ref[rows, :] = both[:, 128:]
+            keep_ref[n, cols, :] = both[:, :128]
+            send_ref[n, cols, :] = both[:, 128:]
         both = dot_tn(hbuf[2], xbuf[1, :, cols])
         for h in range(2):
-            rows = pl.ds(pl.multiple_of(2 * D + 256 * t + 128 * h, 128), 128)
-            keep_ref[rows, :] = both[:128, 128 * h : 128 * h + 128]
-            send_ref[rows, :] = both[128:, 128 * h : 128 * h + 128]
+            at = pl.ds(pl.multiple_of(256 * t + 128 * h, 128), 128)
+            keep_ref[2, at, :] = both[:128, 128 * h : 128 * h + 128]
+            send_ref[2, at, :] = both[128:, 128 * h : 128 * h + 128]
         return 0
 
     lax.fori_loop(0, N_TP, columns, 0)
 
 
-def weight_grads(rows, far, acts):
-    part = pltpu.HBM((3 * D, 128), F32)
+def weight_grads(rows, acts):
+    part = pltpu.HBM((3, D, 128), F32)
     return pl.pallas_call(
         weight_grad_kernel,
-        in_specs=[pl.BlockSpec(memory_space=pl.ANY)] * 9,
+        in_specs=[pl.BlockSpec(memory_space=pl.ANY)] * 6,
         out_shape=(part, part),
         scratch_shapes=[
-            pltpu.VMEM((2, 4 * ROWS, D), BF16),
-            pltpu.VMEM((3, 4 * ROWS, 256), BF16),
-            pltpu.SemaphoreType.DMA((2, 5)),
+            pltpu.VMEM((2, 3 * ROWS, D), BF16),
+            pltpu.VMEM((3, 3 * ROWS, 256), BF16),
+            pltpu.SemaphoreType.DMA((2, 3)),
         ],
-        compiler_params=vmem(26),
+        compiler_params=vmem(22),
         name="weight_grads",
-    )(*in_hbm(*rows, *far, *acts))
-
-
-def finish_kernel(keep_g, keep_u, keep_d, got_g, got_u, got_d, gate_ref, up_ref, down_ref):
-    gate_ref[...] = keep_g[...] + got_g[...]
-    up_ref[...] = keep_u[...] + got_u[...]
-    for n in range(4):
-        rows = slice(128 * n, 128 * n + 128)
-        down_ref[:, rows] = keep_d[rows, :] + got_d[rows, :]
+    )(*in_hbm(*rows, *acts))
+
+
+def far_grad_kernel(in_ref, cot_ref, act_ref, keep_in, send_in, keep_ref, send_ref):
+    for n in range(2):
+        both = dot_tn(in_ref[...], act_ref[n])
+        keep_ref[n] = keep_in[n] + both[:, :128]
+        send_ref[n] = send_in[n] + both[:, 128:]
+    both = dot_tn(act_ref[2], cot_ref[...])
+    for h in range(both.shape[1] // 128):
+        at = slice(128 * h, 128 * h + 128)
+        keep_ref[2, at, :] = keep_in[2, at, :] + both[:128, at]
+        send_ref[2, at, :] = send_in[2, at, :] + both[128:, at]
+
+
+def far_grads(far_in, far_cot, act, keep, send):
+    block = 512
+    part = pltpu.HBM((3, D, 128), F32)
+    cols = pl.BlockSpec((ROWS, block), lambda t: (0, t))
+    sums = pl.BlockSpec((3, block, 128), lambda t: (0, t, 0))
+    return pl.pallas_call(
+        far_grad_kernel,
+        grid=(D // block,),
+        in_specs=[cols, cols, pl.BlockSpec(act.shape, lambda t: (0, 0, 0)), sums, sums],
+        out_specs=(sums, sums),
+        out_shape=(part, part),
+        compiler_params=vmem(12),
+        name="far_grads",
+    )(far_in, far_cot, act, *in_hbm(keep, send))
+
+
+def finish_kernel(keep_ref, got_ref, gate_ref, up_ref, down_ref):
+    gate_ref[...] = keep_ref[0] + got_ref[0]
+    up_ref[...] = keep_ref[1] + got_ref[1]
+    for n in range(keep_ref.shape[1] // 128):
+        at = slice(128 * n, 128 * n + 128)
+        down_ref[:, at] = keep_ref[2, at, :] + got_ref[2, at, :]
 
 
 def finish(keep, got):
     block = 512
-    count = D // block
-    tall = [pl.BlockSpec((block, 128), functools.partial(lambda k, n: (n + k * count, 0), k)) for k in range(3)]
+    sums = pl.BlockSpec((3, block, 128), lambda t: (0, t, 0))
+    tall = pl.BlockSpec((block, 128), lambda t: (t, 0))
     return pl.pallas_call(
         finish_kernel,
-        grid=(count,),
-        in_specs=tall + tall,
-        out_specs=(tall[0], tall[0], pl.BlockSpec((128, block), lambda n: (0, n))),
+        grid=(D // block,),
+        in_specs=[sums, sums],
+        out_specs=(tall, tall, pl.BlockSpec((128, block), lambda t: (0, t))),
         out_shape=(
             jax.ShapeDtypeStruct((D, 128), F32),
             jax.ShapeDtypeStruct((D, 128), F32),
@@ -361,7 +387,7 @@
         ),
         compiler_params=vmem(8),
         name="finish",
-    )(*[in_hbm(keep)] * 3, *[in_hbm(got)] * 3)
+    )(*in_hbm(keep, got))
 
 
 def combine_kernel(tp_ref, place_ref, back_ref, cot_ref, out_ref):
@@ -560,11 +586,12 @@
     rows = select(got)
     rows_after = shifted(rows, "y", -1)
     rows_before = shifted(rows, "y", 1)
-    back, acts = experts(rows, weights)
+    back, *acts = experts(rows, weights)
     back = lax.all_to_all(back.reshape(N_EXP * N_TP, 16, 128), ALL, split_axis=0, concat_axis=0, tiled=True)
-    all_acts = [acts]
+    all_acts = [acts[0]]
     for j, by in ((1, -1), (2, 1), (3, 2)):
         all_acts.append(shifted(acts[j], "y", by))
+    keep, send = weight_grads((rows, rows_after, rows_before), all_acts[:3])
     part = combine(tp_vec, placed, back, cotangent)
 
     near = (part, shifted(part, "y", 1), shifted(part, "y", -1), shifted(part, "y", 2))
@@ -588,8 +615,7 @@
 
     far_in = shifted(far_in, "y", 1)
     far_cot = shifted(far_cot, "y", -1)
-    far = (far_in, far_cot)
-    keep, send = weight_grads((rows, rows_after, rows_before), far, all_acts)
+    keep, send = far_grads(far_in, far_cot, all_acts[3], keep, send)
     send = shifted(send, "c", 1)
     grad_gate, grad_up, grad_down = finish(keep, send)
     return (

time: 271 us -> 274 us (1.011)
  the two profiles are of different devices: /device:TPU:8 before, /device:TPU:24 now
where the time goes in v1:
time: 274 us; the launch traced here: 273 us
  waiting for transfers between devices  128 us (47%)
  Pallas kernels  70.3 us (26%)
  starting transfers between devices  63.2 us (23%)
  local copies, waits for them, and re-layouts  9.3 us (3%)
    ppermute x32, waiting for transfers between devices, shifted(): return lax.ppermute(value, axis, [(i, (i + by) % n) for i in range(n)])  107 us
    ppermute x32, starting transfers between devices, shifted(): return lax.ppermute(value, axis, [(i, (i + by) % n) for i in range(n)])  26.4 us
    all_to_all x1, waiting for transfers between devices, on_device(): lax.all_to_all(back.reshape(N_EXP * N_TP, 16, 128), ALL, split_axis=0, co...  14.6 us
    pallas_call x1, Pallas kernels, experts(): pl.pallas_call(expert_kernel, in_specs=[pl.BlockSpec(memory_space=pltpu.V...  14.3 us
    all_to_all x1, starting transfers between devices, on_device(): lax.all_to_all(back.reshape(N_EXP * N_TP, 16, 128), ALL, split_axis=0, co...  12.2 us
    all_to_all x1, starting transfers between devices, on_device(): got = lax.all_to_all(sent, SP, split_axis=0, concat_axis=0, tiled=True)  11.3 us
    pallas_call x1, Pallas kernels, weight_grads(): pl.pallas_call(weight_grad_kernel, in_specs=[pl.BlockSpec(memory_space=pl...  9.61 us
    pallas_call x1, Pallas kernels, prepare(): pl.pallas_call(prepare_kernel, out_shape=(pltpu.HBM(shape[::-1], BF16), w...  8.12 us
  transfers between devices with their start and end apart: 36, of which 13 were waited for; matrix products, arithmetic and copies ran while one was open for 2% of the time, Pallas kernels for 13%

profile of v1, /device:TPU:24, one launch (start us, length us, event | category | flops | bytes accessed | tf_op | source)
XLA Modules:
  0.0 273.4 jit_solution(14455747675364409881)
XLA Ops:
  2.0 5.7 %dispatch.1 = bf16[32,24,1024]{2,1,0:T(8,128)(2,1)} custom-call(s32[1]{0:T(128)} %bitcast.tp_ref, s32[2,384]{1,0:T(2,128)S(1)} %bitcast.36, f32[2,384]{1,0:T(2,128)S(1)} %bitcast.37, bf16[384,2048]{1,0:T(8,128)(2,1)} %res_b.1, bf16[384,2048]{1,0:T(8,128)(2,1)} %res_b.1, bf16[384,2048]{1,0:T(8,128)(2,1)} %cot_ref.1, bf16[384,2048]{1,0:T(8,128)(2,1)} %cot_ref.1), custom_call_target="tpu_custom_call" | custom-call | tf_op jit(solution)/shard_map/dispatch/pallas_call | solution.py:134
  7.7 11.3 %all-to-all-start = ((bf16[32,24,1024]{2,1,0:T(8,128)(2,1)}), bf16[32,24,1024]{2,1,0:T(8,128)(2,1)S(1)}, u32[]{:S(2)}, u32[]{:S(2)}) async-start(bf16[32,24,1024]{2,1,0:T(8,128)(2,1)} %dispatch.1), calls=%async_computation | async-start | bytes 3145728 | tf_op jit(solution)/shard_map/all_to_all | solution.py:577
  25.6 16.6 %collective-permute-done.2.refs_2_ = bf16[3072,128]{1,0:T(8,128)(2,1)S(1)} collective-permute-done((bf16[3072,128]{1,0:T(8,128)(2,1)}, bf16[3072,128]{1,0:T(8,128)(2,1)S(1)}, u32[]{:S(2)}, u32[]{:S(2)}) %collective-permute-start.2) | collective-permute-done | bytes 786464 | tf_op jit(solution)/shard_map/ppermute | solution.py:557
  44.1 15.1 %collective-permute-done.3.refs_3_ = bf16[3072,128]{1,0:T(8,128)(2,1)} collective-permute-done((bf16[3072,128]{1,0:T(8,128)(2,1)}, bf16[3072,128]{1,0:T(8,128)(2,1)}, u32[]{:S(2)}, u32[]{:S(2)}) %collective-permute-start.3) | collective-permute-done | bytes 786464 | tf_op jit(solution)/shard_map/ppermute | solution.py:557
  60.5 14.1 %collective-permute-done.6.refs_6_ = bf16[3072,128]{1,0:T(8,128)(2,1)} collective-permute-done((bf16[3072,128]{1,0:T(8,128)(2,1)S(1)}, bf16[3072,128]{1,0:T(8,128)(2,1)}, u32[]{:S(2)}, u32[]{:S(2)}) %collective-permute-start.6) | collective-permute-done | bytes 786464 | tf_op jit(solution)/shard_map/ppermute | solution.py:557
  74.6 2.8 %collective-permute-done.7.refs_7_ = bf16[3072,128]{1,0:T(8,128)(2,1)} collective-permute-done((bf16[3072,128]{1,0:T(8,128)(2,1)}, bf16[3072,128]{1,0:T(8,128)(2,1)}, u32[]{:S(2)}, u32[]{:S(2)}) %collective-permute-start.7) | collective-permute-done | bytes 786464 | tf_op jit(solution)/shard_map/ppermute | solution.py:557
  81.2 14.3 %experts.1 = (bf16[32,8,16,128]{3,2,1,0:T(8,128)(2,1)}, bf16[3,192,256]{2,1,0:T(8,128)(2,1)}, bf16[3,192,256]{2,1,0:T(8,128)(2,1)}, bf16[3,192,256]{2,1,0:T(8,128)(2,1)}, bf16[3,192,256]{2,1,0:T(8,128)(2,1)}) custom-call(bf16[2,192,2048]{2,1,0:T(8,128)(2,1)} %select.3.rows_ref.refs_0_, bf16[3072,128]{1,0:T(8,128)(2,1)} %get-tuple-element.42.refs_0_, ...), custom_call_target="tpu_custom_call" | custom-call | tf_op jit(solution)/shard_map/experts/pallas_call | solution.py:278
  95.4 12.2 %all-to-all-start.1 = ((bf16[256,16,128]{2,1,0:T(8,128)(2,1)}), bf16[256,16,128]{2,1,0:T(8,128)(2,1)S(1)}, u32[]{:S(2)}, u32[]{:S(2)}) async-start(bf16[256,16,128]{2,1,0:T(8,128)(2,1)} %bitcast.38), calls=%async_computation.1 | async-start | bytes 2097152 | tf_op jit(solution)/shard_map/all_to_all | solution.py:590
  116.2 8.1 %prepare.1 = (bf16[384,352]{1,0:T(8,128)(2,1)}, f32[352,384]{1,0:T(8,128)}, f32[352,384]{1,0:T(8,128)}, f32[352,384]{1,0:T(8,128)}, f32[352,384]{1,0:T(8,128)}) custom-call(bf16[352,384]{1,0:T(8,128)(2,1)S(1)} %bitcast.34, f32[352,384]{1,0:T(8,128)S(1)} %bitcast.28, f32[352,384]{1,0:T(8,128)S(1)} %bitcast.31, bf16[352,384]{1,0:T(8,128)(2,1)S(1)} %bitcast.35), custom_call_target="tpu_custom_call" | custom-call | tf_op jit(solution)/shard_map/prepare/pallas_call | solution.py:452
  124.3 14.6 %all-to-all-done.1.back_ref = bf16[256,16,128]{2,1,0:T(8,128)(2,1)S(1)} async-done(((bf16[256,16,128]{2,1,0:T(8,128)(2,1)}), bf16[256,16,128]{2,1,0:T(8,128)(2,1)S(1)}, u32[]{:S(2)}, u32[]{:S(2)}) %all-to-all-start.1) | async-done | bytes 1048608 | tf_op jit(solution)/shard_map/all_to_all | solution.py:590
  143.8 12.0 %collective-permute-done.1.refs_1_ = bf16[2,192,2048]{2,1,0:T(8,128)(2,1)} collective-permute-done((bf16[2,192,2048]{2,1,0:T(8,128)(2,1)}, bf16[2,192,2048]{2,1,0:T(8,128)(2,1)}, u32[]{:S(2)}, u32[]{:S(2)}) %collective-permute-start.1) | collective-permute-done | bytes 1572896 | tf_op jit(solution)/shard_map/ppermute | solution.py:557
  159.7 3.9 %collective-permute-done.17.refs_2_ = bf16[256,384]{1,0:T(8,128)(2,1)S(1)} collective-permute-done((bf16[256,384]{1,0:T(8,128)(2,1)S(1)}, bf16[256,384]{1,0:T(8,128)(2,1)S(1)}, u32[]{:S(2)}, u32[]{:S(2)}) %collective-permute-start.17) | collective-permute-done | bytes 196640 | tf_op jit(solution)/shard_map/ppermute | solution.py:557
  165.4 4.2 %project.1 = (bf16[8,64,352]{2,1,0:T(8,128)(2,1)}, bf16[8,64,352]{2,1,0:T(8,128)(2,1)}, bf16[8,64,352]{2,1,0:T(8,128)(2,1)}, bf16[8,64,352]{2,1,0:T(8,128)(2,1)}...) custom-call(s32[9]{0:T(128)S(1)} %pad_add_fusion.order_ref, ...), custom_call_target="tpu_custom_call" | custom-call | tf_op jit(solution)/shard_map/project/pallas_call | solution.py:485
  169.6 3.0 %collective-permute-start.23 = (bf16[192,2048]{1,0:T(8,128)(2,1)S(1)}, bf16[192,2048]{1,0:T(8,128)(2,1)S(1)}, u32[]{:S(2)}, u32[]{:S(2)}) collective-permute-start(bf16[192,2048]{1,0:T(8,128)(2,1)S(1)} %slice_bitcast_fusion.1), channel_id=1, source_target_pairs={{0,2},{2,4},{4,6},{6,0},{1,3},{3,5},{5,7},{7,1},{8,10},{10,12},{12... | collective-permute-start | bytes 2359304 | tf_op jit(solution)/shard_map/ppermute | solution.py:557
  172.6 3.3 %collective-permute-start.27 = (bf16[3,192,256]{2,1,0:T(8,128)(2,1)S(1)}, bf16[3,192,256]{2,1,0:T(8,128)(2,1)S(1)}, u32[]{:S(2)}, u32[]{:S(2)}) collective-permute-start(bf16[3,192,256]{2,1,0:T(8,128)(2,1)S(1)} %copy-done.27), channel_id=1, source_target_pairs={{0,2},{2,4},{4,6},{6,0},{1,3},{3,5},{5,7},{7,1},{8,10},{10,12},{12... | collective-permute-start | bytes 884744 | tf_op jit(solution)/shard_map/ppermute | solution.py:557
  177.4 28.4 %collective-permute-done.26.refs_4_ = bf16[3,192,256]{2,1,0:T(8,128)(2,1)S(1)} collective-permute-done((bf16[3,192,256]{2,1,0:T(8,128)(2,1)S(1)}, bf16[3,192,256]{2,1,0:T(8,128)(2,1)S(1)}, u32[]{:S(2)}, u32[]{:S(2)}) %collective-permute-start.26) | collective-permute-done | bytes 294944 | tf_op jit(solution)/shard_map/ppermute | solution.py:557
  206.6 9.6 %weight_grads.1 = (f32[3,2048,128]{2,1,0:T(8,128)}, f32[3,2048,128]{2,1,0:T(8,128)}) custom-call(bf16[2,192,2048]{2,1,0:T(8,128)(2,1)} %select.3.rows_ref.refs_0_, bf16[2,192,2048]{2,1,0:T(8,128)(2,1)} %collective-permute-done.1.refs_1_, bf16[2,192,2048]{2,1,0:T(8,128)(2,1)} %collective-permute-done.refs_2_, bf16[3,192,256]{2,1,0:T(8,128)(2,1)} %get-tuple-element.53.refs_3_, ...), custom_call_target="tpu_custom_call" | custom-call | tf_op jit(solution)/shard_map/weight_grads/pallas_call | solution.py:324
  216.3 6.6 %far_grads.1 = (f32[3,2048,128]{2,1,0:T(8,128)}, f32[3,2048,128]{2,1,0:T(8,128)}) custom-call(bf16[192,2048]{1,0:T(8,128)(2,1)S(1)} %collective-permute-done.23.in_ref, bf16[192,2048]{1,0:T(8,128)(2,1)S(1)} %collective-permute-done.24.cot_ref, bf16[3,192,256]{2,1,0:T(8,128)(2,1)S(1)} %collective-permute-done.25.act_ref, ...), custom_call_target="tpu_custom_call" | custom-call | tf_op jit(solution)/shard_map/far_grads/pallas_call | solution.py:355
  229.1 6.7 %all-to-all-start.3 = ((f32[32,2,352]{2,1,0:T(2,128)}), f32[32,2,352]{2,1,0:T(2,128)S(1)}, u32[]{:S(2)}, u32[]{:S(2)}) async-start(f32[32,2,352]{2,1,0:T(2,128)} %broadcast_in_dim.27), calls=%async_computation.3 | async-start | bytes 196608 | tf_op jit(solution)/shard_map/all_to_all | solution.py:607
  235.8 10.1 %collective-permute-done.30 = bf16[8,64,352]{2,1,0:T(8,128)(2,1)S(1)} collective-permute-done((bf16[8,64,352]{2,1,0:T(8,128)(2,1)S(1)}, bf16[8,64,352]{2,1,0:T(8,128)(2,1)S(1)}, u32[]{:S(2)}, u32[]{:S(2)}) %collective-permute-start.30) | collective-permute-done | bytes 360480 | tf_op jit(solution)/shard_map/ppermute | solution.py:557
  246.9 6.5 %all-to-all-start.2 = ((bf16[8,64,352]{2,1,0:T(8,128)(2,1)}), bf16[8,64,352]{2,1,0:T(8,128)(2,1)S(1)}, u32[]{:S(2)}, u32[]{:S(2)}) async-start(bf16[8,64,352]{2,1,0:T(8,128)(2,1)} %add_convert_fusion), calls=%async_computation.2 | async-start | bytes 786432 | tf_op jit(solution)/shard_map/all_to_all | solution.py:609
  253.5 7.0 %local_scan.1.local_ref = f32[352,384]{1,0:T(8,128)S(1)} custom-call(f32[352,384]{1,0:T(8,128)S(1)} %copy-done.8, f32[352,384]{1,0:T(8,128)S(1)} %bitcast.29), custom_call_target="tpu_custom_call" | custom-call | tf_op jit(solution)/shard_map/local_scan/pallas_call | solution.py:520
  261.8 6.0 %all-to-all-done.2 = bf16[8,64,352]{2,1,0:T(8,128)(2,1)S(1)} async-done(((bf16[8,64,352]{2,1,0:T(8,128)(2,1)}), bf16[8,64,352]{2,1,0:T(8,128)(2,1)S(1)}, u32[]{:S(2)}, u32[]{:S(2)}) %all-to-all-start.2) | async-done | bytes 360480 | tf_op jit(solution)/shard_map/all_to_all | solution.py:609
  268.5 4.9 %finish.1 = (f32[2048,128]{1,0:T(8,128)}, f32[2048,128]{1,0:T(8,128)}, f32[128,2048]{1,0:T(8,128)}) custom-call(f32[3,2048,128]{2,1,0:T(8,128)} %get-tuple-element.58.keep_ref, f32[3,2048,128]{2,1,0:T(8,128)} %collective-permute-done.28.got_ref), custom_call_target="tpu_custom_call" | custom-call | tf_op jit(solution)/shard_map/finish/pallas_call | solution.py:378
  (128 shorter events, 45.5 us)
Async XLA Ops:
  7.7 71.3 %all-to-all-start = ((bf16[32,24,1024]{2,1,0:T(8,128)(2,1)}), bf16[32,24,1024]{2,1,0:T(8,128)(2,1)S(1)}, u32[]{:S(2)}, u32[]{:S(2)}) async-start(bf16[32,24,1024]{2,1,0:T(8,128)(2,1)} %dispatch.1), calls=%async_computation | async-start | bytes 3145728 | tf_op jit(solution)/shard_map/all_to_all | solution.py:577
  21.5 20.7 %collective-permute-start.2 = (bf16[3072,128]{1,0:T(8,128)(2,1)}, bf16[3072,128]{1,0:T(8,128)(2,1)S(1)}, u32[]{:S(2)}, u32[]{:S(2)}) collective-permute-start(bf16[3072,128]{1,0:T(8,128)(2,1)} %get-tuple-element.42.refs_0_), channel_id=1, source_target_pairs={{0,2},{2,4},{4,6},{6,0},{1,3},{3,5},{5,7},{7,1},{8,10},{10,12},{12... | collective-permute-start | bytes 2359304 | tf_op jit(solution)/shard_map/ppermute | solution.py:557
  21.8 21.9 %collective-permute-start.5 = (bf16[3072,128]{1,0:T(8,128)(2,1)}, bf16[3072,128]{1,0:T(8,128)(2,1)}, u32[]{:S(2)}, u32[]{:S(2)}) collective-permute-start(bf16[3072,128]{1,0:T(8,128)(2,1)} %get-tuple-element.43.refs_1_), channel_id=1, source_target_pairs={{0,6},{2,0},{4,2},{6,4},{1,7},{3,1},{5,3},{7,5},{8,14},{10,8},{12,... | collective-permute-start | bytes 2359304 | tf_op jit(solution)/shard_map/ppermute | solution.py:557
  23.6 35.6 %collective-permute-start.3 = (bf16[3072,128]{1,0:T(8,128)(2,1)}, bf16[3072,128]{1,0:T(8,128)(2,1)}, u32[]{:S(2)}, u32[]{:S(2)}) collective-permute-start(bf16[3072,128]{1,0:T(8,128)(2,1)} %get-tuple-element.43.refs_1_), channel_id=1, source_target_pairs={{0,2},{2,4},{4,6},{6,0},{1,3},{3,5},{5,7},{7,1},{8,10},{10,12},{12... | collective-permute-start | bytes 2359304 | tf_op jit(solution)/shard_map/ppermute | solution.py:557
  25.0 34.9 %collective-permute-start.4 = (bf16[3072,128]{1,0:T(8,128)(2,1)}, bf16[3072,128]{1,0:T(8,128)(2,1)}, u32[]{:S(2)}, u32[]{:S(2)}) collective-permute-start(bf16[3072,128]{1,0:T(8,128)(2,1)} %get-tuple-element.42.refs_0_), channel_id=1, source_target_pairs={{0,6},{2,0},{4,2},{6,4},{1,7},{3,1},{5,3},{7,5},{8,14},{10,8},{12,... | collective-permute-start | bytes 2359304 | tf_op jit(solution)/shard_map/ppermute | solution.py:557
  25.6 34.3 %collective-permute-start.8 = (bf16[3072,128]{1,0:T(8,128)(2,1)}, bf16[3072,128]{1,0:T(8,128)(2,1)S(1)}, u32[]{:S(2)}, u32[]{:S(2)}) collective-permute-start(bf16[3072,128]{1,0:T(8,128)(2,1)} %get-tuple-element.42.refs_0_), channel_id=1, source_target_pairs={{0,1},{1,0},{2,3},{3,2},{4,5},{5,4},{6,7},{7,6},{8,9},{9,8},{10,11... | collective-permute-start | bytes 2359304 | tf_op jit(solution)/shard_map/ppermute | solution.py:557
  43.7 30.9 %collective-permute-start.6 = (bf16[3072,128]{1,0:T(8,128)(2,1)S(1)}, bf16[3072,128]{1,0:T(8,128)(2,1)}, u32[]{:S(2)}, u32[]{:S(2)}) collective-permute-start(bf16[3072,128]{1,0:T(8,128)(2,1)S(1)} %collective-permute-done.2.refs_2_), channel_id=1, source_target_pairs={{0,2},{2,4},{4,6},{6,0},{1,3},{3,5},{5,7},{7,1},{8,10},{10,12},{12... | collective-permute-start | bytes 2359304 | tf_op jit(solution)/shard_map/ppermute | solution.py:557
  59.9 21.1 %collective-permute-start.13 = (bf16[3072,128]{1,0:T(8,128)(2,1)}, bf16[3072,128]{1,0:T(8,128)(2,1)}, u32[]{:S(2)}, u32[]{:S(2)}) collective-permute-start(bf16[3072,128]{1,0:T(8,128)(2,1)} %collective-permute-done.5.refs_5_), channel_id=1, source_target_pairs={{0,1},{1,0},{2,3},{3,2},{4,5},{5,4},{6,7},{7,6},{8,9},{9,8},{10,11... | collective-permute-start | bytes 2359304 | tf_op jit(solution)/shard_map/ppermute | solution.py:557
  60.4 20.6 %collective-permute-start.11 = (bf16[3072,128]{1,0:T(8,128)(2,1)}, bf16[3072,128]{1,0:T(8,128)(2,1)}, u32[]{:S(2)}, u32[]{:S(2)}) collective-permute-start(bf16[3072,128]{1,0:T(8,128)(2,1)} %collective-permute-done.3.refs_3_), channel_id=1, source_target_pairs={{0,1},{1,0},{2,3},{3,2},{4,5},{5,4},{6,7},{7,6},{8,9},{9,8},{10,11... | collective-permute-start | bytes 2359304 | tf_op jit(solution)/shard_map/ppermute | solution.py:557
  95.4 43.4 %all-to-all-start.1 = ((bf16[256,16,128]{2,1,0:T(8,128)(2,1)}), bf16[256,16,128]{2,1,0:T(8,128)(2,1)S(1)}, u32[]{:S(2)}, u32[]{:S(2)}) async-start(bf16[256,16,128]{2,1,0:T(8,128)(2,1)} %bitcast.38), calls=%async_computation.1 | async-start | bytes 2097152 | tf_op jit(solution)/shard_map/all_to_all | solution.py:590
  107.6 48.3 %collective-permute-start.1 = (bf16[2,192,2048]{2,1,0:T(8,128)(2,1)}, bf16[2,192,2048]{2,1,0:T(8,128)(2,1)}, u32[]{:S(2)}, u32[]{:S(2)}) collective-permute-start(bf16[2,192,2048]{2,1,0:T(8,128)(2,1)} %select.3.rows_ref.refs_0_), channel_id=1, source_target_pairs={{0,6},{2,0},{4,2},{6,4},{1,7},{3,1},{5,3},{7,5},{8,14},{10,8},{12,... | collective-permute-start | bytes 4718600 | tf_op jit(solution)/shard_map/ppermute | solution.py:557
  108.5 55.6 %collective-permute-start = (bf16[2,192,2048]{2,1,0:T(8,128)(2,1)}, bf16[2,192,2048]{2,1,0:T(8,128)(2,1)}, u32[]{:S(2)}, u32[]{:S(2)}) collective-permute-start(bf16[2,192,2048]{2,1,0:T(8,128)(2,1)} %select.3.rows_ref.refs_0_), channel_id=1, source_target_pairs={{0,2},{2,4},{4,6},{6,0},{1,3},{3,5},{5,7},{7,1},{8,10},{10,12},{12... | collective-permute-start | bytes 4718600 | tf_op jit(solution)/shard_map/ppermute | solution.py:557
  141.0 18.6 %collective-permute-start.16 = (bf16[256,384]{1,0:T(8,128)(2,1)S(1)}, bf16[256,384]{1,0:T(8,128)(2,1)S(1)}, u32[]{:S(2)}, u32[]{:S(2)}) collective-permute-start(bf16[256,384]{1,0:T(8,128)(2,1)S(1)} %combine.1.refs_0_), channel_id=1, source_target_pairs={{0,2},{2,4},{4,6},{6,0},{1,3},{3,5},{5,7},{7,1},{8,10},{10,12},{12... | collective-permute-start | bytes 589832 | tf_op jit(solution)/shard_map/ppermute | solution.py:557
  141.7 21.9 %collective-permute-start.17 = (bf16[256,384]{1,0:T(8,128)(2,1)S(1)}, bf16[256,384]{1,0:T(8,128)(2,1)S(1)}, u32[]{:S(2)}, u32[]{:S(2)}) collective-permute-start(bf16[256,384]{1,0:T(8,128)(2,1)S(1)} %combine.1.refs_0_), channel_id=1, source_target_pairs={{0,6},{2,0},{4,2},{6,4},{1,7},{3,1},{5,3},{7,5},{8,14},{10,8},{12,... | collective-permute-start | bytes 589832 | tf_op jit(solution)/shard_map/ppermute | solution.py:557
  143.1 20.4 %collective-permute-start.18 = (bf16[256,384]{1,0:T(8,128)(2,1)S(1)}, bf16[256,384]{1,0:T(8,128)(2,1)S(1)}, u32[]{:S(2)}, u32[]{:S(2)}) collective-permute-start(bf16[256,384]{1,0:T(8,128)(2,1)S(1)} %combine.1.refs_0_), channel_id=1, source_target_pairs={{0,4},{2,6},{4,0},{6,2},{1,5},{3,7},{5,1},{7,3},{8,12},{10,14},{12... | collective-permute-start | bytes 589832 | tf_op jit(solution)/shard_map/ppermute | solution.py:557
  169.6 46.6 %collective-permute-start.23 = (bf16[192,2048]{1,0:T(8,128)(2,1)S(1)}, bf16[192,2048]{1,0:T(8,128)(2,1)S(1)}, u32[]{:S(2)}, u32[]{:S(2)}) collective-permute-start(bf16[192,2048]{1,0:T(8,128)(2,1)S(1)} %slice_bitcast_fusion.1), channel_id=1, source_target_pairs={{0,2},{2,4},{4,6},{6,0},{1,3},{3,5},{5,7},{7,1},{8,10},{10,12},{12... | collective-permute-start | bytes 2359304 | tf_op jit(solution)/shard_map/ppermute | solution.py:557
  172.6 43.7 %collective-permute-start.24 = (bf16[192,2048]{1,0:T(8,128)(2,1)S(1)}, bf16[192,2048]{1,0:T(8,128)(2,1)S(1)}, u32[]{:S(2)}, u32[]{:S(2)}) collective-permute-start(bf16[192,2048]{1,0:T(8,128)(2,1)S(1)} %slice_bitcast_fusion), channel_id=1, source_target_pairs={{0,6},{2,0},{4,2},{6,4},{1,7},{3,1},{5,3},{7,5},{8,14},{10,8},{12,... | collective-permute-start | bytes 2359304 | tf_op jit(solution)/shard_map/ppermute | solution.py:557
  172.6 33.2 %collective-permute-start.26 = (bf16[3,192,256]{2,1,0:T(8,128)(2,1)S(1)}, bf16[3,192,256]{2,1,0:T(8,128)(2,1)S(1)}, u32[]{:S(2)}, u32[]{:S(2)}) collective-permute-start(bf16[3,192,256]{2,1,0:T(8,128)(2,1)S(1)} %copy-done.28), channel_id=1, source_target_pairs={{0,6},{2,0},{4,2},{6,4},{1,7},{3,1},{5,3},{7,5},{8,14},{10,8},{12,... | collective-permute-start | bytes 884744 | tf_op jit(solution)/shard_map/ppermute | solution.py:557
  172.6 33.2 %collective-permute-start.27 = (bf16[3,192,256]{2,1,0:T(8,128)(2,1)S(1)}, bf16[3,192,256]{2,1,0:T(8,128)(2,1)S(1)}, u32[]{:S(2)}, u32[]{:S(2)}) collective-permute-start(bf16[3,192,256]{2,1,0:T(8,128)(2,1)S(1)} %copy-done.27), channel_id=1, source_target_pairs={{0,2},{2,4},{4,6},{6,0},{1,3},{3,5},{5,7},{7,1},{8,10},{10,12},{12... | collective-permute-start | bytes 884744 | tf_op jit(solution)/shard_map/ppermute | solution.py:557
  175.9 40.3 %collective-permute-start.25 = (bf16[3,192,256]{2,1,0:T(8,128)(2,1)S(1)}, bf16[3,192,256]{2,1,0:T(8,128)(2,1)S(1)}, u32[]{:S(2)}, u32[]{:S(2)}) collective-permute-start(bf16[3,192,256]{2,1,0:T(8,128)(2,1)S(1)} %copy-done.26), channel_id=1, source_target_pairs={{0,4},{2,6},{4,0},{6,2},{1,5},{3,7},{5,1},{7,3},{8,12},{10,14},{12... | collective-permute-start | bytes 884744 | tf_op jit(solution)/shard_map/ppermute | solution.py:557
  222.8 45.7 %collective-permute-start.28 = (f32[3,2048,128]{2,1,0:T(8,128)}, f32[3,2048,128]{2,1,0:T(8,128)}, u32[]{:S(2)}, u32[]{:S(2)}) collective-permute-start(f32[3,2048,128]{2,1,0:T(8,128)} %get-tuple-element.59), channel_id=1, source_target_pairs={{0,1},{1,0},{2,3},{3,2},{4,5},{5,4},{6,7},{7,6},{8,9},{9,8},{10,11... | collective-permute-start | bytes 9437192 | tf_op jit(solution)/shard_map/ppermute | solution.py:557
  224.4 21.6 %collective-permute-start.30 = (bf16[8,64,352]{2,1,0:T(8,128)(2,1)S(1)}, bf16[8,64,352]{2,1,0:T(8,128)(2,1)S(1)}, u32[]{:S(2)}, u32[]{:S(2)}) collective-permute-start(bf16[8,64,352]{2,1,0:T(8,128)(2,1)S(1)} %copy-done.25), channel_id=1, source_target_pairs={{0,16},{8,24},{16,0},{24,8},{1,17},{9,25},{17,1},{25,9},{2,18},{10... | collective-permute-start | bytes 1081352 | tf_op jit(solution)/shard_map/ppermute | solution.py:557
  226.9 19.1 %collective-permute-start.31 = (bf16[8,64,352]{2,1,0:T(8,128)(2,1)S(1)}, bf16[8,64,352]{2,1,0:T(8,128)(2,1)S(1)}, u32[]{:S(2)}, u32[]{:S(2)}) collective-permute-start(bf16[8,64,352]{2,1,0:T(8,128)(2,1)S(1)} %copy-done.24), channel_id=1, source_target_pairs={{0,24},{8,0},{16,8},{24,16},{1,25},{9,1},{17,9},{25,17},{2,26},{10... | collective-permute-start | bytes 1081352 | tf_op jit(solution)/shard_map/ppermute | solution.py:557
  246.9 20.9 %all-to-all-start.2 = ((bf16[8,64,352]{2,1,0:T(8,128)(2,1)}), bf16[8,64,352]{2,1,0:T(8,128)(2,1)S(1)}, u32[]{:S(2)}, u32[]{:S(2)}) async-start(bf16[8,64,352]{2,1,0:T(8,128)(2,1)} %add_convert_fusion), calls=%async_computation.2 | async-start | bytes 786432 | tf_op jit(solution)/shard_map/all_to_all | solution.py:609
  (41 other events, 523.5 us)

commit v2 on v0

--- a/solution.py
+++ b/solution.py
@@ -1,5 +1,3 @@
-import functools
-
 import jax
 import jax.numpy as jnp
 from jax import lax
@@ -289,71 +287,72 @@
 
 def weight_grad_kernel(*refs):
     rows, far, acts = refs[0:3], refs[3:5], refs[5:9]
-    keep_ref, send_ref, xbuf, hbuf, sems = refs[9:]
+    keep_ref, send_ref, xbuf, hbuf, turned, sems = refs[9:]
     copies = []
     for n in range(4):
         at = pl.ds(ROWS * n, ROWS)
         if n < 3:
-            copies.append(pltpu.make_async_copy(rows[n], xbuf.at[:, at, :], sems.at[0, n]))
+            copies.append(pltpu.make_async_copy(rows[n], xbuf.at[:, at, :], sems.at[3, n]))
         act = acts[n].at[0] if n == 0 else acts[n]
-        copies.append(pltpu.make_async_copy(act, hbuf.at[:, at, :], sems.at[1, n]))
+        for k in range(3):
+            copies.append(pltpu.make_async_copy(act.at[k], hbuf.at[at, pl.ds(256 * k, 256)], sems.at[k, n]))
     for n in range(2):
-        copies.append(pltpu.make_async_copy(far[n], xbuf.at[n, pl.ds(3 * ROWS, ROWS), :], sems.at[0, 3 + n]))
+        copies.append(pltpu.make_async_copy(far[n], xbuf.at[n, pl.ds(3 * ROWS, ROWS), :], sems.at[4, n]))
     for copy in copies:
         copy.start()
     for copy in copies:
         copy.wait()
+    turned[...] = hbuf[:, 512:].T
 
     def columns(t, _):
         cols = pl.ds(pl.multiple_of(256 * t, 256), 256)
+        both = dot_tn(xbuf[0, :, cols], hbuf[:, :512])
         for n in range(2):
-            both = dot_tn(xbuf[0, :, cols], hbuf[n])
-            rows = pl.ds(pl.multiple_of(D * n + 256 * t, 256), 256)
-            keep_ref[rows, :] = both[:, :128]
-            send_ref[rows, :] = both[:, 128:]
-        both = dot_tn(hbuf[2], xbuf[1, :, cols])
+            keep_ref[n, cols, :] = both[:, 256 * n : 256 * n + 128]
+            send_ref[n, cols, :] = both[:, 256 * n + 128 : 256 * n + 256].astype(BF16)
+        both = dot(turned[...], xbuf[1, :, cols])
         for h in range(2):
-            rows = pl.ds(pl.multiple_of(2 * D + 256 * t + 128 * h, 128), 128)
-            keep_ref[rows, :] = both[:128, 128 * h : 128 * h + 128]
-            send_ref[rows, :] = both[128:, 128 * h : 128 * h + 128]
+            at = pl.ds(pl.multiple_of(256 * t + 128 * h, 128), 128)
+            keep_ref[2, at, :] = both[:128, 128 * h : 128 * h + 128]
+            send_ref[2, at, :] = both[128:, 128 * h : 128 * h + 128].astype(BF16)
         return 0
 
     lax.fori_loop(0, N_TP, columns, 0)
 
 
 def weight_grads(rows, far, acts):
-    part = pltpu.HBM((3 * D, 128), F32)
     return pl.pallas_call(
         weight_grad_kernel,
         in_specs=[pl.BlockSpec(memory_space=pl.ANY)] * 9,
-        out_shape=(part, part),
+        out_shape=(pltpu.HBM((3, D, 128), F32), pltpu.HBM((3, D, 128), BF16)),
         scratch_shapes=[
             pltpu.VMEM((2, 4 * ROWS, D), BF16),
-            pltpu.VMEM((3, 4 * ROWS, 256), BF16),
-            pltpu.SemaphoreType.DMA((2, 5)),
+            pltpu.VMEM((4 * ROWS, 768), BF16),
+            pltpu.VMEM((256, 4 * ROWS), BF16),
+            pltpu.SemaphoreType.DMA((5, 4)),
         ],
-        compiler_params=vmem(26),
+        compiler_params=vmem(24),
         name="weight_grads",
     )(*in_hbm(*rows, *far, *acts))
 
 
-def finish_kernel(keep_g, keep_u, keep_d, got_g, got_u, got_d, gate_ref, up_ref, down_ref):
-    gate_ref[...] = keep_g[...] + got_g[...]
-    up_ref[...] = keep_u[...] + got_u[...]
-    for n in range(4):
-        rows = slice(128 * n, 128 * n + 128)
-        down_ref[:, rows] = keep_d[rows, :] + got_d[rows, :]
+def finish_kernel(keep_ref, got_ref, gate_ref, up_ref, down_ref):
+    gate_ref[...] = keep_ref[0] + got_ref[0].astype(F32)
+    up_ref[...] = keep_ref[1] + got_ref[1].astype(F32)
+    for n in range(keep_ref.shape[1] // 128):
+        at = slice(128 * n, 128 * n + 128)
+        down_ref[:, at] = keep_ref[2, at, :] + got_ref[2, at, :].astype(F32)
 
 
 def finish(keep, got):
     block = 512
-    count = D // block
-    tall = [pl.BlockSpec((block, 128), functools.partial(lambda k, n: (n + k * count, 0), k)) for k in range(3)]
+    sums = pl.BlockSpec((3, block, 128), lambda t: (0, t, 0))
+    tall = pl.BlockSpec((block, 128), lambda t: (t, 0))
     return pl.pallas_call(
         finish_kernel,
-        grid=(count,),
-        in_specs=tall + tall,
-        out_specs=(tall[0], tall[0], pl.BlockSpec((128, block), lambda n: (0, n))),
+        grid=(D // block,),
+        in_specs=[sums, sums],
+        out_specs=(tall, tall, pl.BlockSpec((128, block), lambda t: (0, t))),
         out_shape=(
             jax.ShapeDtypeStruct((D, 128), F32),
             jax.ShapeDtypeStruct((D, 128), F32),
@@ -361,7 +360,7 @@
         ),
         compiler_params=vmem(8),
         name="finish",
-    )(*[in_hbm(keep)] * 3, *[in_hbm(got)] * 3)
+    )(in_hbm(keep), got)
 
 
 def combine_kernel(tp_ref, place_ref, back_ref, cot_ref, out_ref):
@@ -496,7 +495,7 @@
         out_shape=jax.ShapeDtypeStruct((CH, TOK), F32),
         compiler_params=vmem(6),
         name="local_scan",
-    )(direct, log_decay)
+    )(in_hbm(direct), log_decay)
 
 
 def recur_kernel(at_ref, links_ref, local_ref, suffix_ref, log_ref, before_ref, step_ref, decay_ref, turn_ref):
@@ -523,7 +522,7 @@
         scratch_shapes=[pltpu.VMEM((128, TOK), F32)],
         compiler_params=vmem(8),
         name="recur",
-    )(at, links, local, suffix, log_decay, state_before)
+    )(at, links, local, in_hbm(suffix), log_decay, state_before)
 
 
 def shifted(value, axis, by):
@@ -565,13 +564,14 @@
     all_acts = [acts]
     for j, by in ((1, -1), (2, 1), (3, 2)):
         all_acts.append(shifted(acts[j], "y", by))
+    far_in, far_cot, back = lax.optimization_barrier((rows_before[0], rows_after[1], back))
     part = combine(tp_vec, placed, back, cotangent)
 
     near = (part, shifted(part, "y", 1), shifted(part, "y", -1), shifted(part, "y", 2))
     grads = (*near, *(shifted(g, "c", 1) for g in near))
     *pieces, grad_gate_pre, direct, link = project(order, grads, out_proj.T, mixed, gelu, slope, prefix)
 
-    far_in, far_cot, pieces[0] = lax.optimization_barrier((rows_before[0], rows_after[1], pieces[0]))
+    far_in, far_cot, pieces[0] = lax.optimization_barrier((far_in, far_cot, pieces[0]))
 
     over_x = [pieces[0]]
     for m in (1, 2, 3):

time: 271 us -> 290 us (1.070)
  waiting for transfers between devices: 122 us -> 135 us
  local copies, waits for them, and re-layouts: 13.2 us -> 16.1 us
    ppermute x32, waiting for transfers between devices: 101 us -> 130 us  [shifted(): return lax.ppermute(value, axis, [(i, (i + by) % n) for i in range(n)])]
    all_to_all x1, waiting for transfers between devices: 14.9 us -> 0.01 us  [on_device(): lax.all_to_all(back.reshape(N_EXP * N_TP, 16, 128), ALL, split_axis=0, co...]
  transfers between devices with their start and end apart: 36 -> 36, of which waited for: 16 -> 15; matrix products, arithmetic and copies ran while one was open for 2% -> 2% of each run, Pallas kernels for 9% -> 14%
where the time goes in v2:
time: 290 us; the launch traced here: 288 us
  waiting for transfers between devices  135 us (47%)
  starting transfers between devices  70 us (24%)
  Pallas kernels  64.1 us (22%)
  local copies, waits for them, and re-layouts  16.1 us (6%)
    ppermute x32, waiting for transfers between devices, shifted(): return lax.ppermute(value, axis, [(i, (i + by) % n) for i in range(n)])  130 us
    ppermute x32, starting transfers between devices, shifted(): return lax.ppermute(value, axis, [(i, (i + by) % n) for i in range(n)])  30.3 us
    pallas_call x1, Pallas kernels, experts(): pl.pallas_call(expert_kernel, in_specs=[pl.BlockSpec(memory_space=pltpu.V...  14.2 us
    all_to_all x1, starting transfers between devices, on_device(): lax.all_to_all(back.reshape(N_EXP * N_TP, 16, 128), ALL, split_axis=0, co...  12.9 us
    all_to_all x1, starting transfers between devices, on_device(): got = lax.all_to_all(sent, SP, split_axis=0, concat_axis=0, tiled=True)  11.3 us
    unnamed x65, local copies, waits for them, and re-layouts  11.2 us
    pallas_call x1, Pallas kernels, weight_grads(): pl.pallas_call(weight_grad_kernel, in_specs=[pl.BlockSpec(memory_space=pl...  9.87 us
    all_to_all x1, starting transfers between devices, on_device(): links = lax.all_to_all(link, SP, split_axis=0, concat_axis=0, tiled=True)  8.58 us
  transfers between devices with their start and end apart: 36, of which 15 were waited for; matrix products, arithmetic and copies ran while one was open for 2% of the time, Pallas kernels for 14%

profile of v2, /device:TPU:8, one launch (start us, length us, event | category | flops | bytes accessed | tf_op | source)
XLA Modules:
  0.0 287.6 jit_solution(16149186627299030744)
XLA Ops:
  4.8 4.1 %dispatch.1 = bf16[32,24,1024]{2,1,0:T(8,128)(2,1)} custom-call(s32[1]{0:T(128)} %bitcast.tp_ref, s32[2,384]{1,0:T(2,128)S(1)} %bitcast.42, f32[2,384]{1,0:T(2,128)S(1)} %bitcast.43, bf16[384,2048]{1,0:T(8,128)(2,1)S(1)} %copy-done.2, bf16[384,2048]{1,0:T(8,128)(2,1)S(1)} %copy-done.2, bf16[384,2048]{1,0:T(8,128)(2,1)S(1)} %copy-done, ...), custom_call_target="tpu_custom_call" | custom-call | tf_op jit(solution)/shard_map/dispatch/pallas_call | solution.py:134
  9.0 11.3 %all-to-all-start = ((bf16[32,24,1024]{2,1,0:T(8,128)(2,1)}), bf16[32,24,1024]{2,1,0:T(8,128)(2,1)S(1)}, u32[]{:S(2)}, u32[]{:S(2)}) async-start(bf16[32,24,1024]{2,1,0:T(8,128)(2,1)} %dispatch.1), calls=%async_computation | async-start | bytes 3145728 | tf_op jit(solution)/shard_map/all_to_all | solution.py:550
  26.9 16.6 %collective-permute-done.2.refs_2_ = bf16[3072,128]{1,0:T(8,128)(2,1)S(1)} collective-permute-done((bf16[3072,128]{1,0:T(8,128)(2,1)}, bf16[3072,128]{1,0:T(8,128)(2,1)S(1)}, u32[]{:S(2)}, u32[]{:S(2)}) %collective-permute-start.2) | collective-permute-done | bytes 786464 | tf_op jit(solution)/shard_map/ppermute | solution.py:530
  46.4 13.9 %collective-permute-done.3.refs_3_ = bf16[3072,128]{1,0:T(8,128)(2,1)S(1)} collective-permute-done((bf16[3072,128]{1,0:T(8,128)(2,1)}, bf16[3072,128]{1,0:T(8,128)(2,1)S(1)}, u32[]{:S(2)}, u32[]{:S(2)}) %collective-permute-start.3) | collective-permute-done | bytes 786464 | tf_op jit(solution)/shard_map/ppermute | solution.py:530
  63.6 12.3 %collective-permute-done.6.refs_6_ = bf16[3072,128]{1,0:T(8,128)(2,1)} collective-permute-done((bf16[3072,128]{1,0:T(8,128)(2,1)S(1)}, bf16[3072,128]{1,0:T(8,128)(2,1)}, u32[]{:S(2)}, u32[]{:S(2)}) %collective-permute-start.6) | collective-permute-done | bytes 786464 | tf_op jit(solution)/shard_map/ppermute | solution.py:530
  81.7 14.2 %experts.1 = (bf16[32,8,16,128]{3,2,1,0:T(8,128)(2,1)}, bf16[4,3,192,256]{3,2,1,0:T(8,128)(2,1)}) custom-call(bf16[2,192,2048]{2,1,0:T(8,128)(2,1)} %select.3.rows_ref.refs_0_, bf16[3072,128]{1,0:T(8,128)(2,1)} %get-tuple-element.39.refs_0_, bf16[3072,128]{1,0:T(8,128)(2,1)} %get-tuple-element.40.refs_1_, bf16[3072,128]{1,0:T(8,128)(2,1)} %copy-done.17, ...), custom_call_target="tpu_custom_call" | custom-call | tf_op jit(solution)/shard_map/experts/pallas_call | solution.py:273
  95.9 12.9 %all-to-all-start.1 = ((bf16[256,16,128]{2,1,0:T(8,128)(2,1)}), bf16[256,16,128]{2,1,0:T(8,128)(2,1)S(1)}, u32[]{:S(2)}, u32[]{:S(2)}) async-start(bf16[256,16,128]{2,1,0:T(8,128)(2,1)} %bitcast.44), calls=%async_computation.1 | async-start | bytes 2097152 | tf_op jit(solution)/shard_map/all_to_all | solution.py:563
  112.7 8.4 %collective-permute-done.refs_1_ = bf16[2,192,2048]{2,1,0:T(8,128)(2,1)} collective-permute-done((bf16[2,192,2048]{2,1,0:T(8,128)(2,1)}, bf16[2,192,2048]{2,1,0:T(8,128)(2,1)}, u32[]{:S(2)}, u32[]{:S(2)}) %collective-permute-start) | collective-permute-done | bytes 1572896 | tf_op jit(solution)/shard_map/ppermute | solution.py:530
  123.1 32.7 %collective-permute-done.1.refs_2_ = bf16[2,192,2048]{2,1,0:T(8,128)(2,1)} collective-permute-done((bf16[2,192,2048]{2,1,0:T(8,128)(2,1)}, bf16[2,192,2048]{2,1,0:T(8,128)(2,1)}, u32[]{:S(2)}, u32[]{:S(2)}) %collective-permute-start.1) | collective-permute-done | bytes 1572896 | tf_op jit(solution)/shard_map/ppermute | solution.py:530
  164.6 3.5 %collective-permute-done.16.refs_1_ = bf16[256,384]{1,0:T(8,128)(2,1)S(1)} collective-permute-done((bf16[256,384]{1,0:T(8,128)(2,1)S(1)}, bf16[256,384]{1,0:T(8,128)(2,1)S(1)}, u32[]{:S(2)}, u32[]{:S(2)}) %collective-permute-start.16) | collective-permute-done | bytes 196640 | tf_op jit(solution)/shard_map/ppermute | solution.py:530
  168.7 4.3 %collective-permute-done.18.refs_3_ = bf16[256,384]{1,0:T(8,128)(2,1)S(1)} collective-permute-done((bf16[256,384]{1,0:T(8,128)(2,1)S(1)}, bf16[256,384]{1,0:T(8,128)(2,1)S(1)}, u32[]{:S(2)}, u32[]{:S(2)}) %collective-permute-start.18) | collective-permute-done | bytes 196640 | tf_op jit(solution)/shard_map/ppermute | solution.py:530
  173.0 8.1 %prepare.1 = (bf16[384,352]{1,0:T(8,128)(2,1)}, f32[352,384]{1,0:T(8,128)}, f32[352,384]{1,0:T(8,128)}, f32[352,384]{1,0:T(8,128)}, f32[352,384]{1,0:T(8,128)}) custom-call(bf16[352,384]{1,0:T(8,128)(2,1)S(1)} %bitcast.40, f32[352,384]{1,0:T(8,128)S(1)} %bitcast.34, f32[352,384]{1,0:T(8,128)S(1)} %bitcast.37, bf16[352,384]{1,0:T(8,128)(2,1)S(1)} %bitcast.41), custom_call_target="tpu_custom_call" | custom-call | tf_op jit(solution)/shard_map/prepare/pallas_call | solution.py:425
  185.3 4.1 %project.1 = (bf16[8,64,352]{2,1,0:T(8,128)(2,1)}, bf16[8,64,352]{2,1,0:T(8,128)(2,1)}, bf16[8,64,352]{2,1,0:T(8,128)(2,1)}, bf16[8,64,352]{2,1,0:T(8,128)(2,1)}...) custom-call(s32[9]{0:T(128)S(1)} %pad_add_fusion.order_ref, ...), custom_call_target="tpu_custom_call" | custom-call | tf_op jit(solution)/shard_map/project/pallas_call | solution.py:458
  194.1 4.1 %collective-permute-start.27 = (bf16[3,192,256]{2,1,0:T(8,128)(2,1)S(1)}, bf16[3,192,256]{2,1,0:T(8,128)(2,1)S(1)}, u32[]{:S(2)}, u32[]{:S(2)}) collective-permute-start(bf16[3,192,256]{2,1,0:T(8,128)(2,1)S(1)} %get-tuple-element.71), channel_id=1, source_target_pairs={{0,4},{2,6},{4,0},{6,2},{1,5},{3,7},{5,1},{7,3},{8,12},{10,14},{12... | collective-permute-start | bytes 884744 | tf_op jit(solution)/shard_map/ppermute | solution.py:530
  198.2 18.9 %collective-permute-done.25.refs_6_ = bf16[3,192,256]{2,1,0:T(8,128)(2,1)S(1)} collective-permute-done((bf16[3,192,256]{2,1,0:T(8,128)(2,1)S(1)}, bf16[3,192,256]{2,1,0:T(8,128)(2,1)S(1)}, u32[]{:S(2)}, u32[]{:S(2)}) %collective-permute-start.25) | collective-permute-done | bytes 294944 | tf_op jit(solution)/shard_map/ppermute | solution.py:530
  217.0 7.4 %collective-permute-done.27.refs_8_ = bf16[3,192,256]{2,1,0:T(8,128)(2,1)S(1)} collective-permute-done((bf16[3,192,256]{2,1,0:T(8,128)(2,1)S(1)}, bf16[3,192,256]{2,1,0:T(8,128)(2,1)S(1)}, u32[]{:S(2)}, u32[]{:S(2)}) %collective-permute-start.27) | collective-permute-done | bytes 294944 | tf_op jit(solution)/shard_map/ppermute | solution.py:530
  226.3 9.9 %weight_grads.1 = (f32[3,2048,128]{2,1,0:T(8,128)}, bf16[3,2048,128]{2,1,0:T(8,128)(2,1)}) custom-call(bf16[2,192,2048]{2,1,0:T(8,128)(2,1)} %select.3.rows_ref.refs_0_, bf16[2,192,2048]{2,1,0:T(8,128)(2,1)} %collective-permute-done.refs_1_, bf16[2,192,2048]{2,1,0:T(8,128)(2,1)} %collective-permute-done.1.refs_2_, bf16[192,2048]{1,0:T(8,128)(2,1)} %copy-done.20, ...), custom_call_target="tpu_custom_call" | custom-call | tf_op jit(solution)/shard_map/weight_grads/pallas_call | solution.py:324
  238.3 2.5 collective-permute-start.30
  242.7 8.6 %all-to-all-start.3 = ((f32[32,2,352]{2,1,0:T(2,128)}), f32[32,2,352]{2,1,0:T(2,128)S(1)}, u32[]{:S(2)}, u32[]{:S(2)}) async-start(f32[32,2,352]{2,1,0:T(2,128)} %broadcast_in_dim.27), calls=%async_computation.3 | async-start | bytes 196608 | tf_op jit(solution)/shard_map/all_to_all | solution.py:580
  251.3 8.0 %collective-permute-done.30 = bf16[8,64,352]{2,1,0:T(8,128)(2,1)S(1)} collective-permute-done((bf16[8,64,352]{2,1,0:T(8,128)(2,1)S(1)}, bf16[8,64,352]{2,1,0:T(8,128)(2,1)S(1)}, u32[]{:S(2)}, u32[]{:S(2)}) %collective-permute-start.30) | collective-permute-done | bytes 360480 | tf_op jit(solution)/shard_map/ppermute | solution.py:530
  261.5 6.9 %all-to-all-start.2 = ((bf16[8,64,352]{2,1,0:T(8,128)(2,1)}), bf16[8,64,352]{2,1,0:T(8,128)(2,1)S(1)}, u32[]{:S(2)}, u32[]{:S(2)}) async-start(bf16[8,64,352]{2,1,0:T(8,128)(2,1)} %add_convert_fusion), calls=%async_computation.2 | async-start | bytes 786432 | tf_op jit(solution)/shard_map/all_to_all | solution.py:582
  268.4 8.0 %local_scan.1.local_ref = f32[352,384]{1,0:T(8,128)S(1)} custom-call(f32[352,384]{1,0:T(8,128)} %get-tuple-element.65.direct_ref, f32[352,384]{1,0:T(8,128)S(1)} %bitcast.35), custom_call_target="tpu_custom_call" | custom-call | tf_op jit(solution)/shard_map/local_scan/pallas_call | solution.py:493
  278.8 3.6 %all-to-all-done.2 = bf16[8,64,352]{2,1,0:T(8,128)(2,1)S(1)} async-done(((bf16[8,64,352]{2,1,0:T(8,128)(2,1)}), bf16[8,64,352]{2,1,0:T(8,128)(2,1)S(1)}, u32[]{:S(2)}, u32[]{:S(2)}) %all-to-all-start.2) | async-done | bytes 360480 | tf_op jit(solution)/shard_map/all_to_all | solution.py:582
  283.2 4.5 %finish.1 = (f32[2048,128]{1,0:T(8,128)}, f32[2048,128]{1,0:T(8,128)}, f32[128,2048]{1,0:T(8,128)}) custom-call(f32[3,2048,128]{2,1,0:T(8,128)} %get-tuple-element.54.keep_ref, bf16[3,2048,128]{2,1,0:T(8,128)(2,1)} %collective-permute-done.28.got_ref), custom_call_target="tpu_custom_call" | custom-call | tf_op jit(solution)/shard_map/finish/pallas_call | solution.py:351
  (134 shorter events, 58.0 us)
Async XLA Ops:
  9.0 69.0 %all-to-all-start = ((bf16[32,24,1024]{2,1,0:T(8,128)(2,1)}), bf16[32,24,1024]{2,1,0:T(8,128)(2,1)S(1)}, u32[]{:S(2)}, u32[]{:S(2)}) async-start(bf16[32,24,1024]{2,1,0:T(8,128)(2,1)} %dispatch.1), calls=%async_computation | async-start | bytes 3145728 | tf_op jit(solution)/shard_map/all_to_all | solution.py:550
  22.8 20.7 %collective-permute-start.2 = (bf16[3072,128]{1,0:T(8,128)(2,1)}, bf16[3072,128]{1,0:T(8,128)(2,1)S(1)}, u32[]{:S(2)}, u32[]{:S(2)}) collective-permute-start(bf16[3072,128]{1,0:T(8,128)(2,1)} %get-tuple-element.39.refs_0_), channel_id=1, source_target_pairs={{0,2},{2,4},{4,6},{6,0},{1,3},{3,5},{5,7},{7,1},{8,10},{10,12},{12... | collective-permute-start | bytes 2359304 | tf_op jit(solution)/shard_map/ppermute | solution.py:530
  24.4 20.7 %collective-permute-start.5 = (bf16[3072,128]{1,0:T(8,128)(2,1)}, bf16[3072,128]{1,0:T(8,128)(2,1)}, u32[]{:S(2)}, u32[]{:S(2)}) collective-permute-start(bf16[3072,128]{1,0:T(8,128)(2,1)} %get-tuple-element.40.refs_1_), channel_id=1, source_target_pairs={{0,6},{2,0},{4,2},{6,4},{1,7},{3,1},{5,3},{7,5},{8,14},{10,8},{12,... | collective-permute-start | bytes 2359304 | tf_op jit(solution)/shard_map/ppermute | solution.py:530
  24.9 35.5 %collective-permute-start.3 = (bf16[3072,128]{1,0:T(8,128)(2,1)}, bf16[3072,128]{1,0:T(8,128)(2,1)S(1)}, u32[]{:S(2)}, u32[]{:S(2)}) collective-permute-start(bf16[3072,128]{1,0:T(8,128)(2,1)} %get-tuple-element.40.refs_1_), channel_id=1, source_target_pairs={{0,2},{2,4},{4,6},{6,0},{1,3},{3,5},{5,7},{7,1},{8,10},{10,12},{12... | collective-permute-start | bytes 2359304 | tf_op jit(solution)/shard_map/ppermute | solution.py:530
  26.4 35.5 %collective-permute-start.4 = (bf16[3072,128]{1,0:T(8,128)(2,1)}, bf16[3072,128]{1,0:T(8,128)(2,1)S(1)}, u32[]{:S(2)}, u32[]{:S(2)}) collective-permute-start(bf16[3072,128]{1,0:T(8,128)(2,1)} %get-tuple-element.39.refs_0_), channel_id=1, source_target_pairs={{0,6},{2,0},{4,2},{6,4},{1,7},{3,1},{5,3},{7,5},{8,14},{10,8},{12,... | collective-permute-start | bytes 2359304 | tf_op jit(solution)/shard_map/ppermute | solution.py:530
  26.9 36.0 %collective-permute-start.8 = (bf16[3072,128]{1,0:T(8,128)(2,1)}, bf16[3072,128]{1,0:T(8,128)(2,1)}, u32[]{:S(2)}, u32[]{:S(2)}) collective-permute-start(bf16[3072,128]{1,0:T(8,128)(2,1)} %get-tuple-element.39.refs_0_), channel_id=1, source_target_pairs={{0,1},{1,0},{2,3},{3,2},{4,5},{5,4},{6,7},{7,6},{8,9},{9,8},{10,11... | collective-permute-start | bytes 2359304 | tf_op jit(solution)/shard_map/ppermute | solution.py:530
  43.5 20.0 %collective-permute-start.9 = (bf16[3072,128]{1,0:T(8,128)(2,1)}, bf16[3072,128]{1,0:T(8,128)(2,1)}, u32[]{:S(2)}, u32[]{:S(2)}) collective-permute-start(bf16[3072,128]{1,0:T(8,128)(2,1)} %get-tuple-element.40.refs_1_), channel_id=1, source_target_pairs={{0,1},{1,0},{2,3},{3,2},{4,5},{5,4},{6,7},{7,6},{8,9},{9,8},{10,11... | collective-permute-start | bytes 2359304 | tf_op jit(solution)/shard_map/ppermute | solution.py:530
  45.1 30.7 %collective-permute-start.6 = (bf16[3072,128]{1,0:T(8,128)(2,1)S(1)}, bf16[3072,128]{1,0:T(8,128)(2,1)}, u32[]{:S(2)}, u32[]{:S(2)}) collective-permute-start(bf16[3072,128]{1,0:T(8,128)(2,1)S(1)} %collective-permute-done.2.refs_2_), channel_id=1, source_target_pairs={{0,2},{2,4},{4,6},{6,0},{1,3},{3,5},{5,7},{7,1},{8,10},{10,12},{12... | collective-permute-start | bytes 2359304 | tf_op jit(solution)/shard_map/ppermute | solution.py:530
  60.3 17.0 %collective-permute-start.7 = (bf16[3072,128]{1,0:T(8,128)(2,1)}, bf16[3072,128]{1,0:T(8,128)(2,1)}, u32[]{:S(2)}, u32[]{:S(2)}) collective-permute-start(bf16[3072,128]{1,0:T(8,128)(2,1)} %collective-permute-done.5.refs_5_), channel_id=1, source_target_pairs={{0,6},{2,0},{4,2},{6,4},{1,7},{3,1},{5,3},{7,5},{8,14},{10,8},{12,... | collective-permute-start | bytes 2359304 | tf_op jit(solution)/shard_map/ppermute | solution.py:530
  62.9 17.0 %collective-permute-start.13 = (bf16[3072,128]{1,0:T(8,128)(2,1)}, bf16[3072,128]{1,0:T(8,128)(2,1)}, u32[]{:S(2)}, u32[]{:S(2)}) collective-permute-start(bf16[3072,128]{1,0:T(8,128)(2,1)} %collective-permute-done.5.refs_5_), channel_id=1, source_target_pairs={{0,1},{1,0},{2,3},{3,2},{4,5},{5,4},{6,7},{7,6},{8,9},{9,8},{10,11... | collective-permute-start | bytes 2359304 | tf_op jit(solution)/shard_map/ppermute | solution.py:530
  63.5 18.2 %collective-permute-start.11 = (bf16[3072,128]{1,0:T(8,128)(2,1)}, bf16[3072,128]{1,0:T(8,128)(2,1)}, u32[]{:S(2)}, u32[]{:S(2)}) collective-permute-start(bf16[3072,128]{1,0:T(8,128)(2,1)} %copy-done.18), channel_id=1, source_target_pairs={{0,1},{1,0},{2,3},{3,2},{4,5},{5,4},{6,7},{7,6},{8,9},{9,8},{10,11... | collective-permute-start | bytes 2359304 | tf_op jit(solution)/shard_map/ppermute | solution.py:530
  79.9 41.1 %collective-permute-start = (bf16[2,192,2048]{2,1,0:T(8,128)(2,1)}, bf16[2,192,2048]{2,1,0:T(8,128)(2,1)}, u32[]{:S(2)}, u32[]{:S(2)}) collective-permute-start(bf16[2,192,2048]{2,1,0:T(8,128)(2,1)} %select.3.rows_ref.refs_0_), channel_id=1, source_target_pairs={{0,6},{2,0},{4,2},{6,4},{1,7},{3,1},{5,3},{7,5},{8,14},{10,8},{12,... | collective-permute-start | bytes 4718600 | tf_op jit(solution)/shard_map/ppermute | solution.py:530
  95.9 62.1 %all-to-all-start.1 = ((bf16[256,16,128]{2,1,0:T(8,128)(2,1)}), bf16[256,16,128]{2,1,0:T(8,128)(2,1)S(1)}, u32[]{:S(2)}, u32[]{:S(2)}) async-start(bf16[256,16,128]{2,1,0:T(8,128)(2,1)} %bitcast.44), calls=%async_computation.1 | async-start | bytes 2097152 | tf_op jit(solution)/shard_map/all_to_all | solution.py:563
  108.8 47.1 %collective-permute-start.1 = (bf16[2,192,2048]{2,1,0:T(8,128)(2,1)}, bf16[2,192,2048]{2,1,0:T(8,128)(2,1)}, u32[]{:S(2)}, u32[]{:S(2)}) collective-permute-start(bf16[2,192,2048]{2,1,0:T(8,128)(2,1)} %select.3.rows_ref.refs_0_), channel_id=1, source_target_pairs={{0,2},{2,4},{4,6},{6,0},{1,3},{3,5},{5,7},{7,1},{8,10},{10,12},{12... | collective-permute-start | bytes 4718600 | tf_op jit(solution)/shard_map/ppermute | solution.py:530
  189.4 35.1 %collective-permute-start.23 = (bf16[192,2048]{1,0:T(8,128)(2,1)S(1)}, bf16[192,2048]{1,0:T(8,128)(2,1)S(1)}, u32[]{:S(2)}, u32[]{:S(2)}) collective-permute-start(bf16[192,2048]{1,0:T(8,128)(2,1)S(1)} %copy-done.23), channel_id=1, source_target_pairs={{0,2},{2,4},{4,6},{6,0},{1,3},{3,5},{5,7},{7,1},{8,10},{10,12},{12... | collective-permute-start | bytes 2359304 | tf_op jit(solution)/shard_map/ppermute | solution.py:530
  189.6 34.9 %collective-permute-start.24 = (bf16[192,2048]{1,0:T(8,128)(2,1)S(1)}, bf16[192,2048]{1,0:T(8,128)(2,1)S(1)}, u32[]{:S(2)}, u32[]{:S(2)}) collective-permute-start(bf16[192,2048]{1,0:T(8,128)(2,1)S(1)} %copy-done.22), channel_id=1, source_target_pairs={{0,6},{2,0},{4,2},{6,4},{1,7},{3,1},{5,3},{7,5},{8,14},{10,8},{12,... | collective-permute-start | bytes 2359304 | tf_op jit(solution)/shard_map/ppermute | solution.py:530
  191.7 25.4 %collective-permute-start.25 = (bf16[3,192,256]{2,1,0:T(8,128)(2,1)S(1)}, bf16[3,192,256]{2,1,0:T(8,128)(2,1)S(1)}, u32[]{:S(2)}, u32[]{:S(2)}) collective-permute-start(bf16[3,192,256]{2,1,0:T(8,128)(2,1)S(1)} %get-tuple-element.73), channel_id=1, source_target_pairs={{0,6},{2,0},{4,2},{6,4},{1,7},{3,1},{5,3},{7,5},{8,14},{10,8},{12,... | collective-permute-start | bytes 884744 | tf_op jit(solution)/shard_map/ppermute | solution.py:530
  194.1 23.0 %collective-permute-start.26 = (bf16[3,192,256]{2,1,0:T(8,128)(2,1)S(1)}, bf16[3,192,256]{2,1,0:T(8,128)(2,1)S(1)}, u32[]{:S(2)}, u32[]{:S(2)}) collective-permute-start(bf16[3,192,256]{2,1,0:T(8,128)(2,1)S(1)} %get-tuple-element.72), channel_id=1, source_target_pairs={{0,2},{2,4},{4,6},{6,0},{1,3},{3,5},{5,7},{7,1},{8,10},{10,12},{12... | collective-permute-start | bytes 884744 | tf_op jit(solution)/shard_map/ppermute | solution.py:530
  194.1 30.4 %collective-permute-start.27 = (bf16[3,192,256]{2,1,0:T(8,128)(2,1)S(1)}, bf16[3,192,256]{2,1,0:T(8,128)(2,1)S(1)}, u32[]{:S(2)}, u32[]{:S(2)}) collective-permute-start(bf16[3,192,256]{2,1,0:T(8,128)(2,1)S(1)} %get-tuple-element.71), channel_id=1, source_target_pairs={{0,4},{2,6},{4,0},{6,2},{1,5},{3,7},{5,1},{7,3},{8,12},{10,14},{12... | collective-permute-start | bytes 884744 | tf_op jit(solution)/shard_map/ppermute | solution.py:530
  236.2 46.9 %collective-permute-start.28 = (bf16[3,2048,128]{2,1,0:T(8,128)(2,1)}, bf16[3,2048,128]{2,1,0:T(8,128)(2,1)}, u32[]{:S(2)}, u32[]{:S(2)}) collective-permute-start(bf16[3,2048,128]{2,1,0:T(8,128)(2,1)} %get-tuple-element.55), channel_id=1, source_target_pairs={{0,1},{1,0},{2,3},{3,2},{4,5},{5,4},{6,7},{7,6},{8,9},{9,8},{10,11... | collective-permute-start | bytes 4718600 | tf_op jit(solution)/shard_map/ppermute | solution.py:530
  238.3 21.0 %collective-permute-start.30 = (bf16[8,64,352]{2,1,0:T(8,128)(2,1)S(1)}, bf16[8,64,352]{2,1,0:T(8,128)(2,1)S(1)}, u32[]{:S(2)}, u32[]{:S(2)}) collective-permute-start(bf16[8,64,352]{2,1,0:T(8,128)(2,1)S(1)} %copy-done.30), channel_id=1, source_target_pairs={{0,16},{8,24},{16,0},{24,8},{1,17},{9,25},{17,1},{25,9},{2,18},{10... | collective-permute-start | bytes 1081352 | tf_op jit(solution)/shard_map/ppermute | solution.py:530
  240.7 18.6 %collective-permute-start.31 = (bf16[8,64,352]{2,1,0:T(8,128)(2,1)S(1)}, bf16[8,64,352]{2,1,0:T(8,128)(2,1)S(1)}, u32[]{:S(2)}, u32[]{:S(2)}) collective-permute-start(bf16[8,64,352]{2,1,0:T(8,128)(2,1)S(1)} %copy-done.29), channel_id=1, source_target_pairs={{0,24},{8,0},{16,8},{24,16},{1,25},{9,1},{17,9},{25,17},{2,26},{10... | collective-permute-start | bytes 1081352 | tf_op jit(solution)/shard_map/ppermute | solution.py:530
  242.7 18.8 %all-to-all-start.3 = ((f32[32,2,352]{2,1,0:T(2,128)}), f32[32,2,352]{2,1,0:T(2,128)S(1)}, u32[]{:S(2)}, u32[]{:S(2)}) async-start(f32[32,2,352]{2,1,0:T(2,128)} %broadcast_in_dim.27), calls=%async_computation.3 | async-start | bytes 196608 | tf_op jit(solution)/shard_map/all_to_all | solution.py:580
  261.5 20.9 %all-to-all-start.2 = ((bf16[8,64,352]{2,1,0:T(8,128)(2,1)}), bf16[8,64,352]{2,1,0:T(8,128)(2,1)S(1)}, u32[]{:S(2)}, u32[]{:S(2)}) async-start(bf16[8,64,352]{2,1,0:T(8,128)(2,1)} %add_convert_fusion), calls=%async_computation.2 | async-start | bytes 786432 | tf_op jit(solution)/shard_map/all_to_all | solution.py:582
  (44 other events, 602.2 us)

commit v3 on v2

--- a/solution.py
+++ b/solution.py
@@ -210,9 +210,9 @@
     )(got)
 
 
-def expert_kernel(rows_ref, *refs):
-    weights, out_ref, acts_ref = refs[:16], refs[16], refs[17]
-    gate_up, down, grads, sems = refs[18:]
+def expert_kernel(rows_hbm, *refs):
+    weights, out_ref, acts = refs[:16], refs[16], refs[17:21]
+    rows_ref, gate_up, down, grads, made, sems, row_sems, act_sems = refs[21:]
     mid = D // 2
     copies = [[], [], [], []]
     for j in range(4):
@@ -228,9 +228,12 @@
             )
             for n, (src, dst) in enumerate(moves):
                 copies[j].append(pltpu.make_async_copy(src, dst, sems.at[j, 4 * side + n]))
-    for group in copies:
-        for copy in group:
-            copy.start()
+    rows_in = [pltpu.make_async_copy(rows_hbm.at[n], rows_ref.at[n], row_sems.at[n]) for n in range(2)]
+    acts_out = [pltpu.make_async_copy(made.at[n], acts[n], act_sems.at[n]) for n in range(4)]
+    for copy in [rows_in[0], *copies[0], rows_in[1]]:
+        copy.start()
+    for copy in rows_in:
+        copy.wait()
 
     def chunk(j, _):
         for n in range(4):
@@ -238,6 +241,9 @@
             def _():
                 for copy in copies[n]:
                     copy.wait()
+                if n < 3:
+                    for copy in copies[n + 1]:
+                        copy.start()
 
         at = pl.multiple_of(512 * j, 512)
         both = dot(rows_ref[0], gate_up[:, pl.ds(at, 512)])
@@ -247,14 +253,16 @@
         silu = gate * sig
         d_gate = (d_hidden * up * (sig * (1.0 + gate * (1.0 - sig)))).astype(BF16)
         d_up = (d_hidden * silu).astype(BF16)
-        acts_ref[j, 0] = d_gate
-        acts_ref[j, 1] = d_up
-        acts_ref[j, 2] = (silu * up).astype(BF16)
+        made[j, 0] = d_gate
+        made[j, 1] = d_up
+        made[j, 2] = (silu * up).astype(BF16)
         grads[:, pl.ds(at, 256)] = d_gate
         grads[:, pl.ds(pl.multiple_of(at + 256, 256), 256)] = d_up
         return 0
 
     lax.fori_loop(0, 4, chunk, 0)
+    for copy in acts_out:
+        copy.start()
     line = iota((8 * N_EXP, ROWS), 0)
     spread = (iota((8 * N_EXP, ROWS), 1) == (line >> 3) * PART + (line & 7)) & ((line & 7) < PART)
     spread = jnp.where(spread, 1.0, 0.0).astype(BF16)
@@ -267,73 +275,72 @@
         return 0
 
     lax.fori_loop(0, N_TP, columns, 0)
+    for copy in acts_out:
+        copy.wait()
 
 
 def experts(rows, weights):
+    act = pltpu.HBM((3, ROWS, 256), BF16)
+    anywhere = pl.BlockSpec(memory_space=pl.ANY)
     return pl.pallas_call(
         expert_kernel,
-        in_specs=[pl.BlockSpec(memory_space=pltpu.VMEM)] + [pl.BlockSpec(memory_space=pl.ANY)] * 16,
-        out_shape=(pltpu.HBM((N_EXP, N_TP, 16, 128), BF16), pltpu.HBM((4, 3, ROWS, 256), BF16)),
+        in_specs=[anywhere] * 17,
+        out_specs=(pl.BlockSpec(memory_space=pltpu.VMEM), anywhere, anywhere, anywhere, anywhere),
+        out_shape=(pltpu.HBM((N_EXP, N_TP, 16, 128), BF16), act, act, act, act),
         scratch_shapes=[
+            pltpu.VMEM((2, ROWS, D), BF16),
             pltpu.VMEM((D, D), BF16),
             pltpu.VMEM((D, D // 2), BF16),
             pltpu.VMEM((ROWS, D), BF16),
+            pltpu.VMEM((4, 3, ROWS, 256), BF16),
             pltpu.SemaphoreType.DMA((4, 8)),
+            pltpu.SemaphoreType.DMA((2,)),
+            pltpu.SemaphoreType.DMA((4,)),
         ],
         compiler_params=vmem(32),
         name="experts",
     )(*in_hbm(rows, *weights))
 
 
-def weight_grad_kernel(*refs):
-    rows, far, acts = refs[0:3], refs[3:5], refs[5:9]
-    keep_ref, send_ref, xbuf, hbuf, turned, sems = refs[9:]
-    copies = []
-    for n in range(4):
-        at = pl.ds(ROWS * n, ROWS)
-        if n < 3:
-            copies.append(pltpu.make_async_copy(rows[n], xbuf.at[:, at, :], sems.at[3, n]))
-        act = acts[n].at[0] if n == 0 else acts[n]
-        for k in range(3):
-            copies.append(pltpu.make_async_copy(act.at[k], hbuf.at[at, pl.ds(256 * k, 256)], sems.at[k, n]))
+def weight_grad_kernel(rows_0, rows_1, rows_2, far_in, far_cot, act_0, act_1, act_2, act_3,
+                       keep_ref, send_ref, hbuf, turned):
+    @pl.when(pl.program_id(0) == 0)
+    def _():
+        for n, act in enumerate((act_0, act_1, act_2, act_3)):
+            for k in range(3):
+                hbuf[ROWS * n : ROWS * (n + 1), 256 * k : 256 * (k + 1)] = act[k]
+        turned[...] = hbuf[:, 512:].T
+
+    near = (rows_0, rows_1, rows_2)
+    both = dot_tn(jnp.concatenate([*(r[0] for r in near), far_in[...]], axis=0), hbuf[:, :512])
     for n in range(2):
-        copies.append(pltpu.make_async_copy(far[n], xbuf.at[n, pl.ds(3 * ROWS, ROWS), :], sems.at[4, n]))
-    for copy in copies:
-        copy.start()
-    for copy in copies:
-        copy.wait()
-    turned[...] = hbuf[:, 512:].T
-
-    def columns(t, _):
-        cols = pl.ds(pl.multiple_of(256 * t, 256), 256)
-        both = dot_tn(xbuf[0, :, cols], hbuf[:, :512])
-        for n in range(2):
-            keep_ref[n, cols, :] = both[:, 256 * n : 256 * n + 128]
-            send_ref[n, cols, :] = both[:, 256 * n + 128 : 256 * n + 256].astype(BF16)
-        both = dot(turned[...], xbuf[1, :, cols])
-        for h in range(2):
-            at = pl.ds(pl.multiple_of(256 * t + 128 * h, 128), 128)
-            keep_ref[2, at, :] = both[:128, 128 * h : 128 * h + 128]
-            send_ref[2, at, :] = both[128:, 128 * h : 128 * h + 128].astype(BF16)
-        return 0
-
-    lax.fori_loop(0, N_TP, columns, 0)
+        keep_ref[n] = both[:, 256 * n : 256 * n + 128]
+        send_ref[n] = both[:, 256 * n + 128 : 256 * n + 256].astype(BF16)
+    both = dot(turned[...], jnp.concatenate([*(r[1] for r in near), far_cot[...]], axis=0))
+    for h in range(both.shape[1] // 128):
+        at = slice(128 * h, 128 * h + 128)
+        keep_ref[2, at, :] = both[:128, at]
+        send_ref[2, at, :] = both[128:, at].astype(BF16)
 
 
 def weight_grads(rows, far, acts):
+    block = 256
+    sums = pl.BlockSpec((3, block, 128), lambda t: (0, t, 0))
     return pl.pallas_call(
         weight_grad_kernel,
-        in_specs=[pl.BlockSpec(memory_space=pl.ANY)] * 9,
+        grid=(D // block,),
+        in_specs=[pl.BlockSpec((2, ROWS, block), lambda t: (0, 0, t))] * 3
+        + [pl.BlockSpec((ROWS, block), lambda t: (0, t))] * 2
+        + [pl.BlockSpec((3, ROWS, 256), lambda t: (0, 0, 0))] * 4,
+        out_specs=(sums, sums),
         out_shape=(pltpu.HBM((3, D, 128), F32), pltpu.HBM((3, D, 128), BF16)),
         scratch_shapes=[
-            pltpu.VMEM((2, 4 * ROWS, D), BF16),
             pltpu.VMEM((4 * ROWS, 768), BF16),
             pltpu.VMEM((256, 4 * ROWS), BF16),
-            pltpu.SemaphoreType.DMA((5, 4)),
         ],
-        compiler_params=vmem(24),
+        compiler_params=vmem(12),
         name="weight_grads",
-    )(*in_hbm(*rows, *far, *acts))
+    )(*rows, *far, *acts)
 
 
 def finish_kernel(keep_ref, got_ref, gate_ref, up_ref, down_ref):
@@ -559,9 +566,9 @@
     rows = select(got)
     rows_after = shifted(rows, "y", -1)
     rows_before = shifted(rows, "y", 1)
-    back, acts = experts(rows, weights)
+    back, *acts = experts(rows, weights)
     back = lax.all_to_all(back.reshape(N_EXP * N_TP, 16, 128), ALL, split_axis=0, concat_axis=0, tiled=True)
-    all_acts = [acts]
+    all_acts = [acts[0]]
     for j, by in ((1, -1), (2, 1), (3, 2)):
         all_acts.append(shifted(acts[j], "y", by))
     far_in, far_cot, back = lax.optimization_barrier((rows_before[0], rows_after[1], back))

time: 290 us -> 290 us (level)
    unnamed x65 -> x63, local copies, waits for them, and re-layouts: 11.2 us -> 10.3 us
  transfers between devices with their start and end apart: 36 -> 36, of which waited for: 15 -> 14; matrix products, arithmetic and copies ran while one was open for 2% -> 3% of each run, Pallas kernels for 14% -> 14%
where the time goes in v3:
time: 290 us; the launch traced here: 288 us
  waiting for transfers between devices  133 us (46%)
  starting transfers between devices  71.6 us (25%)
  Pallas kernels  64.8 us (22%)
  local copies, waits for them, and re-layouts  15.1 us (5%)
    ppermute x32, waiting for transfers between devices, shifted(): return lax.ppermute(value, axis, [(i, (i + by) % n) for i in range(n)])  129 us
    ppermute x32, starting transfers between devices, shifted(): return lax.ppermute(value, axis, [(i, (i + by) % n) for i in range(n)])  30.2 us
    pallas_call x1, Pallas kernels, experts(): pl.pallas_call(expert_kernel, in_specs=[anywhere] * 17, out_specs=(pl.Blo...  16 us
    all_to_all x1, starting transfers between devices, on_device(): lax.all_to_all(back.reshape(N_EXP * N_TP, 16, 128), ALL, split_axis=0, co...  13.6 us
    all_to_all x1, starting transfers between devices, on_device(): got = lax.all_to_all(sent, SP, split_axis=0, concat_axis=0, tiled=True)  11.3 us
    unnamed x63, local copies, waits for them, and re-layouts  10.3 us
    pallas_call x1, Pallas kernels, weight_grads(): pl.pallas_call(weight_grad_kernel, grid=(D // block,), in_specs=[pl.Block...  8.7 us
    all_to_all x1, starting transfers between devices, on_device(): links = lax.all_to_all(link, SP, split_axis=0, concat_axis=0, tiled=True)  8.58 us
  transfers between devices with their start and end apart: 36, of which 14 were waited for; matrix products, arithmetic and copies ran while one was open for 3% of the time, Pallas kernels for 14%

profile of v3, /device:TPU:8, one launch (start us, length us, event | category | flops | bytes accessed | tf_op | source)
XLA Modules:
  0.0 288.1 jit_solution(12073272621508656591)
XLA Ops:
  4.8 4.1 %dispatch.1 = bf16[32,24,1024]{2,1,0:T(8,128)(2,1)} custom-call(s32[1]{0:T(128)} %bitcast.tp_ref, s32[2,384]{1,0:T(2,128)S(1)} %bitcast.36, f32[2,384]{1,0:T(2,128)S(1)} %bitcast.37, bf16[384,2048]{1,0:T(8,128)(2,1)S(1)} %copy-done.3, bf16[384,2048]{1,0:T(8,128)(2,1)S(1)} %copy-done.3, bf16[384,2048]{1,0:T(8,128)(2,1)S(1)} %copy-done.1, ...), custom_call_target="tpu_custom_call" | custom-call | tf_op jit(solution)/shard_map/dispatch/pallas_call | solution.py:134
  9.0 11.3 %all-to-all-start = ((bf16[32,24,1024]{2,1,0:T(8,128)(2,1)}), bf16[32,24,1024]{2,1,0:T(8,128)(2,1)S(1)}, u32[]{:S(2)}, u32[]{:S(2)}) async-start(bf16[32,24,1024]{2,1,0:T(8,128)(2,1)} %dispatch.1), calls=%async_computation | async-start | bytes 3145728 | tf_op jit(solution)/shard_map/all_to_all | solution.py:557
  26.9 16.6 %collective-permute-done.2.refs_2_ = bf16[3072,128]{1,0:T(8,128)(2,1)S(1)} collective-permute-done((bf16[3072,128]{1,0:T(8,128)(2,1)}, bf16[3072,128]{1,0:T(8,128)(2,1)S(1)}, u32[]{:S(2)}, u32[]{:S(2)}) %collective-permute-start.2) | collective-permute-done | bytes 786464 | tf_op jit(solution)/shard_map/ppermute | solution.py:537
  46.3 14.0 %collective-permute-done.3.refs_3_ = bf16[3072,128]{1,0:T(8,128)(2,1)S(1)} collective-permute-done((bf16[3072,128]{1,0:T(8,128)(2,1)}, bf16[3072,128]{1,0:T(8,128)(2,1)S(1)}, u32[]{:S(2)}, u32[]{:S(2)}) %collective-permute-start.3) | collective-permute-done | bytes 786464 | tf_op jit(solution)/shard_map/ppermute | solution.py:537
  64.5 11.4 %collective-permute-done.6.refs_6_ = bf16[3072,128]{1,0:T(8,128)(2,1)} collective-permute-done((bf16[3072,128]{1,0:T(8,128)(2,1)S(1)}, bf16[3072,128]{1,0:T(8,128)(2,1)}, u32[]{:S(2)}, u32[]{:S(2)}) %collective-permute-start.6) | collective-permute-done | bytes 786464 | tf_op jit(solution)/shard_map/ppermute | solution.py:537
  81.8 16.0 %experts.1 = (bf16[32,8,16,128]{3,2,1,0:T(8,128)(2,1)}, bf16[3,192,256]{2,1,0:T(8,128)(2,1)}, bf16[3,192,256]{2,1,0:T(8,128)(2,1)}, bf16[3,192,256]{2,1,0:T(8,128)(2,1)}, bf16[3,192,256]{2,1,0:T(8,128)(2,1)}) custom-call(bf16[2,192,2048]{2,1,0:T(8,128)(2,1)} %select.3.rows_hbm.rows_0, bf16[3072,128]{1,0:T(8,128)(2,1)} %get-tuple-element.42.refs_0_, ...), custom_call_target="tpu_custom_call" | custom-call | tf_op jit(solution)/shard_map/experts/pallas_call | solution.py:285
  97.9 13.6 %all-to-all-start.1 = ((bf16[256,16,128]{2,1,0:T(8,128)(2,1)}), bf16[256,16,128]{2,1,0:T(8,128)(2,1)}, u32[]{:S(2)}, u32[]{:S(2)}) async-start(bf16[256,16,128]{2,1,0:T(8,128)(2,1)} %bitcast.38), calls=%async_computation.1 | async-start | bytes 2097152 | tf_op jit(solution)/shard_map/all_to_all | solution.py:570
  115.3 4.1 %collective-permute-done.rows_1 = bf16[2,192,2048]{2,1,0:T(8,128)(2,1)} collective-permute-done((bf16[2,192,2048]{2,1,0:T(8,128)(2,1)}, bf16[2,192,2048]{2,1,0:T(8,128)(2,1)}, u32[]{:S(2)}, u32[]{:S(2)}) %collective-permute-start) | collective-permute-done | bytes 1572896 | tf_op jit(solution)/shard_map/ppermute | solution.py:537
  121.5 36.7 %collective-permute-done.1.rows_2 = bf16[2,192,2048]{2,1,0:T(8,128)(2,1)} collective-permute-done((bf16[2,192,2048]{2,1,0:T(8,128)(2,1)S(1)}, bf16[2,192,2048]{2,1,0:T(8,128)(2,1)}, u32[]{:S(2)}, u32[]{:S(2)}) %collective-permute-start.1) | collective-permute-done | bytes 1572896 | tf_op jit(solution)/shard_map/ppermute | solution.py:537
  167.2 3.3 %collective-permute-done.16.refs_1_ = bf16[256,384]{1,0:T(8,128)(2,1)S(1)} collective-permute-done((bf16[256,384]{1,0:T(8,128)(2,1)S(1)}, bf16[256,384]{1,0:T(8,128)(2,1)S(1)}, u32[]{:S(2)}, u32[]{:S(2)}) %collective-permute-start.16) | collective-permute-done | bytes 196640 | tf_op jit(solution)/shard_map/ppermute | solution.py:537
  171.1 4.6 %collective-permute-done.18.refs_3_ = bf16[256,384]{1,0:T(8,128)(2,1)S(1)} collective-permute-done((bf16[256,384]{1,0:T(8,128)(2,1)S(1)}, bf16[256,384]{1,0:T(8,128)(2,1)S(1)}, u32[]{:S(2)}, u32[]{:S(2)}) %collective-permute-start.18) | collective-permute-done | bytes 196640 | tf_op jit(solution)/shard_map/ppermute | solution.py:537
  175.7 8.1 %prepare.1 = (bf16[384,352]{1,0:T(8,128)(2,1)}, f32[352,384]{1,0:T(8,128)}, f32[352,384]{1,0:T(8,128)}, f32[352,384]{1,0:T(8,128)}, f32[352,384]{1,0:T(8,128)}) custom-call(bf16[352,384]{1,0:T(8,128)(2,1)S(1)} %bitcast.34, f32[352,384]{1,0:T(8,128)S(1)} %bitcast.28, f32[352,384]{1,0:T(8,128)S(1)} %bitcast.31, bf16[352,384]{1,0:T(8,128)(2,1)S(1)} %bitcast.35), custom_call_target="tpu_custom_call" | custom-call | tf_op jit(solution)/shard_map/prepare/pallas_call | solution.py:432
  188.0 4.2 %project.1 = (bf16[8,64,352]{2,1,0:T(8,128)(2,1)}, bf16[8,64,352]{2,1,0:T(8,128)(2,1)}, bf16[8,64,352]{2,1,0:T(8,128)(2,1)}, bf16[8,64,352]{2,1,0:T(8,128)(2,1)}...) custom-call(s32[9]{0:T(128)S(1)} %pad_add_fusion.order_ref, ...), custom_call_target="tpu_custom_call" | custom-call | tf_op jit(solution)/shard_map/project/pallas_call | solution.py:465
  196.6 4.0 %collective-permute-start.27 = (bf16[3,192,256]{2,1,0:T(8,128)(2,1)S(1)}, bf16[3,192,256]{2,1,0:T(8,128)(2,1)S(1)}, u32[]{:S(2)}, u32[]{:S(2)}) collective-permute-start(bf16[3,192,256]{2,1,0:T(8,128)(2,1)S(1)} %copy-done.28), channel_id=1, source_target_pairs={{0,4},{2,6},{4,0},{6,2},{1,5},{3,7},{5,1},{7,3},{8,12},{10,14},{12... | collective-permute-start | bytes 884744 | tf_op jit(solution)/shard_map/ppermute | solution.py:537
  200.5 19.1 %collective-permute-done.25.act_1 = bf16[3,192,256]{2,1,0:T(8,128)(2,1)S(1)} collective-permute-done((bf16[3,192,256]{2,1,0:T(8,128)(2,1)S(1)}, bf16[3,192,256]{2,1,0:T(8,128)(2,1)S(1)}, u32[]{:S(2)}, u32[]{:S(2)}) %collective-permute-start.25) | collective-permute-done | bytes 294944 | tf_op jit(solution)/shard_map/ppermute | solution.py:537
  219.7 7.4 %collective-permute-done.27.act_3 = bf16[3,192,256]{2,1,0:T(8,128)(2,1)S(1)} collective-permute-done((bf16[3,192,256]{2,1,0:T(8,128)(2,1)S(1)}, bf16[3,192,256]{2,1,0:T(8,128)(2,1)S(1)}, u32[]{:S(2)}, u32[]{:S(2)}) %collective-permute-start.27) | collective-permute-done | bytes 294944 | tf_op jit(solution)/shard_map/ppermute | solution.py:537
  227.1 8.7 %weight_grads.1 = (f32[3,2048,128]{2,1,0:T(8,128)}, bf16[3,2048,128]{2,1,0:T(8,128)(2,1)}) custom-call(bf16[2,192,2048]{2,1,0:T(8,128)(2,1)S(1)} %copy-done, bf16[2,192,2048]{2,1,0:T(8,128)(2,1)} %collective-permute-done.rows_1, bf16[2,192,2048]{2,1,0:T(8,128)(2,1)} %collective-permute-done.1.rows_2, bf16[192,2048]{1,0:T(8,128)(2,1)S(1)} %collective-permute-done.23.far_in, ...), custom_call_target="tpu_custom_call" | custom-call | tf_op jit(solution)/shard_map/weight_grads/pallas_call | solution.py:329
  237.8 2.6 collective-permute-start.30
  242.1 8.6 %all-to-all-start.3 = ((f32[32,2,352]{2,1,0:T(2,128)}), f32[32,2,352]{2,1,0:T(2,128)S(1)}, u32[]{:S(2)}, u32[]{:S(2)}) async-start(f32[32,2,352]{2,1,0:T(2,128)} %broadcast_in_dim.27), calls=%async_computation.3 | async-start | bytes 196608 | tf_op jit(solution)/shard_map/all_to_all | solution.py:587
  250.7 8.6 %collective-permute-done.30 = bf16[8,64,352]{2,1,0:T(8,128)(2,1)S(1)} collective-permute-done((bf16[8,64,352]{2,1,0:T(8,128)(2,1)}, bf16[8,64,352]{2,1,0:T(8,128)(2,1)S(1)}, u32[]{:S(2)}, u32[]{:S(2)}) %collective-permute-start.30) | collective-permute-done | bytes 360480 | tf_op jit(solution)/shard_map/ppermute | solution.py:537
  261.3 7.9 %all-to-all-start.2 = ((bf16[8,64,352]{2,1,0:T(8,128)(2,1)}), bf16[8,64,352]{2,1,0:T(8,128)(2,1)S(1)}, u32[]{:S(2)}, u32[]{:S(2)}) async-start(bf16[8,64,352]{2,1,0:T(8,128)(2,1)} %add_convert_fusion), calls=%async_computation.2 | async-start | bytes 786432 | tf_op jit(solution)/shard_map/all_to_all | solution.py:589
  269.1 8.0 %local_scan.1.local_ref = f32[352,384]{1,0:T(8,128)S(1)} custom-call(f32[352,384]{1,0:T(8,128)} %get-tuple-element.71.direct_ref, f32[352,384]{1,0:T(8,128)S(1)} %bitcast.29), custom_call_target="tpu_custom_call" | custom-call | tf_op jit(solution)/shard_map/local_scan/pallas_call | solution.py:500
  279.6 3.6 %all-to-all-done.2 = bf16[8,64,352]{2,1,0:T(8,128)(2,1)S(1)} async-done(((bf16[8,64,352]{2,1,0:T(8,128)(2,1)}), bf16[8,64,352]{2,1,0:T(8,128)(2,1)S(1)}, u32[]{:S(2)}, u32[]{:S(2)}) %all-to-all-start.2) | async-done | bytes 360480 | tf_op jit(solution)/shard_map/all_to_all | solution.py:589
  283.9 4.2 %finish.1 = (f32[2048,128]{1,0:T(8,128)}, f32[2048,128]{1,0:T(8,128)}, f32[128,2048]{1,0:T(8,128)}) custom-call(f32[3,2048,128]{2,1,0:T(8,128)} %get-tuple-element.60.keep_ref, bf16[3,2048,128]{2,1,0:T(8,128)(2,1)S(1)} %collective-permute-done.28.got_ref), custom_call_target="tpu_custom_call" | custom-call | tf_op jit(solution)/shard_map/finish/pallas_call | solution.py:358
  (131 shorter events, 56.4 us)
Async XLA Ops:
  9.0 68.8 %all-to-all-start = ((bf16[32,24,1024]{2,1,0:T(8,128)(2,1)}), bf16[32,24,1024]{2,1,0:T(8,128)(2,1)S(1)}, u32[]{:S(2)}, u32[]{:S(2)}) async-start(bf16[32,24,1024]{2,1,0:T(8,128)(2,1)} %dispatch.1), calls=%async_computation | async-start | bytes 3145728 | tf_op jit(solution)/shard_map/all_to_all | solution.py:557
  22.8 20.7 %collective-permute-start.2 = (bf16[3072,128]{1,0:T(8,128)(2,1)}, bf16[3072,128]{1,0:T(8,128)(2,1)S(1)}, u32[]{:S(2)}, u32[]{:S(2)}) collective-permute-start(bf16[3072,128]{1,0:T(8,128)(2,1)} %get-tuple-element.42.refs_0_), channel_id=1, source_target_pairs={{0,2},{2,4},{4,6},{6,0},{1,3},{3,5},{5,7},{7,1},{8,10},{10,12},{12... | collective-permute-start | bytes 2359304 | tf_op jit(solution)/shard_map/ppermute | solution.py:537
  24.4 20.6 %collective-permute-start.5 = (bf16[3072,128]{1,0:T(8,128)(2,1)}, bf16[3072,128]{1,0:T(8,128)(2,1)S(1)}, u32[]{:S(2)}, u32[]{:S(2)}) collective-permute-start(bf16[3072,128]{1,0:T(8,128)(2,1)} %get-tuple-element.43.refs_1_), channel_id=1, source_target_pairs={{0,6},{2,0},{4,2},{6,4},{1,7},{3,1},{5,3},{7,5},{8,14},{10,8},{12,... | collective-permute-start | bytes 2359304 | tf_op jit(solution)/shard_map/ppermute | solution.py:537
  24.9 35.5 %collective-permute-start.3 = (bf16[3072,128]{1,0:T(8,128)(2,1)}, bf16[3072,128]{1,0:T(8,128)(2,1)S(1)}, u32[]{:S(2)}, u32[]{:S(2)}) collective-permute-start(bf16[3072,128]{1,0:T(8,128)(2,1)} %get-tuple-element.43.refs_1_), channel_id=1, source_target_pairs={{0,2},{2,4},{4,6},{6,0},{1,3},{3,5},{5,7},{7,1},{8,10},{10,12},{12... | collective-permute-start | bytes 2359304 | tf_op jit(solution)/shard_map/ppermute | solution.py:537
  26.4 35.5 %collective-permute-start.4 = (bf16[3072,128]{1,0:T(8,128)(2,1)}, bf16[3072,128]{1,0:T(8,128)(2,1)S(1)}, u32[]{:S(2)}, u32[]{:S(2)}) collective-permute-start(bf16[3072,128]{1,0:T(8,128)(2,1)} %get-tuple-element.42.refs_0_), channel_id=1, source_target_pairs={{0,6},{2,0},{4,2},{6,4},{1,7},{3,1},{5,3},{7,5},{8,14},{10,8},{12,... | collective-permute-start | bytes 2359304 | tf_op jit(solution)/shard_map/ppermute | solution.py:537
  26.9 35.1 %collective-permute-start.8 = (bf16[3072,128]{1,0:T(8,128)(2,1)}, bf16[3072,128]{1,0:T(8,128)(2,1)S(1)}, u32[]{:S(2)}, u32[]{:S(2)}) collective-permute-start(bf16[3072,128]{1,0:T(8,128)(2,1)} %get-tuple-element.42.refs_0_), channel_id=1, source_target_pairs={{0,1},{1,0},{2,3},{3,2},{4,5},{5,4},{6,7},{7,6},{8,9},{9,8},{10,11... | collective-permute-start | bytes 2359304 | tf_op jit(solution)/shard_map/ppermute | solution.py:537
  43.5 20.4 %collective-permute-start.9 = (bf16[3072,128]{1,0:T(8,128)(2,1)}, bf16[3072,128]{1,0:T(8,128)(2,1)}, u32[]{:S(2)}, u32[]{:S(2)}) collective-permute-start(bf16[3072,128]{1,0:T(8,128)(2,1)} %get-tuple-element.43.refs_1_), channel_id=1, source_target_pairs={{0,1},{1,0},{2,3},{3,2},{4,5},{5,4},{6,7},{7,6},{8,9},{9,8},{10,11... | collective-permute-start | bytes 2359304 | tf_op jit(solution)/shard_map/ppermute | solution.py:537
  45.0 30.8 %collective-permute-start.6 = (bf16[3072,128]{1,0:T(8,128)(2,1)S(1)}, bf16[3072,128]{1,0:T(8,128)(2,1)}, u32[]{:S(2)}, u32[]{:S(2)}) collective-permute-start(bf16[3072,128]{1,0:T(8,128)(2,1)S(1)} %collective-permute-done.2.refs_2_), channel_id=1, source_target_pairs={{0,2},{2,4},{4,6},{6,0},{1,3},{3,5},{5,7},{7,1},{8,10},{10,12},{12... | collective-permute-start | bytes 2359304 | tf_op jit(solution)/shard_map/ppermute | solution.py:537
  60.3 16.8 %collective-permute-start.7 = (bf16[3072,128]{1,0:T(8,128)(2,1)S(1)}, bf16[3072,128]{1,0:T(8,128)(2,1)}, u32[]{:S(2)}, u32[]{:S(2)}) collective-permute-start(bf16[3072,128]{1,0:T(8,128)(2,1)S(1)} %collective-permute-done.5.refs_5_), channel_id=1, source_target_pairs={{0,6},{2,0},{4,2},{6,4},{1,7},{3,1},{5,3},{7,5},{8,14},{10,8},{12,... | collective-permute-start | bytes 2359304 | tf_op jit(solution)/shard_map/ppermute | solution.py:537
  63.9 17.9 %collective-permute-start.11 = (bf16[3072,128]{1,0:T(8,128)(2,1)}, bf16[3072,128]{1,0:T(8,128)(2,1)}, u32[]{:S(2)}, u32[]{:S(2)}) collective-permute-start(bf16[3072,128]{1,0:T(8,128)(2,1)} %copy-done.21), channel_id=1, source_target_pairs={{0,1},{1,0},{2,3},{3,2},{4,5},{5,4},{6,7},{7,6},{8,9},{9,8},{10,11... | collective-permute-start | bytes 2359304 | tf_op jit(solution)/shard_map/ppermute | solution.py:537
  79.7 39.6 %collective-permute-start = (bf16[2,192,2048]{2,1,0:T(8,128)(2,1)}, bf16[2,192,2048]{2,1,0:T(8,128)(2,1)}, u32[]{:S(2)}, u32[]{:S(2)}) collective-permute-start(bf16[2,192,2048]{2,1,0:T(8,128)(2,1)} %select.3.rows_hbm.rows_0), channel_id=1, source_target_pairs={{0,6},{2,0},{4,2},{6,4},{1,7},{3,1},{5,3},{7,5},{8,14},{10,8},{12,... | collective-permute-start | bytes 4718600 | tf_op jit(solution)/shard_map/ppermute | solution.py:537
  97.9 62.4 %all-to-all-start.1 = ((bf16[256,16,128]{2,1,0:T(8,128)(2,1)}), bf16[256,16,128]{2,1,0:T(8,128)(2,1)}, u32[]{:S(2)}, u32[]{:S(2)}) async-start(bf16[256,16,128]{2,1,0:T(8,128)(2,1)} %bitcast.38), calls=%async_computation.1 | async-start | bytes 2097152 | tf_op jit(solution)/shard_map/all_to_all | solution.py:570
  111.5 46.7 %collective-permute-start.1 = (bf16[2,192,2048]{2,1,0:T(8,128)(2,1)S(1)}, bf16[2,192,2048]{2,1,0:T(8,128)(2,1)}, u32[]{:S(2)}, u32[]{:S(2)}) collective-permute-start(bf16[2,192,2048]{2,1,0:T(8,128)(2,1)S(1)} %copy-done), channel_id=1, source_target_pairs={{0,2},{2,4},{4,6},{6,0},{1,3},{3,5},{5,7},{7,1},{8,10},{10,12},{12... | collective-permute-start | bytes 4718600 | tf_op jit(solution)/shard_map/ppermute | solution.py:537
  167.2 16.6 %collective-permute-start.19 = (bf16[256,384]{1,0:T(8,128)(2,1)S(1)}, bf16[256,384]{1,0:T(8,128)(2,1)S(1)}, u32[]{:S(2)}, u32[]{:S(2)}) collective-permute-start(bf16[256,384]{1,0:T(8,128)(2,1)S(1)} %combine.1.refs_0_), channel_id=1, source_target_pairs={{0,1},{1,0},{2,3},{3,2},{4,5},{5,4},{6,7},{7,6},{8,9},{9,8},{10,11... | collective-permute-start | bytes 589832 | tf_op jit(solution)/shard_map/ppermute | solution.py:537
  192.1 35.0 %collective-permute-start.23 = (bf16[192,2048]{1,0:T(8,128)(2,1)S(1)}, bf16[192,2048]{1,0:T(8,128)(2,1)S(1)}, u32[]{:S(2)}, u32[]{:S(2)}) collective-permute-start(bf16[192,2048]{1,0:T(8,128)(2,1)S(1)} %copy-done.25), channel_id=1, source_target_pairs={{0,2},{2,4},{4,6},{6,0},{1,3},{3,5},{5,7},{7,1},{8,10},{10,12},{12... | collective-permute-start | bytes 2359304 | tf_op jit(solution)/shard_map/ppermute | solution.py:537
  192.3 34.8 %collective-permute-start.24 = (bf16[192,2048]{1,0:T(8,128)(2,1)S(1)}, bf16[192,2048]{1,0:T(8,128)(2,1)S(1)}, u32[]{:S(2)}, u32[]{:S(2)}) collective-permute-start(bf16[192,2048]{1,0:T(8,128)(2,1)S(1)} %copy-done.24), channel_id=1, source_target_pairs={{0,6},{2,0},{4,2},{6,4},{1,7},{3,1},{5,3},{7,5},{8,14},{10,8},{12,... | collective-permute-start | bytes 2359304 | tf_op jit(solution)/shard_map/ppermute | solution.py:537
  194.3 25.3 %collective-permute-start.25 = (bf16[3,192,256]{2,1,0:T(8,128)(2,1)S(1)}, bf16[3,192,256]{2,1,0:T(8,128)(2,1)S(1)}, u32[]{:S(2)}, u32[]{:S(2)}) collective-permute-start(bf16[3,192,256]{2,1,0:T(8,128)(2,1)S(1)} %copy-done.30), channel_id=1, source_target_pairs={{0,6},{2,0},{4,2},{6,4},{1,7},{3,1},{5,3},{7,5},{8,14},{10,8},{12,... | collective-permute-start | bytes 884744 | tf_op jit(solution)/shard_map/ppermute | solution.py:537
  196.5 23.1 %collective-permute-start.26 = (bf16[3,192,256]{2,1,0:T(8,128)(2,1)S(1)}, bf16[3,192,256]{2,1,0:T(8,128)(2,1)S(1)}, u32[]{:S(2)}, u32[]{:S(2)}) collective-permute-start(bf16[3,192,256]{2,1,0:T(8,128)(2,1)S(1)} %copy-done.29), channel_id=1, source_target_pairs={{0,2},{2,4},{4,6},{6,0},{1,3},{3,5},{5,7},{7,1},{8,10},{10,12},{12... | collective-permute-start | bytes 884744 | tf_op jit(solution)/shard_map/ppermute | solution.py:537
  196.6 30.5 %collective-permute-start.27 = (bf16[3,192,256]{2,1,0:T(8,128)(2,1)S(1)}, bf16[3,192,256]{2,1,0:T(8,128)(2,1)S(1)}, u32[]{:S(2)}, u32[]{:S(2)}) collective-permute-start(bf16[3,192,256]{2,1,0:T(8,128)(2,1)S(1)} %copy-done.28), channel_id=1, source_target_pairs={{0,4},{2,6},{4,0},{6,2},{1,5},{3,7},{5,1},{7,3},{8,12},{10,14},{12... | collective-permute-start | bytes 884744 | tf_op jit(solution)/shard_map/ppermute | solution.py:537
  235.8 48.1 %collective-permute-start.28 = (bf16[3,2048,128]{2,1,0:T(8,128)(2,1)}, bf16[3,2048,128]{2,1,0:T(8,128)(2,1)S(1)}, u32[]{:S(2)}, u32[]{:S(2)}) collective-permute-start(bf16[3,2048,128]{2,1,0:T(8,128)(2,1)} %get-tuple-element.61), channel_id=1, source_target_pairs={{0,1},{1,0},{2,3},{3,2},{4,5},{5,4},{6,7},{7,6},{8,9},{9,8},{10,11... | collective-permute-start | bytes 4718600 | tf_op jit(solution)/shard_map/ppermute | solution.py:537
  237.8 21.5 %collective-permute-start.30 = (bf16[8,64,352]{2,1,0:T(8,128)(2,1)}, bf16[8,64,352]{2,1,0:T(8,128)(2,1)S(1)}, u32[]{:S(2)}, u32[]{:S(2)}) collective-permute-start(bf16[8,64,352]{2,1,0:T(8,128)(2,1)} %get-tuple-element.67), channel_id=1, source_target_pairs={{0,16},{8,24},{16,0},{24,8},{1,17},{9,25},{17,1},{25,9},{2,18},{10... | collective-permute-start | bytes 1081352 | tf_op jit(solution)/shard_map/ppermute | solution.py:537
  240.4 18.9 %collective-permute-start.31 = (bf16[8,64,352]{2,1,0:T(8,128)(2,1)}, bf16[8,64,352]{2,1,0:T(8,128)(2,1)}, u32[]{:S(2)}, u32[]{:S(2)}) collective-permute-start(bf16[8,64,352]{2,1,0:T(8,128)(2,1)} %get-tuple-element.68), channel_id=1, source_target_pairs={{0,24},{8,0},{16,8},{24,16},{1,25},{9,1},{17,9},{25,17},{2,26},{10... | collective-permute-start | bytes 1081352 | tf_op jit(solution)/shard_map/ppermute | solution.py:537
  242.1 19.1 %all-to-all-start.3 = ((f32[32,2,352]{2,1,0:T(2,128)}), f32[32,2,352]{2,1,0:T(2,128)S(1)}, u32[]{:S(2)}, u32[]{:S(2)}) async-start(f32[32,2,352]{2,1,0:T(2,128)} %broadcast_in_dim.27), calls=%async_computation.3 | async-start | bytes 196608 | tf_op jit(solution)/shard_map/all_to_all | solution.py:587
  261.3 21.9 %all-to-all-start.2 = ((bf16[8,64,352]{2,1,0:T(8,128)(2,1)}), bf16[8,64,352]{2,1,0:T(8,128)(2,1)S(1)}, u32[]{:S(2)}, u32[]{:S(2)}) async-start(bf16[8,64,352]{2,1,0:T(8,128)(2,1)} %add_convert_fusion), calls=%async_computation.2 | async-start | bytes 786432 | tf_op jit(solution)/shard_map/all_to_all | solution.py:589
  (43 other events, 526.4 us)

commit v4 on v3

--- a/solution.py
+++ b/solution.py
@@ -230,7 +230,7 @@
                 copies[j].append(pltpu.make_async_copy(src, dst, sems.at[j, 4 * side + n]))
     rows_in = [pltpu.make_async_copy(rows_hbm.at[n], rows_ref.at[n], row_sems.at[n]) for n in range(2)]
     acts_out = [pltpu.make_async_copy(made.at[n], acts[n], act_sems.at[n]) for n in range(4)]
-    for copy in [rows_in[0], *copies[0], rows_in[1]]:
+    for copy in [rows_in[0], *copies[0], rows_in[1], *copies[1], *copies[2], *copies[3]]:
         copy.start()
     for copy in rows_in:
         copy.wait()
@@ -241,9 +241,6 @@
             def _():
                 for copy in copies[n]:
                     copy.wait()
-                if n < 3:
-                    for copy in copies[n + 1]:
-                        copy.start()
 
         at = pl.multiple_of(512 * j, 512)
         both = dot(rows_ref[0], gate_up[:, pl.ds(at, 512)])
@@ -324,7 +321,7 @@
 
 
 def weight_grads(rows, far, acts):
-    block = 256
+    block = 512
     sums = pl.BlockSpec((3, block, 128), lambda t: (0, t, 0))
     return pl.pallas_call(
         weight_grad_kernel,
@@ -338,7 +335,7 @@
             pltpu.VMEM((4 * ROWS, 768), BF16),
             pltpu.VMEM((256, 4 * ROWS), BF16),
         ],
-        compiler_params=vmem(12),
+        compiler_params=vmem(20),
         name="weight_grads",
     )(*rows, *far, *acts)
 

time: 290 us -> 288 us (level)
  no operation moved by 1% of the time
where the time goes in v4:
time: 288 us; the launch traced here: 286 us
  waiting for transfers between devices  133 us (46%)
  starting transfers between devices  71.6 us (25%)
  Pallas kernels  62.3 us (22%)
  local copies, waits for them, and re-layouts  15.1 us (5%)
    ppermute x32, waiting for transfers between devices, shifted(): return lax.ppermute(value, axis, [(i, (i + by) % n) for i in range(n)])  129 us
    ppermute x32, starting transfers between devices, shifted(): return lax.ppermute(value, axis, [(i, (i + by) % n) for i in range(n)])  30.2 us
    pallas_call x1, Pallas kernels, experts(): pl.pallas_call(expert_kernel, in_specs=[anywhere] * 17, out_specs=(pl.Blo...  15.8 us
    all_to_all x1, starting transfers between devices, on_device(): lax.all_to_all(back.reshape(N_EXP * N_TP, 16, 128), ALL, split_axis=0, co...  13.6 us
    all_to_all x1, starting transfers between devices, on_device(): got = lax.all_to_all(sent, SP, split_axis=0, concat_axis=0, tiled=True)  11.3 us
    unnamed x63, local copies, waits for them, and re-layouts  10.3 us
    all_to_all x1, starting transfers between devices, on_device(): links = lax.all_to_all(link, SP, split_axis=0, concat_axis=0, tiled=True)  8.57 us
    pallas_call x1, Pallas kernels, prepare(): pl.pallas_call(prepare_kernel, out_shape=(pltpu.HBM(shape[::-1], BF16), w...  8.11 us
  transfers between devices with their start and end apart: 36, of which 14 were waited for; matrix products, arithmetic and copies ran while one was open for 3% of the time, Pallas kernels for 14%

profile of v4, /device:TPU:8, one launch (start us, length us, event | category | flops | bytes accessed | tf_op | source)
XLA Modules:
  0.0 285.7 jit_solution(3858431654280013354)
XLA Ops:
  4.8 4.1 %dispatch.1 = bf16[32,24,1024]{2,1,0:T(8,128)(2,1)} custom-call(s32[1]{0:T(128)} %bitcast.tp_ref, s32[2,384]{1,0:T(2,128)S(1)} %bitcast.36, f32[2,384]{1,0:T(2,128)S(1)} %bitcast.37, bf16[384,2048]{1,0:T(8,128)(2,1)S(1)} %copy-done.3, bf16[384,2048]{1,0:T(8,128)(2,1)S(1)} %copy-done.3, bf16[384,2048]{1,0:T(8,128)(2,1)S(1)} %copy-done.1, ...), custom_call_target="tpu_custom_call" | custom-call | tf_op jit(solution)/shard_map/dispatch/pallas_call | solution.py:134
  9.0 11.3 %all-to-all-start = ((bf16[32,24,1024]{2,1,0:T(8,128)(2,1)}), bf16[32,24,1024]{2,1,0:T(8,128)(2,1)S(1)}, u32[]{:S(2)}, u32[]{:S(2)}) async-start(bf16[32,24,1024]{2,1,0:T(8,128)(2,1)} %dispatch.1), calls=%async_computation | async-start | bytes 3145728 | tf_op jit(solution)/shard_map/all_to_all | solution.py:554
  26.9 16.6 %collective-permute-done.2.refs_2_ = bf16[3072,128]{1,0:T(8,128)(2,1)S(1)} collective-permute-done((bf16[3072,128]{1,0:T(8,128)(2,1)}, bf16[3072,128]{1,0:T(8,128)(2,1)S(1)}, u32[]{:S(2)}, u32[]{:S(2)}) %collective-permute-start.2) | collective-permute-done | bytes 786464 | tf_op jit(solution)/shard_map/ppermute | solution.py:534
  46.3 14.0 %collective-permute-done.3.refs_3_ = bf16[3072,128]{1,0:T(8,128)(2,1)S(1)} collective-permute-done((bf16[3072,128]{1,0:T(8,128)(2,1)}, bf16[3072,128]{1,0:T(8,128)(2,1)S(1)}, u32[]{:S(2)}, u32[]{:S(2)}) %collective-permute-start.3) | collective-permute-done | bytes 786464 | tf_op jit(solution)/shard_map/ppermute | solution.py:534
  64.5 11.4 %collective-permute-done.6.refs_6_ = bf16[3072,128]{1,0:T(8,128)(2,1)} collective-permute-done((bf16[3072,128]{1,0:T(8,128)(2,1)S(1)}, bf16[3072,128]{1,0:T(8,128)(2,1)}, u32[]{:S(2)}, u32[]{:S(2)}) %collective-permute-start.6) | collective-permute-done | bytes 786464 | tf_op jit(solution)/shard_map/ppermute | solution.py:534
  81.8 15.8 %experts.1 = (bf16[32,8,16,128]{3,2,1,0:T(8,128)(2,1)}, bf16[3,192,256]{2,1,0:T(8,128)(2,1)}, bf16[3,192,256]{2,1,0:T(8,128)(2,1)}, bf16[3,192,256]{2,1,0:T(8,128)(2,1)}, bf16[3,192,256]{2,1,0:T(8,128)(2,1)}) custom-call(bf16[2,192,2048]{2,1,0:T(8,128)(2,1)} %select.3.rows_hbm.rows_0, bf16[3072,128]{1,0:T(8,128)(2,1)} %get-tuple-element.42.refs_0_, ...), custom_call_target="tpu_custom_call" | custom-call | tf_op jit(solution)/shard_map/experts/pallas_call | solution.py:282
  97.6 13.6 %all-to-all-start.1 = ((bf16[256,16,128]{2,1,0:T(8,128)(2,1)}), bf16[256,16,128]{2,1,0:T(8,128)(2,1)}, u32[]{:S(2)}, u32[]{:S(2)}) async-start(bf16[256,16,128]{2,1,0:T(8,128)(2,1)} %bitcast.38), calls=%async_computation.1 | async-start | bytes 2097152 | tf_op jit(solution)/shard_map/all_to_all | solution.py:567
  115.0 4.7 %collective-permute-done.rows_1 = bf16[2,192,2048]{2,1,0:T(8,128)(2,1)} collective-permute-done((bf16[2,192,2048]{2,1,0:T(8,128)(2,1)}, bf16[2,192,2048]{2,1,0:T(8,128)(2,1)}, u32[]{:S(2)}, u32[]{:S(2)}) %collective-permute-start) | collective-permute-done | bytes 1572896 | tf_op jit(solution)/shard_map/ppermute | solution.py:534
  121.8 36.1 %collective-permute-done.1.rows_2 = bf16[2,192,2048]{2,1,0:T(8,128)(2,1)} collective-permute-done((bf16[2,192,2048]{2,1,0:T(8,128)(2,1)S(1)}, bf16[2,192,2048]{2,1,0:T(8,128)(2,1)}, u32[]{:S(2)}, u32[]{:S(2)}) %collective-permute-start.1) | collective-permute-done | bytes 1572896 | tf_op jit(solution)/shard_map/ppermute | solution.py:534
  166.9 3.3 %collective-permute-done.16.refs_1_ = bf16[256,384]{1,0:T(8,128)(2,1)S(1)} collective-permute-done((bf16[256,384]{1,0:T(8,128)(2,1)S(1)}, bf16[256,384]{1,0:T(8,128)(2,1)S(1)}, u32[]{:S(2)}, u32[]{:S(2)}) %collective-permute-start.16) | collective-permute-done | bytes 196640 | tf_op jit(solution)/shard_map/ppermute | solution.py:534
  170.8 4.6 %collective-permute-done.18.refs_3_ = bf16[256,384]{1,0:T(8,128)(2,1)S(1)} collective-permute-done((bf16[256,384]{1,0:T(8,128)(2,1)S(1)}, bf16[256,384]{1,0:T(8,128)(2,1)S(1)}, u32[]{:S(2)}, u32[]{:S(2)}) %collective-permute-start.18) | collective-permute-done | bytes 196640 | tf_op jit(solution)/shard_map/ppermute | solution.py:534
  175.4 8.1 %prepare.1 = (bf16[384,352]{1,0:T(8,128)(2,1)}, f32[352,384]{1,0:T(8,128)}, f32[352,384]{1,0:T(8,128)}, f32[352,384]{1,0:T(8,128)}, f32[352,384]{1,0:T(8,128)}) custom-call(bf16[352,384]{1,0:T(8,128)(2,1)S(1)} %bitcast.34, f32[352,384]{1,0:T(8,128)S(1)} %bitcast.28, f32[352,384]{1,0:T(8,128)S(1)} %bitcast.31, bf16[352,384]{1,0:T(8,128)(2,1)S(1)} %bitcast.35), custom_call_target="tpu_custom_call" | custom-call | tf_op jit(solution)/shard_map/prepare/pallas_call | solution.py:429
  187.7 4.2 %project.1 = (bf16[8,64,352]{2,1,0:T(8,128)(2,1)}, bf16[8,64,352]{2,1,0:T(8,128)(2,1)}, bf16[8,64,352]{2,1,0:T(8,128)(2,1)}, bf16[8,64,352]{2,1,0:T(8,128)(2,1)}...) custom-call(s32[9]{0:T(128)S(1)} %pad_add_fusion.order_ref, ...), custom_call_target="tpu_custom_call" | custom-call | tf_op jit(solution)/shard_map/project/pallas_call | solution.py:462
  196.3 4.0 %collective-permute-start.27 = (bf16[3,192,256]{2,1,0:T(8,128)(2,1)S(1)}, bf16[3,192,256]{2,1,0:T(8,128)(2,1)S(1)}, u32[]{:S(2)}, u32[]{:S(2)}) collective-permute-start(bf16[3,192,256]{2,1,0:T(8,128)(2,1)S(1)} %copy-done.28), channel_id=1, source_target_pairs={{0,4},{2,6},{4,0},{6,2},{1,5},{3,7},{5,1},{7,3},{8,12},{10,14},{12... | collective-permute-start | bytes 884744 | tf_op jit(solution)/shard_map/ppermute | solution.py:534
  200.3 19.1 %collective-permute-done.25.act_1 = bf16[3,192,256]{2,1,0:T(8,128)(2,1)S(1)} collective-permute-done((bf16[3,192,256]{2,1,0:T(8,128)(2,1)S(1)}, bf16[3,192,256]{2,1,0:T(8,128)(2,1)S(1)}, u32[]{:S(2)}, u32[]{:S(2)}) %collective-permute-start.25) | collective-permute-done | bytes 294944 | tf_op jit(solution)/shard_map/ppermute | solution.py:534
  219.4 7.4 %collective-permute-done.27.act_3 = bf16[3,192,256]{2,1,0:T(8,128)(2,1)S(1)} collective-permute-done((bf16[3,192,256]{2,1,0:T(8,128)(2,1)S(1)}, bf16[3,192,256]{2,1,0:T(8,128)(2,1)S(1)}, u32[]{:S(2)}, u32[]{:S(2)}) %collective-permute-start.27) | collective-permute-done | bytes 294944 | tf_op jit(solution)/shard_map/ppermute | solution.py:534
  226.8 6.5 %weight_grads.1 = (f32[3,2048,128]{2,1,0:T(8,128)}, bf16[3,2048,128]{2,1,0:T(8,128)(2,1)}) custom-call(bf16[2,192,2048]{2,1,0:T(8,128)(2,1)S(1)} %copy-done, bf16[2,192,2048]{2,1,0:T(8,128)(2,1)} %collective-permute-done.rows_1, bf16[2,192,2048]{2,1,0:T(8,128)(2,1)} %collective-permute-done.1.rows_2, bf16[192,2048]{1,0:T(8,128)(2,1)S(1)} %collective-permute-done.23.far_in, ...), custom_call_target="tpu_custom_call" | custom-call | tf_op jit(solution)/shard_map/weight_grads/pallas_call | solution.py:326
  235.3 2.6 collective-permute-start.30
  239.7 8.6 %all-to-all-start.3 = ((f32[32,2,352]{2,1,0:T(2,128)}), f32[32,2,352]{2,1,0:T(2,128)S(1)}, u32[]{:S(2)}, u32[]{:S(2)}) async-start(f32[32,2,352]{2,1,0:T(2,128)} %broadcast_in_dim.27), calls=%async_computation.3 | async-start | bytes 196608 | tf_op jit(solution)/shard_map/all_to_all | solution.py:584
  248.3 8.6 %collective-permute-done.30 = bf16[8,64,352]{2,1,0:T(8,128)(2,1)S(1)} collective-permute-done((bf16[8,64,352]{2,1,0:T(8,128)(2,1)}, bf16[8,64,352]{2,1,0:T(8,128)(2,1)S(1)}, u32[]{:S(2)}, u32[]{:S(2)}) %collective-permute-start.30) | collective-permute-done | bytes 360480 | tf_op jit(solution)/shard_map/ppermute | solution.py:534
  258.8 7.9 %all-to-all-start.2 = ((bf16[8,64,352]{2,1,0:T(8,128)(2,1)}), bf16[8,64,352]{2,1,0:T(8,128)(2,1)S(1)}, u32[]{:S(2)}, u32[]{:S(2)}) async-start(bf16[8,64,352]{2,1,0:T(8,128)(2,1)} %add_convert_fusion), calls=%async_computation.2 | async-start | bytes 786432 | tf_op jit(solution)/shard_map/all_to_all | solution.py:586
  266.7 8.0 %local_scan.1.local_ref = f32[352,384]{1,0:T(8,128)S(1)} custom-call(f32[352,384]{1,0:T(8,128)} %get-tuple-element.71.direct_ref, f32[352,384]{1,0:T(8,128)S(1)} %bitcast.29), custom_call_target="tpu_custom_call" | custom-call | tf_op jit(solution)/shard_map/local_scan/pallas_call | solution.py:497
  277.1 3.6 %all-to-all-done.2 = bf16[8,64,352]{2,1,0:T(8,128)(2,1)S(1)} async-done(((bf16[8,64,352]{2,1,0:T(8,128)(2,1)}), bf16[8,64,352]{2,1,0:T(8,128)(2,1)S(1)}, u32[]{:S(2)}, u32[]{:S(2)}) %all-to-all-start.2) | async-done | bytes 360480 | tf_op jit(solution)/shard_map/all_to_all | solution.py:586
  281.5 4.2 %finish.1 = (f32[2048,128]{1,0:T(8,128)}, f32[2048,128]{1,0:T(8,128)}, f32[128,2048]{1,0:T(8,128)}) custom-call(f32[3,2048,128]{2,1,0:T(8,128)} %get-tuple-element.60.keep_ref, bf16[3,2048,128]{2,1,0:T(8,128)(2,1)S(1)} %collective-permute-done.28.got_ref), custom_call_target="tpu_custom_call" | custom-call | tf_op jit(solution)/shard_map/finish/pallas_call | solution.py:355
  (131 shorter events, 56.4 us)
Async XLA Ops:
  9.0 68.8 %all-to-all-start = ((bf16[32,24,1024]{2,1,0:T(8,128)(2,1)}), bf16[32,24,1024]{2,1,0:T(8,128)(2,1)S(1)}, u32[]{:S(2)}, u32[]{:S(2)}) async-start(bf16[32,24,1024]{2,1,0:T(8,128)(2,1)} %dispatch.1), calls=%async_computation | async-start | bytes 3145728 | tf_op jit(solution)/shard_map/all_to_all | solution.py:554
  22.8 20.7 %collective-permute-start.2 = (bf16[3072,128]{1,0:T(8,128)(2,1)}, bf16[3072,128]{1,0:T(8,128)(2,1)S(1)}, u32[]{:S(2)}, u32[]{:S(2)}) collective-permute-start(bf16[3072,128]{1,0:T(8,128)(2,1)} %get-tuple-element.42.refs_0_), channel_id=1, source_target_pairs={{0,2},{2,4},{4,6},{6,0},{1,3},{3,5},{5,7},{7,1},{8,10},{10,12},{12... | collective-permute-start | bytes 2359304 | tf_op jit(solution)/shard_map/ppermute | solution.py:534
  24.4 20.6 %collective-permute-start.5 = (bf16[3072,128]{1,0:T(8,128)(2,1)}, bf16[3072,128]{1,0:T(8,128)(2,1)S(1)}, u32[]{:S(2)}, u32[]{:S(2)}) collective-permute-start(bf16[3072,128]{1,0:T(8,128)(2,1)} %get-tuple-element.43.refs_1_), channel_id=1, source_target_pairs={{0,6},{2,0},{4,2},{6,4},{1,7},{3,1},{5,3},{7,5},{8,14},{10,8},{12,... | collective-permute-start | bytes 2359304 | tf_op jit(solution)/shard_map/ppermute | solution.py:534
  24.9 35.5 %collective-permute-start.3 = (bf16[3072,128]{1,0:T(8,128)(2,1)}, bf16[3072,128]{1,0:T(8,128)(2,1)S(1)}, u32[]{:S(2)}, u32[]{:S(2)}) collective-permute-start(bf16[3072,128]{1,0:T(8,128)(2,1)} %get-tuple-element.43.refs_1_), channel_id=1, source_target_pairs={{0,2},{2,4},{4,6},{6,0},{1,3},{3,5},{5,7},{7,1},{8,10},{10,12},{12... | collective-permute-start | bytes 2359304 | tf_op jit(solution)/shard_map/ppermute | solution.py:534
  26.4 35.5 %collective-permute-start.4 = (bf16[3072,128]{1,0:T(8,128)(2,1)}, bf16[3072,128]{1,0:T(8,128)(2,1)S(1)}, u32[]{:S(2)}, u32[]{:S(2)}) collective-permute-start(bf16[3072,128]{1,0:T(8,128)(2,1)} %get-tuple-element.42.refs_0_), channel_id=1, source_target_pairs={{0,6},{2,0},{4,2},{6,4},{1,7},{3,1},{5,3},{7,5},{8,14},{10,8},{12,... | collective-permute-start | bytes 2359304 | tf_op jit(solution)/shard_map/ppermute | solution.py:534
  26.9 35.1 %collective-permute-start.8 = (bf16[3072,128]{1,0:T(8,128)(2,1)}, bf16[3072,128]{1,0:T(8,128)(2,1)S(1)}, u32[]{:S(2)}, u32[]{:S(2)}) collective-permute-start(bf16[3072,128]{1,0:T(8,128)(2,1)} %get-tuple-element.42.refs_0_), channel_id=1, source_target_pairs={{0,1},{1,0},{2,3},{3,2},{4,5},{5,4},{6,7},{7,6},{8,9},{9,8},{10,11... | collective-permute-start | bytes 2359304 | tf_op jit(solution)/shard_map/ppermute | solution.py:534
  43.5 20.4 %collective-permute-start.9 = (bf16[3072,128]{1,0:T(8,128)(2,1)}, bf16[3072,128]{1,0:T(8,128)(2,1)}, u32[]{:S(2)}, u32[]{:S(2)}) collective-permute-start(bf16[3072,128]{1,0:T(8,128)(2,1)} %get-tuple-element.43.refs_1_), channel_id=1, source_target_pairs={{0,1},{1,0},{2,3},{3,2},{4,5},{5,4},{6,7},{7,6},{8,9},{9,8},{10,11... | collective-permute-start | bytes 2359304 | tf_op jit(solution)/shard_map/ppermute | solution.py:534
  45.0 30.8 %collective-permute-start.6 = (bf16[3072,128]{1,0:T(8,128)(2,1)S(1)}, bf16[3072,128]{1,0:T(8,128)(2,1)}, u32[]{:S(2)}, u32[]{:S(2)}) collective-permute-start(bf16[3072,128]{1,0:T(8,128)(2,1)S(1)} %collective-permute-done.2.refs_2_), channel_id=1, source_target_pairs={{0,2},{2,4},{4,6},{6,0},{1,3},{3,5},{5,7},{7,1},{8,10},{10,12},{12... | collective-permute-start | bytes 2359304 | tf_op jit(solution)/shard_map/ppermute | solution.py:534
  60.3 16.8 %collective-permute-start.7 = (bf16[3072,128]{1,0:T(8,128)(2,1)S(1)}, bf16[3072,128]{1,0:T(8,128)(2,1)}, u32[]{:S(2)}, u32[]{:S(2)}) collective-permute-start(bf16[3072,128]{1,0:T(8,128)(2,1)S(1)} %collective-permute-done.5.refs_5_), channel_id=1, source_target_pairs={{0,6},{2,0},{4,2},{6,4},{1,7},{3,1},{5,3},{7,5},{8,14},{10,8},{12,... | collective-permute-start | bytes 2359304 | tf_op jit(solution)/shard_map/ppermute | solution.py:534
  63.9 17.9 %collective-permute-start.11 = (bf16[3072,128]{1,0:T(8,128)(2,1)}, bf16[3072,128]{1,0:T(8,128)(2,1)}, u32[]{:S(2)}, u32[]{:S(2)}) collective-permute-start(bf16[3072,128]{1,0:T(8,128)(2,1)} %copy-done.21), channel_id=1, source_target_pairs={{0,1},{1,0},{2,3},{3,2},{4,5},{5,4},{6,7},{7,6},{8,9},{9,8},{10,11... | collective-permute-start | bytes 2359304 | tf_op jit(solution)/shard_map/ppermute | solution.py:534
  79.7 40.0 %collective-permute-start = (bf16[2,192,2048]{2,1,0:T(8,128)(2,1)}, bf16[2,192,2048]{2,1,0:T(8,128)(2,1)}, u32[]{:S(2)}, u32[]{:S(2)}) collective-permute-start(bf16[2,192,2048]{2,1,0:T(8,128)(2,1)} %select.3.rows_hbm.rows_0), channel_id=1, source_target_pairs={{0,6},{2,0},{4,2},{6,4},{1,7},{3,1},{5,3},{7,5},{8,14},{10,8},{12,... | collective-permute-start | bytes 4718600 | tf_op jit(solution)/shard_map/ppermute | solution.py:534
  97.6 62.4 %all-to-all-start.1 = ((bf16[256,16,128]{2,1,0:T(8,128)(2,1)}), bf16[256,16,128]{2,1,0:T(8,128)(2,1)}, u32[]{:S(2)}, u32[]{:S(2)}) async-start(bf16[256,16,128]{2,1,0:T(8,128)(2,1)} %bitcast.38), calls=%async_computation.1 | async-start | bytes 2097152 | tf_op jit(solution)/shard_map/all_to_all | solution.py:567
  111.2 46.7 %collective-permute-start.1 = (bf16[2,192,2048]{2,1,0:T(8,128)(2,1)S(1)}, bf16[2,192,2048]{2,1,0:T(8,128)(2,1)}, u32[]{:S(2)}, u32[]{:S(2)}) collective-permute-start(bf16[2,192,2048]{2,1,0:T(8,128)(2,1)S(1)} %copy-done), channel_id=1, source_target_pairs={{0,2},{2,4},{4,6},{6,0},{1,3},{3,5},{5,7},{7,1},{8,10},{10,12},{12... | collective-permute-start | bytes 4718600 | tf_op jit(solution)/shard_map/ppermute | solution.py:534
  166.9 16.6 %collective-permute-start.19 = (bf16[256,384]{1,0:T(8,128)(2,1)S(1)}, bf16[256,384]{1,0:T(8,128)(2,1)S(1)}, u32[]{:S(2)}, u32[]{:S(2)}) collective-permute-start(bf16[256,384]{1,0:T(8,128)(2,1)S(1)} %combine.1.refs_0_), channel_id=1, source_target_pairs={{0,1},{1,0},{2,3},{3,2},{4,5},{5,4},{6,7},{7,6},{8,9},{9,8},{10,11... | collective-permute-start | bytes 589832 | tf_op jit(solution)/shard_map/ppermute | solution.py:534
  191.9 35.0 %collective-permute-start.23 = (bf16[192,2048]{1,0:T(8,128)(2,1)S(1)}, bf16[192,2048]{1,0:T(8,128)(2,1)S(1)}, u32[]{:S(2)}, u32[]{:S(2)}) collective-permute-start(bf16[192,2048]{1,0:T(8,128)(2,1)S(1)} %copy-done.25), channel_id=1, source_target_pairs={{0,2},{2,4},{4,6},{6,0},{1,3},{3,5},{5,7},{7,1},{8,10},{10,12},{12... | collective-permute-start | bytes 2359304 | tf_op jit(solution)/shard_map/ppermute | solution.py:534
  192.0 34.8 %collective-permute-start.24 = (bf16[192,2048]{1,0:T(8,128)(2,1)S(1)}, bf16[192,2048]{1,0:T(8,128)(2,1)S(1)}, u32[]{:S(2)}, u32[]{:S(2)}) collective-permute-start(bf16[192,2048]{1,0:T(8,128)(2,1)S(1)} %copy-done.24), channel_id=1, source_target_pairs={{0,6},{2,0},{4,2},{6,4},{1,7},{3,1},{5,3},{7,5},{8,14},{10,8},{12,... | collective-permute-start | bytes 2359304 | tf_op jit(solution)/shard_map/ppermute | solution.py:534
  194.0 25.3 %collective-permute-start.25 = (bf16[3,192,256]{2,1,0:T(8,128)(2,1)S(1)}, bf16[3,192,256]{2,1,0:T(8,128)(2,1)S(1)}, u32[]{:S(2)}, u32[]{:S(2)}) collective-permute-start(bf16[3,192,256]{2,1,0:T(8,128)(2,1)S(1)} %copy-done.30), channel_id=1, source_target_pairs={{0,6},{2,0},{4,2},{6,4},{1,7},{3,1},{5,3},{7,5},{8,14},{10,8},{12,... | collective-permute-start | bytes 884744 | tf_op jit(solution)/shard_map/ppermute | solution.py:534
  196.3 23.1 %collective-permute-start.26 = (bf16[3,192,256]{2,1,0:T(8,128)(2,1)S(1)}, bf16[3,192,256]{2,1,0:T(8,128)(2,1)S(1)}, u32[]{:S(2)}, u32[]{:S(2)}) collective-permute-start(bf16[3,192,256]{2,1,0:T(8,128)(2,1)S(1)} %copy-done.29), channel_id=1, source_target_pairs={{0,2},{2,4},{4,6},{6,0},{1,3},{3,5},{5,7},{7,1},{8,10},{10,12},{12... | collective-permute-start | bytes 884744 | tf_op jit(solution)/shard_map/ppermute | solution.py:534
  196.3 30.5 %collective-permute-start.27 = (bf16[3,192,256]{2,1,0:T(8,128)(2,1)S(1)}, bf16[3,192,256]{2,1,0:T(8,128)(2,1)S(1)}, u32[]{:S(2)}, u32[]{:S(2)}) collective-permute-start(bf16[3,192,256]{2,1,0:T(8,128)(2,1)S(1)} %copy-done.28), channel_id=1, source_target_pairs={{0,4},{2,6},{4,0},{6,2},{1,5},{3,7},{5,1},{7,3},{8,12},{10,14},{12... | collective-permute-start | bytes 884744 | tf_op jit(solution)/shard_map/ppermute | solution.py:534
  233.4 48.1 %collective-permute-start.28 = (bf16[3,2048,128]{2,1,0:T(8,128)(2,1)}, bf16[3,2048,128]{2,1,0:T(8,128)(2,1)S(1)}, u32[]{:S(2)}, u32[]{:S(2)}) collective-permute-start(bf16[3,2048,128]{2,1,0:T(8,128)(2,1)} %get-tuple-element.61), channel_id=1, source_target_pairs={{0,1},{1,0},{2,3},{3,2},{4,5},{5,4},{6,7},{7,6},{8,9},{9,8},{10,11... | collective-permute-start | bytes 4718600 | tf_op jit(solution)/shard_map/ppermute | solution.py:534
  235.3 21.5 %collective-permute-start.30 = (bf16[8,64,352]{2,1,0:T(8,128)(2,1)}, bf16[8,64,352]{2,1,0:T(8,128)(2,1)S(1)}, u32[]{:S(2)}, u32[]{:S(2)}) collective-permute-start(bf16[8,64,352]{2,1,0:T(8,128)(2,1)} %get-tuple-element.67), channel_id=1, source_target_pairs={{0,16},{8,24},{16,0},{24,8},{1,17},{9,25},{17,1},{25,9},{2,18},{10... | collective-permute-start | bytes 1081352 | tf_op jit(solution)/shard_map/ppermute | solution.py:534
  237.9 18.9 %collective-permute-start.31 = (bf16[8,64,352]{2,1,0:T(8,128)(2,1)}, bf16[8,64,352]{2,1,0:T(8,128)(2,1)}, u32[]{:S(2)}, u32[]{:S(2)}) collective-permute-start(bf16[8,64,352]{2,1,0:T(8,128)(2,1)} %get-tuple-element.68), channel_id=1, source_target_pairs={{0,24},{8,0},{16,8},{24,16},{1,25},{9,1},{17,9},{25,17},{2,26},{10... | collective-permute-start | bytes 1081352 | tf_op jit(solution)/shard_map/ppermute | solution.py:534
  239.7 19.1 %all-to-all-start.3 = ((f32[32,2,352]{2,1,0:T(2,128)}), f32[32,2,352]{2,1,0:T(2,128)S(1)}, u32[]{:S(2)}, u32[]{:S(2)}) async-start(f32[32,2,352]{2,1,0:T(2,128)} %broadcast_in_dim.27), calls=%async_computation.3 | async-start | bytes 196608 | tf_op jit(solution)/shard_map/all_to_all | solution.py:584
  258.8 21.9 %all-to-all-start.2 = ((bf16[8,64,352]{2,1,0:T(8,128)(2,1)}), bf16[8,64,352]{2,1,0:T(8,128)(2,1)S(1)}, u32[]{:S(2)}, u32[]{:S(2)}) async-start(bf16[8,64,352]{2,1,0:T(8,128)(2,1)} %add_convert_fusion), calls=%async_computation.2 | async-start | bytes 786432 | tf_op jit(solution)/shard_map/all_to_all | solution.py:586
  (43 other events, 522.2 us)
